TPU v7x, 32 devices: a whole 2x2x4 slice. The times are simulated.
32 devices in a mesh: sp: 8 (over z, core), tp: 4 (over y, x).
Axes of the slice: x: 2, y: 2, z: 4, core: 2. Of those that a mesh axis runs over, the one named last changes fastest.
Arguments:
- queries: bfloat16 [2048, 2048], P('sp', 'tp'), may hold values from -6 to 6
- keys: bfloat16 [2048, 256], P('sp'), may hold values from -6 to 6
- values: bfloat16 [2048, 256], P('sp'), may hold values from -6 to 6
- query_gain: float32 [128], replicated, may hold values from 0.1 to 5.5
- key_gain: float32 [128], replicated, may hold values from 0.1 to 5.5
- out_proj: bfloat16 [2048, 2048], P(None, 'tp'), may hold values from -0.125 to 0.125
- expert_norm_scale: float32 [2048], replicated, may hold values from 0.1 to 1.9
- residual: bfloat16 [2048, 2048], P(('sp', 'tp')), may hold values from -6 to 6
- routes: int32 [2048, 2], P(('sp', 'tp')), may hold values from 0 to 7, all different within a row; in each aligned block of 64 rows (0 to 63, 64 to 127, ...) at most 32 rows name the same one
- route_weights: float32 [2048, 2], P(('sp', 'tp')), may hold values from 0.1 to 0.9
- w_gate: bfloat16 [8, 2048, 4096], P('sp', None, 'tp'), may hold values from -0.125 to 0.125
- w_up: bfloat16 [8, 2048, 4096], P('sp', None, 'tp'), may hold values from -0.125 to 0.125
- w_down: bfloat16 [8, 4096, 2048], P('sp', 'tp'), may hold values from -0.09375 to 0.09375
Outputs:
- layer_out: bfloat16 [2048, 2048], P(('sp', 'tp'))
Inputs may be any that keep to these rules, and one draw needn't show every extreme that they name: `routes`: in the rows of one device no expert is named by more than 32 rows, a bound that some block reaches; a row names 2 different experts.
All inputs are finite; a program needn't handle non-finite values.
Results may differ from a plain program's by a relative error of at most 0.0095.
The roundings to bfloat16 on the way count: a program that leaves them out, or rounds other values in their place, can miss the bound.
Values may be sent and summed in bfloat16 or wider, within the bound.
A program may use at most 64 MiB of HBM per device.

v0:
```python
import functools

import jax
import jax.numpy as jnp
from jax import lax
from jax.experimental import pallas as pl
from jax.experimental.pallas import tpu as pltpu
from jax.sharding import PartitionSpec as P

GRID_W = 64


EPS = 1e-06
ROPE_BASE = 10000.0
NEG_START = -1e30


def rotate(field, position):
    half = field.shape[-1] // 2
    quarter = half // 2
    freqs = ROPE_BASE ** (-jnp.arange(quarter, dtype=jnp.float32) / quarter)
    grid_row = (position // GRID_W).astype(jnp.float32)
    grid_col = (position % GRID_W).astype(jnp.float32)

    def turn_half(part, coord):
        angle = coord[:, None] * freqs[None, :]
        cosine = jnp.cos(angle)[:, None, :]
        sine = jnp.sin(angle)[:, None, :]
        first, second = (part[..., :quarter], part[..., quarter:])
        return jnp.concatenate(
            [first * cosine - second * sine, second * cosine + first * sine], axis=-1
        )

    return jnp.concatenate(
        [turn_half(field[..., :half], grid_row), turn_half(field[..., half:], grid_col)], axis=-1
    )


def prepare(field, gain, position):
    count = field.shape[0]
    width = gain.shape[0]
    heads_here = field.shape[1] // width
    values_f = field.reshape(count, heads_here, width).astype(jnp.float32)
    scaled = (
        values_f * lax.rsqrt(jnp.mean(values_f * values_f, axis=-1, keepdims=True) + EPS) * gain
    )
    return rotate(scaled, position).reshape(count, heads_here * width).astype(jnp.bfloat16)


def absorb(carry, query_matrix, key_rows, value_rows, scale):
    count = key_rows.shape[0]
    width = 2048 if count > 2048 and count % 2048 == 0 else count
    key_blocks = key_rows.reshape(count // width, width, key_rows.shape[1], key_rows.shape[2])
    value_blocks = value_rows.reshape(
        count // width, width, value_rows.shape[1], value_rows.shape[2]
    )

    def step(state, block):
        run_max, run_sum, run_acc = state
        key_tile_rows, value_tile_rows = block
        scores = (
            jnp.einsum(
                "hxt,ght->hxg", query_matrix, key_tile_rows, preferred_element_type=jnp.float32
            )
            * scale
        )
        new_max = jnp.maximum(run_max, jnp.max(scores, axis=-1))
        weight_tensors = jnp.exp(scores - new_max[..., None]).astype(jnp.bfloat16)
        factor = jnp.exp(run_max - new_max)
        run_sum = run_sum * factor + jnp.sum(weight_tensors.astype(jnp.float32), axis=-1)
        run_acc = run_acc * factor[..., None] + jnp.einsum(
            "zij,jzu->ziu", weight_tensors, value_tile_rows, preferred_element_type=jnp.float32
        )
        return ((new_max, run_sum, run_acc), None)

    result, unused = lax.scan(step, carry, (key_blocks, value_blocks))
    return result


MESH = pl.DeviceIdType.MESH
VMEM_LIMIT = 60 * 1024 * 1024


def greet(partners, count):
    barrier = pltpu.get_barrier_semaphore()
    for where in partners:
        pl.semaphore_signal(barrier, inc=1, device_id=where, device_id_type=MESH)
    pl.semaphore_wait(barrier, count)


def remote(src, dst, send, recv, where):
    return pltpu.make_async_remote_copy(
        src_ref=src, dst_ref=dst, send_sem=send, recv_sem=recv, device_id=where, device_id_type=MESH
    )


def square():
    mine = lax.axis_index("tp")
    return mine, mine + 1 - 2 * lax.rem(mine, 2), lax.rem(mine + 2, 4), 3 - mine


def gather_kernel(n, k_ref, v_ref, ko_ref, vo_ref, send, recv):
    me = lax.axis_index("sp")
    chips = n // 2
    chip, core = me // 2, lax.rem(me, 2)
    partner = 2 * chip + 1 - core
    rows = k_ref.shape[0]
    has_right, has_left = chip < chips - 1, chip > 0
    right, left = me + 2, me - 2
    barrier = pltpu.get_barrier_semaphore()
    pl.semaphore_signal(barrier, inc=1, device_id={"sp": partner}, device_id_type=MESH)

    @pl.when(has_right)
    def _():
        pl.semaphore_signal(barrier, inc=1, device_id={"sp": right}, device_id_type=MESH)

    @pl.when(has_left)
    def _():
        pl.semaphore_signal(barrier, inc=1, device_id={"sp": left}, device_id_type=MESH)

    pl.semaphore_wait(barrier, 1 + has_right.astype(jnp.int32) + has_left.astype(jnp.int32))

    def block(out, origin):
        return out.at[pl.ds(pl.multiple_of(origin * rows, rows), rows)]

    def copies(origin, way, where, own=False):
        return [
            remote(
                ref if own else block(out, origin),
                block(out, origin),
                send.at[origin, way, i],
                recv.at[origin, i],
                {"sp": where},
            )
            for i, (ref, out) in enumerate(((k_ref, ko_ref), (v_ref, vo_ref)))
        ]

    def start(*args, **kw):
        for c in copies(*args, **kw):
            c.start()

    def sent(*args, **kw):
        for c in copies(*args, **kw):
            c.wait_send()

    def arrived(origin):
        for c in copies(origin, 0, partner):
            c.wait_recv()

    @pl.when(has_right)
    def _():
        start(me, 0, right, own=True)

    @pl.when(has_left)
    def _():
        start(me, 2, left, own=True)

    start(me, 1, partner, own=True)
    block(ko_ref, me)[...] = k_ref[...]
    block(vo_ref, me)[...] = v_ref[...]
    for j in range(1, chips):

        @pl.when(chip - j >= 0)
        def _(origin=me - 2 * j):
            arrived(origin)

            @pl.when(has_right)
            def _():
                start(origin, 0, right)

            start(origin, 1, partner)

        @pl.when(chip + j < chips)
        def _(origin=me + 2 * j):
            arrived(origin)

            @pl.when(has_left)
            def _():
                start(origin, 2, left)

            start(origin, 1, partner)

    for z in range(chips):
        arrived(2 * z + 1 - core)
    sent(me, 1, partner, own=True)

    @pl.when(has_right)
    def _():
        sent(me, 0, right, own=True)

    @pl.when(has_left)
    def _():
        sent(me, 2, left, own=True)

    for j in range(1, chips):

        @pl.when(chip - j >= 0)
        def _(origin=me - 2 * j):
            @pl.when(has_right)
            def _():
                sent(origin, 0, right)

            sent(origin, 1, partner)

        @pl.when(chip + j < chips)
        def _(origin=me + 2 * j):
            @pl.when(has_left)
            def _():
                sent(origin, 2, left)

            sent(origin, 1, partner)


def in_vmem(count):
    return [pl.BlockSpec(memory_space=pltpu.VMEM)] * count


def params(number):
    return pltpu.CompilerParams(
        collective_id=number, has_side_effects=True, vmem_limit_bytes=VMEM_LIMIT
    )


def gather_rows(n, own_keys, own_values):
    rows, width = own_keys.shape
    shape = jax.ShapeDtypeStruct((n * rows, width), own_keys.dtype)
    return pl.pallas_call(
        functools.partial(gather_kernel, n),
        out_shape=(shape, shape),
        in_specs=in_vmem(2),
        out_specs=tuple(in_vmem(2)),
        scratch_shapes=[pltpu.SemaphoreType.DMA((n, 3, 2)), pltpu.SemaphoreType.DMA((n, 2))],
        compiler_params=params(0),
        name="gather_rows",
    )(own_keys, own_values)


def project_kernel(attn_ref, w_ref, out_ref, held, stage, send, recv, give, take):
    mine, across, along, corner = square()
    rows, width = attn_ref.shape
    half = rows // 2
    share = out_ref.shape[0]
    greet([{"tp": across}, {"tp": along}, {"tp": corner}], 3)
    first = [
        remote(attn_ref, held.at[mine], send.at[0], recv.at[0], {"tp": across}),
        remote(attn_ref, held.at[mine], send.at[1], recv.at[1], {"tp": along}),
    ]
    for c in first:
        c.start()
    top, low = pl.ds(0, half), pl.ds(half, half)
    second = [
        remote(held.at[across, top], held.at[across, top], send.at[2], recv.at[2], {"tp": along}),
        remote(held.at[along, low], held.at[along, low], send.at[3], recv.at[3], {"tp": across}),
    ]

    def term(rows_here, owner):
        part = w_ref[pl.ds(pl.multiple_of(owner * width, width), width), :]
        return jnp.dot(rows_here, part, preferred_element_type=jnp.float32)

    total = term(attn_ref[...], mine)
    first[0].wait_recv()
    second[0].start()
    first[1].wait_recv()
    second[1].start()
    total += term(held[across], across)
    total += term(held[along], along)
    for c in second:
        c.wait_recv()
    total += term(held[corner], corner)
    stage[...] = total.astype(stage.dtype)
    columns = pl.ds(pl.multiple_of(mine * width, width), width)

    def piece(owner):
        return pl.ds(pl.multiple_of(owner * share, share), share)

    back = [
        remote(stage.at[piece(p)], out_ref.at[:, columns], give.at[i], take.at[i], {"tp": p})
        for i, p in enumerate((corner, across, along))
    ]
    for c in back:
        c.start()
    out_ref[:, columns] = stage[piece(mine), :]
    for c in back:
        c.wait()
    for c in first + second:
        c.wait_send()


def project(attn, out_proj, share):
    rows, width = attn.shape
    parts = out_proj.shape[0] // width
    return pl.pallas_call(
        project_kernel,
        out_shape=jax.ShapeDtypeStruct((share, out_proj.shape[1] * parts), jnp.bfloat16),
        in_specs=in_vmem(2),
        out_specs=in_vmem(1)[0],
        scratch_shapes=[
            pltpu.VMEM((parts, rows, width), jnp.bfloat16),
            pltpu.VMEM((rows, out_proj.shape[1]), jnp.bfloat16),
            pltpu.SemaphoreType.DMA((4,)),
            pltpu.SemaphoreType.DMA((4,)),
            pltpu.SemaphoreType.DMA((3,)),
            pltpu.SemaphoreType.DMA((3,)),
        ],
        compiler_params=params(1),
        name="project",
    )(attn, out_proj)


def everyone(n, me):
    mine, across, along, corner = square()
    peers = [{"sp": lax.rem(me + off, n)} for off in range(1, n)]
    return peers + [{"tp": across}, {"tp": along}]


def dispatch_kernel(
    n, chunks, rows_ref, wg_ref, wu_ref, hidden_ref, held, wg, wu, gate, upper, load, send, recv, send_sq, recv_sq
):
    me = lax.axis_index("sp")
    mine, across, along, corner = square()
    parts, _, capacity, depth = held.shape
    width = depth // chunks
    half = width // 2
    rows = n * capacity
    loads = [
        pltpu.make_async_copy(wg_ref.at[0], wg, load.at[0]),
        pltpu.make_async_copy(wu_ref.at[0], wu, load.at[1]),
    ]
    for c in loads:
        c.start()
    own = pltpu.make_async_copy(rows_ref.at[me], held.at[mine, me], load.at[2])
    own.start()
    greet(everyone(n, me), n + 1)

    def span(k, side=0, size=width):
        return pl.ds(pl.multiple_of(k * width + side * half, half), size)

    def scatter(k, off):
        to = lax.rem(me + off, n)
        return remote(
            rows_ref.at[to, :, span(k)],
            held.at[mine, me, :, span(k)],
            send.at[k, off],
            recv.at[k, off],
            {"sp": to},
        )

    def pass_on(k, way):
        group, cols, where = (
            (mine, span(k), across),
            (mine, span(k), along),
            (across, span(k, 0, half), along),
            (along, span(k, 1, half), across),
        )[way]
        ref = held.at[group, :, :, cols]
        return remote(ref, ref, send_sq.at[k, way], recv_sq.at[k, way], {"tp": where})

    @pl.loop(0, chunks)
    def _(k):
        for off in range(1, n):
            scatter(k, off).start()

    for weight in (gate, upper):
        weight[...] = jnp.zeros_like(weight)
    own.wait()
    for c in loads:
        c.wait()

    def absorb_chunk(group, k):
        block = held[group, :, :, span(k)].reshape(rows, width)
        for total, weight in ((gate, wg), (upper, wu)):
            total[group] += jnp.dot(block, weight[span(k), :], preferred_element_type=jnp.float32)

        @pl.when(k == chunks - 1)
        def _():
            act = jax.nn.silu(gate[group]) * upper[group]
            hidden_ref[group] = act.astype(hidden_ref.dtype)

    @pl.loop(0, chunks + 2)
    def _(step):
        @pl.when(step < chunks)
        def _():
            for off in range(1, n):
                scatter(step, off).wait_recv()
            pass_on(step, 0).start()
            pass_on(step, 1).start()

        @pl.when((step >= 1) & (step <= chunks))
        def _():
            for way in (0, 1):
                pass_on(step - 1, way).wait_recv()
                pass_on(step - 1, way + 2).start()

        @pl.when(step < chunks)
        def _():
            absorb_chunk(mine, step)

        @pl.when((step >= 1) & (step <= chunks))
        def _():
            absorb_chunk(across, step - 1)
            absorb_chunk(along, step - 1)

        @pl.when(step >= 2)
        def _():
            for way in (2, 3):
                pass_on(step - 2, way).wait_recv()
            absorb_chunk(corner, step - 2)

    @pl.loop(0, chunks)
    def _(k):
        for off in range(1, n):
            scatter(k, off).wait_send()
        for way in range(4):
            pass_on(k, way).wait_send()


def dispatch(n, parts, rows, w_gate, w_up, chunks=8):
    count, capacity, width = rows.shape
    depth, units = w_gate.shape[1:]
    total = pltpu.VMEM((parts, count * capacity, units), jnp.float32)
    return pl.pallas_call(
        functools.partial(dispatch_kernel, n, chunks),
        out_shape=jax.ShapeDtypeStruct((parts, count * capacity, units), rows.dtype),
        in_specs=in_vmem(1) + [pl.BlockSpec(memory_space=pl.ANY)] * 2,
        out_specs=in_vmem(1)[0],
        scratch_shapes=[
            pltpu.VMEM((parts, count, capacity, width), rows.dtype),
            pltpu.VMEM((depth, units), w_gate.dtype),
            pltpu.VMEM((depth, units), w_up.dtype),
            total,
            total,
            pltpu.SemaphoreType.DMA((3,)),
            pltpu.SemaphoreType.DMA((chunks, n)),
            pltpu.SemaphoreType.DMA((chunks, n)),
            pltpu.SemaphoreType.DMA((chunks, 4)),
            pltpu.SemaphoreType.DMA((chunks, 4)),
        ],
        compiler_params=params(2),
        name="dispatch",
    )(rows, w_gate, w_up)


def combine_kernel(
    n, chunks, hid_ref, wd_ref, out_ref, wd, part, from_x, from_y, to_y, to_x, last_x, last_y, done,
    load, send, recv, send_sq, recv_sq,
):
    me = lax.axis_index("sp")
    mine, across, along, corner = square()
    x, y = lax.rem(mine, 2), mine // 2
    capacity = out_ref.shape[1]
    half = out_ref.shape[2] // chunks // 2
    low, high = pl.ds(0, half), pl.ds(half, half)

    def span(k):
        return pl.ds(pl.multiple_of(2 * k * half, 2 * half), 2 * half)

    def fetch(k):
        return pltpu.make_async_copy(wd_ref.at[0, :, span(k)], wd.at[k], load.at[k])

    @pl.loop(0, chunks)
    def _(k):
        fetch(k).start()

    greet(everyone(n, me), n + 1)

    def hop(k, way):
        src, dst, where = (
            (part.at[k, :, 1 - x, :, low], from_x.at[k], across),
            (part.at[k, 1 - y, :, :, high], from_y.at[k], along),
            (to_y.at[k], last_y.at[k], along),
            (to_x.at[k], last_x.at[k], across),
        )[way]
        return remote(src, dst, send_sq.at[k, way], recv_sq.at[k, way], {"tp": where})

    def home(k, off):
        to = lax.rem(me + off, n)
        return remote(
            done.at[k, to], out_ref.at[me, :, span(k)], send.at[k, off], recv.at[k, off], {"sp": to}
        )

    def wide(value):
        return value.astype(jnp.float32)

    @pl.loop(0, chunks + 2)
    def _(step):
        @pl.when(step < chunks)
        def _(k=step):
            fetch(k).wait()
            for p in range(4):
                product = jnp.dot(hid_ref[p], wd[k], preferred_element_type=jnp.float32)
                part[k, p // 2, p % 2] = product.astype(part.dtype)
            hop(k, 0).start()
            hop(k, 1).start()

        @pl.when((step >= 1) & (step <= chunks))
        def _(k=step - 1):
            hop(k, 0).wait_recv()
            pair = wide(part[k, 1 - y, x, :, low]) + wide(from_x[k, 1 - y])
            to_y[k] = pair.astype(to_y.dtype)
            hop(k, 2).start()
            hop(k, 1).wait_recv()
            pair = wide(part[k, y, 1 - x, :, high]) + wide(from_y[k, 1 - x])
            to_x[k] = pair.astype(to_x.dtype)
            hop(k, 3).start()

        @pl.when(step >= 2)
        def _(k=step - 2):
            hop(k, 2).wait_recv()
            total = wide(part[k, y, x, :, low]) + wide(from_x[k, y]) + wide(last_y[k])
            done[k, :, :, low] = total.astype(done.dtype).reshape(n, capacity, half)
            hop(k, 3).wait_recv()
            total = wide(part[k, y, x, :, high]) + wide(from_y[k, x]) + wide(last_x[k])
            done[k, :, :, high] = total.astype(done.dtype).reshape(n, capacity, half)
            for off in range(1, n):
                home(k, off).start()
            out_ref[me, :, span(k)] = done[k, me]

    @pl.loop(0, chunks)
    def _(k):
        for off in range(1, n):
            home(k, off).wait()
        for way in range(4):
            hop(k, way).wait_send()


def combine(n, hidden, w_down, capacity, chunks=8):
    rows = hidden.shape[1]
    units, width = w_down.shape[1:]
    half = width // chunks // 2
    kind = hidden.dtype
    one = pltpu.VMEM((chunks, rows, half), kind)
    two = pltpu.VMEM((chunks, 2, rows, half), kind)
    return pl.pallas_call(
        functools.partial(combine_kernel, n, chunks),
        out_shape=jax.ShapeDtypeStruct((n, capacity, width), kind),
        in_specs=in_vmem(1) + [pl.BlockSpec(memory_space=pl.ANY)],
        out_specs=in_vmem(1)[0],
        scratch_shapes=[
            pltpu.VMEM((chunks, units, 2 * half), kind),
            pltpu.VMEM((chunks, 2, 2, rows, 2 * half), kind),
            two,
            two,
            one,
            one,
            one,
            one,
            pltpu.VMEM((chunks, n, capacity, 2 * half), kind),
            pltpu.SemaphoreType.DMA((chunks,)),
            pltpu.SemaphoreType.DMA((chunks, n)),
            pltpu.SemaphoreType.DMA((chunks, n)),
            pltpu.SemaphoreType.DMA((chunks, 4)),
            pltpu.SemaphoreType.DMA((chunks, 4)),
        ],
        compiler_params=params(3),
        name="combine",
    )(hidden, w_down)


def start_state(batch, rows, width):
    return (
        jnp.full((batch, rows), NEG_START, jnp.float32),
        jnp.zeros((batch, rows), jnp.float32),
        jnp.zeros((batch, rows, width), jnp.float32),
    )


def local(
    queries,
    keys,
    values,
    query_gain,
    key_gain,
    out_proj,
    expert_norm_scale,
    residual,
    routes,
    route_weights,
    w_gate,
    w_up,
    w_down,
):
    head_size = query_gain.shape[0]
    tok_sp = queries.shape[0]
    tp_count = lax.axis_size("tp")
    sp_count = lax.axis_size("sp")
    heads_dev = queries.shape[1] // head_size
    all_heads = heads_dev * tp_count
    kv_heads = keys.shape[1] // head_size
    group = all_heads // kv_heads
    scale = head_size ** (-0.5)
    tp_index = lax.axis_index("tp")
    sp_index = lax.axis_index("sp")
    position = sp_index * tok_sp + jnp.arange(tok_sp, dtype=jnp.int32)
    q_rot = prepare(queries, query_gain, position)
    shared_value_head = tp_index * heads_dev // group
    own_keys = prepare(
        lax.dynamic_slice_in_dim(keys, shared_value_head * head_size, head_size, 1),
        key_gain,
        position,
    )
    own_values = lax.dynamic_slice_in_dim(values, shared_value_head * head_size, head_size, 1)
    query_matrix = (
        q_rot.reshape(tok_sp, heads_dev, head_size)
        .transpose(1, 0, 2)
        .reshape(1, heads_dev * tok_sp, head_size)
    )
    tok_dev = residual.shape[0]
    top = routes.shape[1]
    capacity = max(2, 2 * tok_dev * top // sp_count)
    direct = tp_count == 4 and sp_count % 2 == 0 and capacity % 16 == 0
    if direct:
        key_piece, value_piece = gather_rows(sp_count, own_keys, own_values)
    else:
        key_piece = lax.all_gather(own_keys, "sp", axis=0, tiled=True)
        value_piece = lax.all_gather(own_values, "sp", axis=0, tiled=True)
    run_max, run_sum, run_acc = absorb(
        start_state(1, heads_dev * tok_sp, head_size),
        query_matrix,
        key_piece[:, None, :],
        value_piece[:, None, :],
        scale,
    )
    attn = (run_acc / run_sum[..., None]).astype(jnp.bfloat16)
    attn = (
        attn.reshape(heads_dev, tok_sp, head_size)
        .transpose(1, 0, 2)
        .reshape(tok_sp, heads_dev * head_size)
    )
    if direct:
        projected = project(attn, out_proj, tok_dev)
    else:
        columns = jnp.dot(
            lax.all_gather(attn, "tp", axis=1, tiled=True),
            out_proj,
            preferred_element_type=jnp.float32,
        )
        projected = lax.all_to_all(
            columns.astype(jnp.bfloat16), "tp", split_axis=0, concat_axis=1, tiled=True
        )
    mixed_float_output = residual.astype(jnp.float32) + projected.astype(jnp.float32)
    mixed = mixed_float_output.astype(jnp.bfloat16)
    mixed_float_output = mixed.astype(jnp.float32)
    normed = (
        mixed_float_output
        * lax.rsqrt(jnp.mean(mixed_float_output * mixed_float_output, axis=-1, keepdims=True) + EPS)
        * expert_norm_scale
    ).astype(jnp.bfloat16)
    flat_routes = routes.reshape(-1)
    one_hot = (flat_routes[:, None] == jnp.arange(sp_count, dtype=jnp.int32)[None, :]).astype(
        jnp.int32
    )
    earlier = jnp.cumsum(one_hot, axis=0) - one_hot
    slot_index = jnp.sum(earlier * one_hot, axis=1)
    target = flat_routes * capacity + slot_index
    selector = (
        jnp.arange(sp_count * capacity, dtype=jnp.int32)[:, None] == target[None, :]
    ).astype(jnp.bfloat16)
    selector = jnp.sum(selector.reshape(sp_count * capacity, tok_dev, top), axis=2)
    send_rows = jnp.dot(selector, normed, preferred_element_type=jnp.float32).astype(jnp.bfloat16)
    if direct:
        hidden = dispatch(
            sp_count,
            tp_count,
            send_rows.reshape(sp_count, capacity, send_rows.shape[1]),
            w_gate,
            w_up,
        )
        returned = combine(sp_count, hidden, w_down, capacity).reshape(send_rows.shape)
        places = jnp.arange(sp_count * capacity, dtype=jnp.int32)[None, None, :]
        chosen = target.reshape(tok_dev, top)[:, :, None] == places
        spread = jnp.sum(jnp.where(chosen, route_weights[:, :, None], 0.0), axis=1)
        coarse = lax.reduce_precision(spread, 8, 7)
        both = jnp.concatenate([coarse, spread - coarse], axis=0).astype(jnp.bfloat16)
        sums = jnp.dot(both, returned, preferred_element_type=jnp.float32)
        return (mixed_float_output + (sums[:tok_dev] + sums[tok_dev:])).astype(jnp.bfloat16)
    arrived = lax.all_to_all(send_rows, "sp", split_axis=0, concat_axis=0, tiled=True)
    piece = lax.all_gather(arrived, "tp", axis=0, tiled=True)
    gate = jnp.dot(piece, w_gate[0], preferred_element_type=jnp.float32)
    upper = jnp.dot(piece, w_up[0], preferred_element_type=jnp.float32)
    hidden = (jax.nn.silu(gate) * upper).astype(jnp.bfloat16)
    partial = jnp.dot(hidden, w_down[0], preferred_element_type=jnp.float32).astype(jnp.bfloat16)
    expert_out = lax.psum_scatter(partial, "tp", scatter_dimension=0, tiled=True)
    returned = lax.all_to_all(expert_out, "sp", split_axis=0, concat_axis=0, tiled=True)
    picked = (
        jnp.take(returned, target, axis=0)
        .astype(jnp.float32)
        .reshape(tok_dev, top, returned.shape[1])
    )
    moe_sum = jnp.sum(picked * route_weights[:, :, None], axis=1)
    return (mixed_float_output + moe_sum).astype(jnp.bfloat16)


def solution(mesh):
    placed = (
        P("sp", "tp"),
        P("sp", None),
        P("sp", None),
        P(),
        P(),
        P(None, "tp"),
        P(),
        P(("sp", "tp"), None),
        P(("sp", "tp"), None),
        P(("sp", "tp"), None),
        P("sp", None, "tp"),
        P("sp", None, "tp"),
        P("sp", "tp", None),
    )
    return jax.shard_map(
        local, mesh=mesh, in_specs=placed, out_specs=P(("sp", "tp"), None), check_vma=False
    )
```

profile of v0, /device:TPU:0, one launch (start us, length us, event | category | flops | bytes accessed | tf_op | source)
XLA Modules:
  0.0 160.5 jit_solution(2987005701598767054)
XLA Ops:
  0.0 0.0 copy-start
  0.0 1.0 fusion.19
  1.0 1.0 fusion.21
  2.0 1.2 fusion.27
  3.2 0.8 maximum_bitcast_fusion.1.k_ref
  4.0 0.0 copy-done
  4.0 0.6 constant_dynamic-slice_fusion.v_ref
  4.6 19.9 %gather_rows.1 = (bf16[2048,128]{1,0:T(8,128)(2,1)}, bf16[2048,128]{1,0:T(8,128)(2,1)}) custom-call(bf16[256,128]{1,0:T(8,128)(2,1)} %maximum_bitcast_fusion.1.k_ref, bf16[256,128]{1,0:T(8,128)(2,1)} %constant_dynamic-slice_fusion.v_ref), custom_call_target="tpu_custom_call" | custom-call | tf_op jit(solution)/shard_map/gather_rows/pallas_call | solution.py:227
  24.5 0.3 multiply_cosine_fusion.3
  24.8 1.1 copy.39
  25.9 0.1 fusion.2
  26.0 0.8 fusion.3
  26.7 0.1 subtract_convert_fusion.1
  26.9 0.2 copy.40
  27.0 2.4 %multiply_reduce_fusion = (f32[1024]{0:T(1024)S(1)}, f32[1024,2048]{1,0:T(8,128)S(1)}) fusion(bf16[1024,128]{1,0:T(8,128)(2,1)S(1)} %bitcast.27, bf16[2048,128]{1,0:T(8,128)(2,1)} %get-tuple-element.19), kind=kOutput, calls=%fused_computation.2 | convolution fusion | flops 541064192 | bytes 9179136 | tf_op jit(solution)/shard_map/while/body/eval_jaxpr/hxt,ght->hxg/dot_general | solution.py:62
  29.4 0.0 copy-start.6
  29.4 2.1 %convert_reduce_fusion = (f32[1024]{0:T(1024)S(1)}, bf16[1024,2048]{1,0:T(8,128)(2,1)S(1)}) fusion(f32[1024]{0:T(1024)S(1)} %broadcast_maximum_fusion, f32[1024,2048]{1,0:T(8,128)S(1)} %get-tuple-element.55), kind=kLoop, calls=%fused_computation | loop fusion | flops 10484736 | bytes 12591104 | tf_op jit(solution)/shard_map/while/body/eval_jaxpr/reduce_sum | solution.py:70
  31.5 0.0 copy-start.2
  31.6 0.0 copy-start.4
  31.6 0.0 copy-start.3
  31.6 0.0 copy-done.6
  31.6 1.3 fusion.1
  32.9 0.2 copy.43
  33.1 0.7 copy.48
  33.8 20.8 %project.1 = bf16[64,2048]{1,0:T(8,128)(2,1)} custom-call(bf16[256,512]{1,0:T(8,128)(2,1)} %bitcast.28, bf16[2048,512]{1,0:T(8,128)(2,1)} %w_ref.1), custom_call_target="tpu_custom_call" | custom-call | tf_op jit(solution)/shard_map/project/pallas_call | solution.py:292
  54.6 0.0 copy-done.2
  54.6 1.1 fusion.4
  55.8 0.0 copy-done.4
  55.8 0.1 copy.44
  55.9 0.1 eq.45
  56.0 0.1 fusion.37
  56.1 0.2 reduce_window_sum.11
  56.3 0.2 select_reduce_fusion.1
  56.5 0.1 reduce_sum.73
  56.6 0.1 copy.45
  56.7 0.1 fusion.32
  56.8 0.0 copy-done.3
  56.8 2.4 %convolution_convert_fusion = bf16[256,2048]{1,0:T(8,128)(2,1)} fusion(bf16[256,64]{0,1:T(8,128)(2,1)S(1)} %fusion.32, f32[2048]{0:T(1024)S(1)} %copy-done.3, f32[64]{0:T(128)S(1)} %add_rsqrt_fusion.2, bf16[64,2048]{1,0:T(8,128)(2,1)} %project.1, bf16[64,2048]{1,0:T(8,128)(2,1)S(1)} %copy-done.2), kind=kOutput, calls=%fused_computation.3 | convolution fusion | flops 68681728 | bytes 1614080 | tf_op jit(solution)/shard_map/dot_general | solution.py:659
  59.2 0.0 copy-start.5
  59.2 0.0 copy-start.1
  59.2 48.9 %dispatch.1.hid_ref = bf16[4,256,1024]{2,1,0:T(8,128)(2,1)} custom-call(bf16[8,32,2048]{2,1,0:T(8,128)(2,1)} %bitcast.26, bf16[1,2048,1024]{2,1,0:T(8,128)(2,1)} %wg_ref.1, bf16[1,2048,1024]{2,1,0:T(8,128)(2,1)} %wu_ref.1), custom_call_target="tpu_custom_call" | custom-call | tf_op jit(solution)/shard_map/dispatch/pallas_call | solution.py:421
  108.1 49.9 %combine.1 = bf16[8,32,2048]{2,1,0:T(8,128)(2,1)} custom-call(bf16[4,256,1024]{2,1,0:T(8,128)(2,1)} %dispatch.1.hid_ref, bf16[1,1024,2048]{2,1,0:T(8,128)(2,1)} %wd_ref.1), custom_call_target="tpu_custom_call" | custom-call | tf_op jit(solution)/shard_map/combine/pallas_call | solution.py:533
  158.0 0.0 copy-done.5
  158.0 0.1 select_reduce_fusion
  158.2 1.5 fusion.33
  159.7 0.0 copy-done.1
  159.7 0.8 fusion.7
  (10 shorter events, 0.1 us)
Async XLA Ops:
  0.0 4.0 %copy-start = (bf16[256,256]{1,0:T(8,128)(2,1)S(1)}, bf16[256,256]{1,0:T(8,128)(2,1)}, u32[]{:S(2)}) copy-start(bf16[256,256]{1,0:T(8,128)(2,1)} %param.15) | copy-start | bytes 393220
  29.4 2.2 %copy-start.6 = (bf16[2048,128]{1,0:T(8,128)(2,1)S(1)}, bf16[2048,128]{1,0:T(8,128)(2,1)}, u32[]{:S(2)}) copy-start(bf16[2048,128]{1,0:T(8,128)(2,1)} %get-tuple-element.20) | copy-start | bytes 1572868
  31.5 23.1 %copy-start.2 = (bf16[64,2048]{1,0:T(8,128)(2,1)S(1)}, bf16[64,2048]{1,0:T(8,128)(2,1)}, u32[]{:S(2)}) copy-start(bf16[64,2048]{1,0:T(8,128)(2,1)} %param.20) | copy-start | bytes 786436
  31.6 24.2 %copy-start.4 = (s32[64,2]{0,1:T(2,128)S(1)}, s32[64,2]{0,1:T(2,128)}, u32[]{:S(2)}) copy-start(s32[64,2]{0,1:T(2,128)} %param.21) | copy-start | bytes 1540
  31.6 25.2 %copy-start.3 = (f32[2048]{0:T(1024)S(1)}, f32[2048]{0:T(1024)}, u32[]{:S(2)}) copy-start(f32[2048]{0:T(1024)} %param.19) | copy-start | bytes 24580
  59.2 98.8 %copy-start.5 = (f32[64,2]{0,1:T(2,128)S(1)}, f32[64,2]{0,1:T(2,128)}, u32[]{:S(2)}) copy-start(f32[64,2]{0,1:T(2,128)} %param.22) | copy-start | bytes 1540
  59.2 100.5 %copy-start.1 = (bf16[64,2048]{1,0:T(8,128)(2,1)S(1)}, bf16[64,2048]{1,0:T(8,128)(2,1)}, u32[]{:S(2)}) copy-start(bf16[64,2048]{1,0:T(8,128)(2,1)} %project.1) | copy-start | bytes 786436
where the time goes:
time: 161 us
  Pallas kernels  139 us (86%)
  other arithmetic  9.91 us (6%)
  matrix products  7.6 us (5%)
  local copies, waits for them, and re-layouts  3.3 us (2%)
    pallas_call x1, Pallas kernels, combine(): pl.pallas_call(functools.partial(combine_kernel, n, chunks), out_shape=ja...  49.9 us
    pallas_call x1, Pallas kernels, dispatch(): pl.pallas_call(functools.partial(dispatch_kernel, n, chunks), out_shape=j...  48.9 us
    pallas_call x1, Pallas kernels, project(): pl.pallas_call(project_kernel, out_shape=jax.ShapeDtypeStruct((share, out...  20.8 us
    pallas_call x1, Pallas kernels, gather_rows(): pl.pallas_call(functools.partial(gather_kernel, n), out_shape=(shape, sha...  19.9 us

commit v1 on v0

v1 whole, which is shorter than its diff:
```python
import functools

import jax
import jax.numpy as jnp
from jax import lax
from jax.experimental import pallas as pl
from jax.experimental.pallas import tpu as pltpu
from jax.sharding import PartitionSpec as P

GRID_W = 64


EPS = 1e-06
ROPE_BASE = 10000.0
NEG_START = -1e30


def rotate(field, position):
    half = field.shape[-1] // 2
    quarter = half // 2
    freqs = ROPE_BASE ** (-jnp.arange(quarter, dtype=jnp.float32) / quarter)
    grid_row = (position // GRID_W).astype(jnp.float32)
    grid_col = (position % GRID_W).astype(jnp.float32)

    def turn_half(part, coord):
        angle = coord[:, None] * freqs[None, :]
        cosine = jnp.cos(angle)[:, None, :]
        sine = jnp.sin(angle)[:, None, :]
        first, second = (part[..., :quarter], part[..., quarter:])
        return jnp.concatenate(
            [first * cosine - second * sine, second * cosine + first * sine], axis=-1
        )

    return jnp.concatenate(
        [turn_half(field[..., :half], grid_row), turn_half(field[..., half:], grid_col)], axis=-1
    )


def prepare(field, gain, position):
    count = field.shape[0]
    width = gain.shape[0]
    heads_here = field.shape[1] // width
    values_f = field.reshape(count, heads_here, width).astype(jnp.float32)
    scaled = (
        values_f * lax.rsqrt(jnp.mean(values_f * values_f, axis=-1, keepdims=True) + EPS) * gain
    )
    return rotate(scaled, position).reshape(count, heads_here * width).astype(jnp.bfloat16)


def absorb(carry, query_matrix, key_rows, value_rows, scale):
    count = key_rows.shape[0]
    width = 2048 if count > 2048 and count % 2048 == 0 else count
    key_blocks = key_rows.reshape(count // width, width, key_rows.shape[1], key_rows.shape[2])
    value_blocks = value_rows.reshape(
        count // width, width, value_rows.shape[1], value_rows.shape[2]
    )

    def step(state, block):
        run_max, run_sum, run_acc = state
        key_tile_rows, value_tile_rows = block
        scores = (
            jnp.einsum(
                "hxt,ght->hxg", query_matrix, key_tile_rows, preferred_element_type=jnp.float32
            )
            * scale
        )
        new_max = jnp.maximum(run_max, jnp.max(scores, axis=-1))
        weight_tensors = jnp.exp(scores - new_max[..., None]).astype(jnp.bfloat16)
        factor = jnp.exp(run_max - new_max)
        run_sum = run_sum * factor + jnp.sum(weight_tensors.astype(jnp.float32), axis=-1)
        run_acc = run_acc * factor[..., None] + jnp.einsum(
            "zij,jzu->ziu", weight_tensors, value_tile_rows, preferred_element_type=jnp.float32
        )
        return ((new_max, run_sum, run_acc), None)

    result, unused = lax.scan(step, carry, (key_blocks, value_blocks))
    return result


MESH = pl.DeviceIdType.MESH
VMEM_LIMIT = 60 * 1024 * 1024


def greet(partners, count):
    barrier = pltpu.get_barrier_semaphore()
    for where in partners:
        pl.semaphore_signal(barrier, inc=1, device_id=where, device_id_type=MESH)
    pl.semaphore_wait(barrier, count)


def remote(src, dst, send, recv, where):
    return pltpu.make_async_remote_copy(
        src_ref=src, dst_ref=dst, send_sem=send, recv_sem=recv, device_id=where, device_id_type=MESH
    )


def square():
    mine = lax.axis_index("tp")
    return mine, mine + 1 - 2 * lax.rem(mine, 2), lax.rem(mine + 2, 4), 3 - mine


def gather_kernel(n, k_ref, v_ref, n_ref, ko_ref, vo_ref, no_ref, send, recv):
    me = lax.axis_index("sp")
    chips = n // 2
    chip, core = me // 2, lax.rem(me, 2)
    partner = 2 * chip + 1 - core
    has_right, has_left = chip < chips - 1, chip > 0
    right, left = me + 2, me - 2
    barrier = pltpu.get_barrier_semaphore()
    pl.semaphore_signal(barrier, inc=1, device_id={"sp": partner}, device_id_type=MESH)

    @pl.when(has_right)
    def _():
        pl.semaphore_signal(barrier, inc=1, device_id={"sp": right}, device_id_type=MESH)

    @pl.when(has_left)
    def _():
        pl.semaphore_signal(barrier, inc=1, device_id={"sp": left}, device_id_type=MESH)

    pl.semaphore_wait(barrier, 1 + has_right.astype(jnp.int32) + has_left.astype(jnp.int32))

    pairs = ((k_ref, ko_ref), (v_ref, vo_ref), (n_ref, no_ref))

    def block(out, origin):
        rows = out.shape[0] // n
        return out.at[pl.ds(pl.multiple_of(origin * rows, rows), rows)]

    def copies(origin, way, where, own=False):
        return [
            remote(
                ref if own else block(out, origin),
                block(out, origin),
                send.at[origin, way, i],
                recv.at[origin, i],
                {"sp": where},
            )
            for i, (ref, out) in enumerate(pairs)
        ]

    def start(*args, **kw):
        for c in copies(*args, **kw):
            c.start()

    def sent(*args, **kw):
        for c in copies(*args, **kw):
            c.wait_send()

    def arrived(origin):
        for c in copies(origin, 0, partner):
            c.wait_recv()

    @pl.when(has_right)
    def _():
        start(me, 0, right, own=True)

    @pl.when(has_left)
    def _():
        start(me, 2, left, own=True)

    start(me, 1, partner, own=True)
    for ref, out in pairs:
        block(out, me)[...] = ref[...]
    for j in range(1, chips):

        @pl.when(chip - j >= 0)
        def _(origin=me - 2 * j):
            arrived(origin)

            @pl.when(has_right)
            def _():
                start(origin, 0, right)

            start(origin, 1, partner)

        @pl.when(chip + j < chips)
        def _(origin=me + 2 * j):
            arrived(origin)

            @pl.when(has_left)
            def _():
                start(origin, 2, left)

            start(origin, 1, partner)

    for z in range(chips):
        arrived(2 * z + 1 - core)
    sent(me, 1, partner, own=True)

    @pl.when(has_right)
    def _():
        sent(me, 0, right, own=True)

    @pl.when(has_left)
    def _():
        sent(me, 2, left, own=True)

    for j in range(1, chips):

        @pl.when(chip - j >= 0)
        def _(origin=me - 2 * j):
            @pl.when(has_right)
            def _():
                sent(origin, 0, right)

            sent(origin, 1, partner)

        @pl.when(chip + j < chips)
        def _(origin=me + 2 * j):
            @pl.when(has_left)
            def _():
                sent(origin, 2, left)

            sent(origin, 1, partner)


def in_vmem(count):
    return [pl.BlockSpec(memory_space=pltpu.VMEM)] * count


def params(number):
    return pltpu.CompilerParams(
        collective_id=number, has_side_effects=True, vmem_limit_bytes=VMEM_LIMIT
    )


def gather_rows(n, own_keys, own_values, notes):
    arrays = (own_keys, own_values, notes)
    return pl.pallas_call(
        functools.partial(gather_kernel, n),
        out_shape=tuple(
            jax.ShapeDtypeStruct((n * a.shape[0], a.shape[1]), a.dtype) for a in arrays
        ),
        in_specs=in_vmem(3),
        out_specs=tuple(in_vmem(3)),
        scratch_shapes=[pltpu.SemaphoreType.DMA((n, 3, 3)), pltpu.SemaphoreType.DMA((n, 3))],
        compiler_params=params(0),
        name="gather_rows",
    )(*arrays)


def project_kernel(
    attn_ref, w_ref, n_ref, out_ref, no_ref, held, stage, send, recv, give, take, tell, told
):
    mine, across, along, corner = square()
    rows, width = attn_ref.shape
    half = rows // 2
    share = out_ref.shape[0]
    greet([{"tp": across}, {"tp": along}, {"tp": corner}], 3)
    first = [
        remote(attn_ref, held.at[mine], send.at[0], recv.at[0], {"tp": across}),
        remote(attn_ref, held.at[mine], send.at[1], recv.at[1], {"tp": along}),
    ]
    for c in first:
        c.start()
    notes = [
        remote(n_ref, no_ref.at[mine], tell.at[i], told.at[i], {"tp": p})
        for i, p in enumerate((corner, across, along))
    ]
    for c in notes:
        c.start()
    no_ref[mine] = n_ref[...]
    top, low = pl.ds(0, half), pl.ds(half, half)
    second = [
        remote(held.at[across, top], held.at[across, top], send.at[2], recv.at[2], {"tp": along}),
        remote(held.at[along, low], held.at[along, low], send.at[3], recv.at[3], {"tp": across}),
    ]

    def term(rows_here, owner):
        part = w_ref[pl.ds(pl.multiple_of(owner * width, width), width), :]
        return jnp.dot(rows_here, part, preferred_element_type=jnp.float32)

    total = term(attn_ref[...], mine)
    first[0].wait_recv()
    second[0].start()
    first[1].wait_recv()
    second[1].start()
    total += term(held[across], across)
    total += term(held[along], along)
    for c in second:
        c.wait_recv()
    total += term(held[corner], corner)
    stage[...] = total.astype(stage.dtype)
    columns = pl.ds(pl.multiple_of(mine * width, width), width)

    def piece(owner):
        return pl.ds(pl.multiple_of(owner * share, share), share)

    back = [
        remote(stage.at[piece(p)], out_ref.at[:, columns], give.at[i], take.at[i], {"tp": p})
        for i, p in enumerate((corner, across, along))
    ]
    for c in back:
        c.start()
    out_ref[:, columns] = stage[piece(mine), :]
    for c in back + notes:
        c.wait()
    for c in first + second:
        c.wait_send()


def project(attn, out_proj, notes, share):
    rows, width = attn.shape
    parts = out_proj.shape[0] // width
    return pl.pallas_call(
        project_kernel,
        out_shape=(
            jax.ShapeDtypeStruct((share, out_proj.shape[1] * parts), jnp.bfloat16),
            jax.ShapeDtypeStruct((parts,) + notes.shape, notes.dtype),
        ),
        in_specs=in_vmem(3),
        out_specs=tuple(in_vmem(2)),
        scratch_shapes=[
            pltpu.VMEM((parts, rows, width), jnp.bfloat16),
            pltpu.VMEM((rows, out_proj.shape[1]), jnp.bfloat16),
            pltpu.SemaphoreType.DMA((4,)),
            pltpu.SemaphoreType.DMA((4,)),
            pltpu.SemaphoreType.DMA((3,)),
            pltpu.SemaphoreType.DMA((3,)),
            pltpu.SemaphoreType.DMA((3,)),
            pltpu.SemaphoreType.DMA((3,)),
        ],
        compiler_params=params(1),
        name="project",
    )(attn, out_proj, notes)


def visit(chip, chips, step):
    near = jnp.minimum(chip, chips - 1 - chip)
    swing = chip + ((step + 1) // 2) * (1 - 2 * lax.rem(step, 2))
    up = chip < chips - 1 - chip
    tail = jnp.where(up, chip + (step - near), chip - (step - near))
    return jnp.where(step <= 2 * near, swing, tail)


def wide(value):
    return value.astype(jnp.float32)


def moe_kernel(
    n, cuts, x_ref, mixed_ref, slot_ref, part_ref, wg_ref, wu_ref, wd_ref, out_ref,
    tok, wg, wu, wd, picked, hid, wsel, held, own, give, take,
    low, high, from_x, from_y, to_y, to_x, last_y, last_x, acc, zsend, zrecv,
    load, zs, zr, sq_s, sq_r, pd_s, pd_r, tk_s, tk_r, hop_s, hop_r, hz_s, hz_r,
):
    me = lax.axis_index("sp")
    chips = n // 2
    chip, core = me // 2, lax.rem(me, 2)
    other = 1 - core
    partner = {"sp": 2 * chip + other}
    mine, across, along, corner = square()
    x, y = lax.rem(mine, 2), mine // 2
    share, depth = x_ref.shape
    units = wg.shape[1]
    group = 4 * share
    slots = wsel.shape[2] // 2
    width = depth // cuts
    half = width // 2
    steps = chips * cuts

    def column(k):
        return pl.ds(pl.multiple_of(k * width, width), width)

    loads = [
        pltpu.make_async_copy(wg_ref.at[0], wg, load.at[0]),
        pltpu.make_async_copy(wu_ref.at[0], wu, load.at[1]),
    ] + [
        pltpu.make_async_copy(wd_ref.at[0, :, pl.ds(q * width, width)], wd.at[q], load.at[2 + q])
        for q in range(cuts)
    ]
    for c in loads:
        c.start()

    barrier = pltpu.get_barrier_semaphore()

    def greet_one(where):
        pl.semaphore_signal(barrier, inc=1, device_id=where, device_id_type=MESH)

    greet_one(partner)
    greet_one({"tp": across})
    greet_one({"tp": along})
    for d in range(1, chips):
        greet_one({"sp": 2 * lax.rem(chip + d, chips) + core})
    pl.semaphore_wait(barrier, chips + 2)

    def to_plane(p):
        return remote(x_ref, tok.at[chip, core, mine], zs.at[p], zr.at[chip], {"sp": 2 * p + core})

    def from_plane(p):
        return remote(x_ref, tok.at[p, core, mine], zs.at[p], zr.at[p], {"sp": 2 * p + core})

    upper, lower = pl.ds(0, share // 2), pl.ds(share // 2, share // 2)

    def pass_on(p, way, first=False):
        block = tok.at[p, core]
        src, dst, where = (
            (x_ref if first else block.at[mine], block.at[mine], across),
            (x_ref if first else block.at[mine], block.at[mine], along),
            (block.at[across, upper], block.at[across, upper], along),
            (block.at[along, lower], block.at[along, lower], across),
        )[way]
        return remote(src, dst, sq_s.at[p, way], sq_r.at[p, way], {"tp": where})

    def arrive(p, way):
        block = tok.at[p, core]
        dst = (
            block.at[across],
            block.at[along],
            block.at[corner, upper],
            block.at[corner, lower],
        )[way]
        remote(dst, dst, sq_s.at[p, way], sq_r.at[p, way], {"tp": across}).wait_recv()

    def hand(p, t, first=False):
        block = tok.at[p, core, t]
        return remote(x_ref if first else block, block, pd_s.at[p, t], pd_r.at[p, t], partner)

    def handed(p, t):
        block = tok.at[p, other, t]
        remote(block, block, pd_s.at[p, t], pd_r.at[p, t], partner).wait_recv()

    pass_on(chip, 0, True).start()
    pass_on(chip, 1, True).start()
    for j in range(1, chips):

        @pl.when(chip + j < chips)
        def _():
            to_plane(chip + j).start()

        @pl.when(chip - j >= 0)
        def _():
            to_plane(chip - j).start()

    hand(chip, mine, True).start()
    tok[chip, core, mine] = x_ref[...]

    def expert(p):
        arrive(p, 2)
        arrive(p, 3)
        hand(p, corner).start()
        for t in range(4):
            handed(p, t)
        for side in range(2):
            spot = slot_ref[2 * p + side]
            hit = lax.broadcasted_iota(jnp.int32, (slots, group), 0) == spot
            pick = jnp.where(hit, 1.0, 0.0).astype(tok.dtype)
            parts = part_ref[2 * p + side]
            wsel[p, side, :slots] = jnp.where(hit, parts[0:1], 0.0).astype(wsel.dtype)
            wsel[p, side, slots:] = jnp.where(hit, parts[1:2], 0.0).astype(wsel.dtype)

            @pl.loop(0, cuts)
            def _(q):
                block = tok[p, side, :, :, column(q)].reshape(group, width)
                rows = jnp.dot(pick, block, preferred_element_type=jnp.float32)
                picked[side * slots : (side + 1) * slots, column(q)] = rows.astype(picked.dtype)

        @pl.loop(0, units // 256)
        def _(u):
            cols = pl.ds(pl.multiple_of(u * 256, 256), 256)
            gate = jnp.dot(picked[...], wg[:, cols], preferred_element_type=jnp.float32)
            upper_part = jnp.dot(picked[...], wu[:, cols], preferred_element_type=jnp.float32)
            hid[p, :, cols] = (jax.nn.silu(gate) * upper_part).astype(hid.dtype)

    @pl.loop(0, chips)
    def _(s):
        @pl.when(s + 1 < chips)
        def _():
            p = visit(chip, chips, s + 1)
            from_plane(p).wait_recv()
            pass_on(p, 0).start()
            pass_on(p, 1).start()
            hand(p, mine).start()

        p = visit(chip, chips, s)
        arrive(p, 0)
        pass_on(p, 2).start()
        hand(p, across).start()
        arrive(p, 1)
        pass_on(p, 3).start()
        hand(p, along).start()

        @pl.when(s == 0)
        def _():
            for c in loads:
                c.wait()

        @pl.when(s >= 1)
        def _():
            expert(visit(chip, chips, s - 1))

    def plane_of(k):
        return visit(chip, chips, lax.rem(k // cuts + 1, chips))

    def swap(k):
        return remote(give.at[k], take.at[k], tk_s.at[k], tk_r.at[k], partner)

    def hop(k, way):
        src, dst, where = (
            (low.at[k, 1 - x], from_x.at[k], across),
            (high.at[k, 1 - y], from_y.at[k], along),
            (to_y.at[k], last_y.at[k], along),
            (to_x.at[k], last_x.at[k], across),
        )[way]
        return remote(src, dst, hop_s.at[k, way], hop_r.at[k, way], {"tp": where})

    def home(k):
        p, q = plane_of(k), lax.rem(k, cuts)
        return remote(
            zsend.at[k], zrecv.at[chip, q], hz_s.at[k], hz_r.at[chip, q], {"sp": 2 * p + core}
        )

    def homed(p, q):
        return remote(zsend.at[0], zrecv.at[p, q], hz_s.at[0], hz_r.at[p, q], partner)

    @pl.loop(0, steps + 5)
    def _(step):
        @pl.when((step >= 1) & (step <= steps))
        def _(k=step - 1):
            swap(k).wait_recv()
            total = own[lax.rem(k, 2)] + wide(take[k])
            cast = total.astype(low.dtype).reshape(4, share, width)
            for t in range(4):
                low[k, t % 2, t // 2] = cast[t, :, :half]
                high[k, t // 2, t % 2] = cast[t, :, half:]
            hop(k, 0).start()
            hop(k, 1).start()

        @pl.when(step < steps)
        def _(k=step):
            @pl.when(k == cuts)
            def _():
                expert(visit(chip, chips, chips - 1))

            p, q = plane_of(k), lax.rem(k, cuts)
            out = jnp.dot(hid[p], wd[q], preferred_element_type=jnp.float32).astype(held.dtype)
            for side in range(2):
                block = out[side * slots : (side + 1) * slots]
                held[side, :slots] = block
                held[side, slots:] = block

            def spread(side):
                return lax.dot_general(
                    wsel[p, side], held[side], (((0,), (0,)), ((), ())),
                    preferred_element_type=jnp.float32,
                )

            give[k] = spread(other).astype(give.dtype)
            swap(k).start()
            own[lax.rem(k, 2)] = spread(core)

        @pl.when((step >= 3) & (step < steps + 3))
        def _(k=step - 3):
            hop(k, 0).wait_recv()
            to_y[k] = (wide(low[k, x, 1 - y]) + wide(from_x[k, 1 - y])).astype(to_y.dtype)
            hop(k, 2).start()
            hop(k, 1).wait_recv()
            to_x[k] = (wide(high[k, y, 1 - x]) + wide(from_y[k, 1 - x])).astype(to_x.dtype)
            hop(k, 3).start()

        @pl.when(step >= 5)
        def _(k=step - 5):
            hop(k, 2).wait_recv()
            left = wide(low[k, x, y]) + wide(from_x[k, y]) + wide(last_y[k])
            hop(k, 3).wait_recv()
            right = wide(high[k, y, x]) + wide(from_y[k, x]) + wide(last_x[k])

            @pl.when(k < steps - cuts)
            def _():
                zsend[k, :, :half] = left.astype(zsend.dtype)
                zsend[k, :, half:] = right.astype(zsend.dtype)
                home(k).start()

            @pl.when(k >= steps - cuts)
            def _():
                acc[lax.rem(k, cuts), :, :half] = left
                acc[lax.rem(k, cuts), :, half:] = right

    @pl.loop(0, cuts)
    def _(q):
        total = acc[q] + wide(mixed_ref[:, column(q)])
        for d in range(1, chips):
            p = lax.rem(chip + d, chips)
            homed(p, q).wait_recv()
            total += wide(zrecv[p, q])
        out_ref[:, column(q)] = total.astype(out_ref.dtype)

    for d in range(1, chips):
        to_plane(lax.rem(chip + d, chips)).wait_send()

    @pl.loop(0, chips)
    def _(p):
        for way in range(4):
            pass_on(p, way).wait_send()
            hand(p, way).wait_send()

    @pl.loop(0, steps)
    def _(k):
        swap(k).wait_send()
        for way in range(4):
            hop(k, way).wait_send()

        @pl.when(k < steps - cuts)
        def _():
            home(k).wait_send()


def moe(n, normed, mixed, slot_rows, weight_rows, capacity, w_gate, w_up, w_down, cuts=4):
    share, depth = normed.shape
    units = w_gate.shape[2]
    chips = n // 2
    kind = normed.dtype
    width = depth // cuts
    half = width // 2
    steps = chips * cuts
    group, slots = 4 * share, 4 * capacity
    dma = pltpu.SemaphoreType.DMA

    def room(*extent):
        return pltpu.VMEM(extent, kind)

    def exact(*extent):
        return pltpu.VMEM(extent, jnp.float32)

    return pl.pallas_call(
        functools.partial(moe_kernel, n, cuts),
        out_shape=jax.ShapeDtypeStruct((share, depth), kind),
        in_specs=in_vmem(4) + [pl.BlockSpec(memory_space=pl.ANY)] * 3,
        out_specs=in_vmem(1)[0],
        scratch_shapes=[
            room(chips, 2, 4, share, depth),
            room(depth, units),
            room(depth, units),
            room(cuts, units, width),
            room(2 * slots, depth),
            room(chips, 2 * slots, units),
            room(chips, 2, 2 * slots, group),
            room(2, 2 * slots, width),
            exact(2, group, width),
            room(steps, group, width),
            room(steps, group, width),
            room(steps, 2, 2, share, half),
            room(steps, 2, 2, share, half),
            room(steps, 2, share, half),
            room(steps, 2, share, half),
            room(steps, share, half),
            room(steps, share, half),
            room(steps, share, half),
            room(steps, share, half),
            exact(cuts, share, width),
            room(steps - cuts, share, width),
            room(chips, cuts, share, width),
            dma((2 + cuts,)),
            dma((chips,)),
            dma((chips,)),
            dma((chips, 4)),
            dma((chips, 4)),
            dma((chips, 4)),
            dma((chips, 4)),
            dma((steps,)),
            dma((steps,)),
            dma((steps, 4)),
            dma((steps, 4)),
            dma((steps,)),
            dma((chips, cuts)),
        ],
        compiler_params=params(2),
        name="moe",
    )(normed, mixed, slot_rows, weight_rows, w_gate, w_up, w_down)


def start_state(batch, rows, width):
    return (
        jnp.full((batch, rows), NEG_START, jnp.float32),
        jnp.zeros((batch, rows), jnp.float32),
        jnp.zeros((batch, rows, width), jnp.float32),
    )


def local(
    queries,
    keys,
    values,
    query_gain,
    key_gain,
    out_proj,
    expert_norm_scale,
    residual,
    routes,
    route_weights,
    w_gate,
    w_up,
    w_down,
):
    head_size = query_gain.shape[0]
    tok_sp = queries.shape[0]
    tp_count = lax.axis_size("tp")
    sp_count = lax.axis_size("sp")
    heads_dev = queries.shape[1] // head_size
    all_heads = heads_dev * tp_count
    kv_heads = keys.shape[1] // head_size
    group = all_heads // kv_heads
    scale = head_size ** (-0.5)
    tp_index = lax.axis_index("tp")
    sp_index = lax.axis_index("sp")
    position = sp_index * tok_sp + jnp.arange(tok_sp, dtype=jnp.int32)
    q_rot = prepare(queries, query_gain, position)
    shared_value_head = tp_index * heads_dev // group
    own_keys = prepare(
        lax.dynamic_slice_in_dim(keys, shared_value_head * head_size, head_size, 1),
        key_gain,
        position,
    )
    own_values = lax.dynamic_slice_in_dim(values, shared_value_head * head_size, head_size, 1)
    query_matrix = (
        q_rot.reshape(tok_sp, heads_dev, head_size)
        .transpose(1, 0, 2)
        .reshape(1, heads_dev * tok_sp, head_size)
    )
    tok_dev = residual.shape[0]
    top = routes.shape[1]
    capacity = max(2, 2 * tok_dev * top // sp_count)
    direct = (
        tp_count == 4 and sp_count % 2 == 0 and capacity % 16 == 0 and 2 * tok_dev % 128 == 0
    )
    named = routes[:, :, None] == jnp.arange(sp_count, dtype=jnp.int32)[None, None, :]
    if direct:
        taken = jnp.any(named, axis=1).astype(jnp.int32)
        place = jnp.where(taken > 0, jnp.cumsum(taken, axis=0) - 1, -1).astype(jnp.float32)
        load = jnp.sum(jnp.where(named, route_weights[:, :, None], 0.0), axis=1)
        notes = jnp.concatenate([place, load], axis=0).T
        key_piece, value_piece, notes = gather_rows(sp_count, own_keys, own_values, notes)
    else:
        key_piece = lax.all_gather(own_keys, "sp", axis=0, tiled=True)
        value_piece = lax.all_gather(own_values, "sp", axis=0, tiled=True)
    run_max, run_sum, run_acc = absorb(
        start_state(1, heads_dev * tok_sp, head_size),
        query_matrix,
        key_piece[:, None, :],
        value_piece[:, None, :],
        scale,
    )
    attn = (run_acc / run_sum[..., None]).astype(jnp.bfloat16)
    attn = (
        attn.reshape(heads_dev, tok_sp, head_size)
        .transpose(1, 0, 2)
        .reshape(tok_sp, heads_dev * head_size)
    )
    if direct:
        projected, notes = project(attn, out_proj, notes, tok_dev)
    else:
        columns = jnp.dot(
            lax.all_gather(attn, "tp", axis=1, tiled=True),
            out_proj,
            preferred_element_type=jnp.float32,
        )
        projected = lax.all_to_all(
            columns.astype(jnp.bfloat16), "tp", split_axis=0, concat_axis=1, tiled=True
        )
    mixed_float_output = residual.astype(jnp.float32) + projected.astype(jnp.float32)
    mixed = mixed_float_output.astype(jnp.bfloat16)
    mixed_float_output = mixed.astype(jnp.float32)
    normed = (
        mixed_float_output
        * lax.rsqrt(jnp.mean(mixed_float_output * mixed_float_output, axis=-1, keepdims=True) + EPS)
        * expert_norm_scale
    ).astype(jnp.bfloat16)
    if direct:
        notes = notes.reshape(tp_count, sp_count, sp_count, 2, tok_dev)
        notes = lax.dynamic_index_in_dim(notes, sp_index, 2, keepdims=False)
        notes = notes.transpose(1, 2, 0, 3)
        base = capacity * jnp.arange(tp_count, dtype=jnp.float32)[:, None]
        spots = jnp.where(notes[:, 0] >= 0, notes[:, 0] + base, -1.0).astype(jnp.int32)
        coarse = lax.reduce_precision(notes[:, 1], 8, 7)
        pair = jnp.stack([coarse, notes[:, 1] - coarse], axis=1)
        return moe(
            sp_count,
            normed,
            mixed,
            spots.reshape(sp_count, 1, tp_count * tok_dev),
            pair.reshape(sp_count, 2, tp_count * tok_dev),
            capacity,
            w_gate,
            w_up,
            w_down,
        )
    flat_routes = routes.reshape(-1)
    one_hot = (flat_routes[:, None] == jnp.arange(sp_count, dtype=jnp.int32)[None, :]).astype(
        jnp.int32
    )
    earlier = jnp.cumsum(one_hot, axis=0) - one_hot
    slot_index = jnp.sum(earlier * one_hot, axis=1)
    target = flat_routes * capacity + slot_index
    selector = (
        jnp.arange(sp_count * capacity, dtype=jnp.int32)[:, None] == target[None, :]
    ).astype(jnp.bfloat16)
    selector = jnp.sum(selector.reshape(sp_count * capacity, tok_dev, top), axis=2)
    send_rows = jnp.dot(selector, normed, preferred_element_type=jnp.float32).astype(jnp.bfloat16)
    arrived = lax.all_to_all(send_rows, "sp", split_axis=0, concat_axis=0, tiled=True)
    piece = lax.all_gather(arrived, "tp", axis=0, tiled=True)
    gate = jnp.dot(piece, w_gate[0], preferred_element_type=jnp.float32)
    upper = jnp.dot(piece, w_up[0], preferred_element_type=jnp.float32)
    hidden = (jax.nn.silu(gate) * upper).astype(jnp.bfloat16)
    partial = jnp.dot(hidden, w_down[0], preferred_element_type=jnp.float32).astype(jnp.bfloat16)
    expert_out = lax.psum_scatter(partial, "tp", scatter_dimension=0, tiled=True)
    returned = lax.all_to_all(expert_out, "sp", split_axis=0, concat_axis=0, tiled=True)
    picked = (
        jnp.take(returned, target, axis=0)
        .astype(jnp.float32)
        .reshape(tok_dev, top, returned.shape[1])
    )
    moe_sum = jnp.sum(picked * route_weights[:, :, None], axis=1)
    return (mixed_float_output + moe_sum).astype(jnp.bfloat16)


def solution(mesh):
    placed = (
        P("sp", "tp"),
        P("sp", None),
        P("sp", None),
        P(),
        P(),
        P(None, "tp"),
        P(),
        P(("sp", "tp"), None),
        P(("sp", "tp"), None),
        P(("sp", "tp"), None),
        P("sp", None, "tp"),
        P("sp", None, "tp"),
        P("sp", "tp", None),
    )
    return jax.shard_map(
        local, mesh=mesh, in_specs=placed, out_specs=P(("sp", "tp"), None), check_vma=False
    )
```

time: 161 us -> 163 us (1.012)
  matrix products: 7.6 us -> 3.64 us
  local copies, waits for them, and re-layouts: 3.3 us -> 6.21 us
  other arithmetic: 9.91 us -> 12.7 us
    dot_general x2 -> x0, matrix products: 3.96 us -> none  [the longest x1 2.42 us: local(): jnp.dot(selector, normed, preferred_element_type=jnp.float32)]
    unnamed x17 -> x13, local copies, waits for them, and re-layouts: 1.95 us -> 3.52 us
    pallas_call x4 -> x3, Pallas kernels: 139 us -> 140 us  [the longest x1 98.3 us: moe(): pl.pallas_call(functools.partial(moe_kernel, n, cuts), out_shape=jax.Shap...]
where the time goes in v1:
time: 163 us
  Pallas kernels  140 us (86%)
  other arithmetic  12.7 us (8%)
  local copies, waits for them, and re-layouts  6.21 us (4%)
  matrix products  3.64 us (2%)
    pallas_call x1, Pallas kernels, moe(): pl.pallas_call(functools.partial(moe_kernel, n, cuts), out_shape=jax.Shap...  98.3 us
    pallas_call x1, Pallas kernels, project(): pl.pallas_call(project_kernel, out_shape=(jax.ShapeDtypeStruct((share, ou...  21.4 us
    pallas_call x1, Pallas kernels, gather_rows(): pl.pallas_call(functools.partial(gather_kernel, n), out_shape=tuple((jax....  20.4 us
    unnamed x13, local copies, waits for them, and re-layouts  3.52 us

profile of v1, /device:TPU:0, one launch (start us, length us, event | category | flops | bytes accessed | tf_op | source)
XLA Modules:
  0.0 162.8 jit_solution(17963045720108055634)
XLA Ops:
  0.0 0.0 copy-start
  0.0 1.0 fusion.15
  1.0 1.0 fusion.17
  2.0 1.2 fusion.23
  3.2 0.8 maximum_bitcast_fusion.1.k_ref
  4.0 0.0 copy-done
  4.0 0.6 constant_dynamic-slice_fusion.1.v_ref
  4.6 0.7 fusion.27
  5.3 0.1 copy.44
  5.4 0.1 reduce_window_sum.11
  5.5 0.1 copy.45
  5.6 0.7 select_reduce_fusion
  6.3 0.7 maximum_bitcast_fusion.2.n_ref
  6.9 20.4 %gather_rows.1 = (bf16[2048,128]{1,0:T(8,128)(2,1)}, bf16[2048,128]{1,0:T(8,128)(2,1)}, f32[64,128]{1,0:T(8,128)}) custom-call(bf16[256,128]{1,0:T(8,128)(2,1)} %maximum_bitcast_fusion.1.k_ref, bf16[256,128]{1,0:T(8,128)(2,1)} %constant_dynamic-slice_fusion.1.v_ref, f32[8,128]{1,0:T(8,128)} %maximum_bitcast_fusion.2.n_ref), custom_call_target="tpu_custom_call" | custom-call | tf_op jit(solution)/shard_map/gather_rows/pallas_call | solution.py:228
  27.3 0.3 multiply_cosine_fusion.3
  27.6 1.1 copy.40
  28.7 0.1 fusion.5
  28.8 0.8 fusion.6
  29.6 0.1 subtract_convert_fusion.1
  29.7 0.2 copy.41
  29.9 2.4 %multiply_reduce_fusion = (f32[1024]{0:T(1024)S(1)}, f32[1024,2048]{1,0:T(8,128)S(1)}) fusion(bf16[1024,128]{1,0:T(8,128)(2,1)S(1)} %bitcast.34, bf16[2048,128]{1,0:T(8,128)(2,1)} %get-tuple-element.30), kind=kOutput, calls=%fused_computation.2 | convolution fusion | flops 541064192 | bytes 9179136 | tf_op jit(solution)/shard_map/while/body/eval_jaxpr/hxt,ght->hxg/dot_general | solution.py:62
  32.2 0.0 copy-start.4
  32.3 2.1 %convert_reduce_fusion = (f32[1024]{0:T(1024)S(1)}, bf16[1024,2048]{1,0:T(8,128)(2,1)S(1)}) fusion(f32[1024]{0:T(1024)S(1)} %broadcast_maximum_fusion, f32[1024,2048]{1,0:T(8,128)S(1)} %get-tuple-element.64), kind=kLoop, calls=%fused_computation | loop fusion | flops 10484736 | bytes 12591104 | tf_op jit(solution)/shard_map/while/body/eval_jaxpr/reduce_sum | solution.py:70
  34.4 0.0 copy-start.2
  34.4 0.0 copy-start.3
  34.4 0.0 copy-done.4
  34.4 1.3 fusion.1
  35.7 0.2 copy.46
  35.9 0.7 copy.51
  36.7 21.4 %project.1 = (bf16[64,2048]{1,0:T(8,128)(2,1)}, f32[4,64,128]{2,1,0:T(8,128)}) custom-call(bf16[256,512]{1,0:T(8,128)(2,1)} %bitcast.35, bf16[2048,512]{1,0:T(8,128)(2,1)} %w_ref.1, f32[64,128]{1,0:T(8,128)} %get-tuple-element.33.n_ref), custom_call_target="tpu_custom_call" | custom-call | tf_op jit(solution)/shard_map/project/pallas_call | solution.py:304
  58.0 1.1 reshape.402
  59.2 0.1 stack.10
  59.3 0.1 stack.9
  59.4 0.6 pad_maximum_fusion.part_ref
  60.0 0.0 copy-done.2
  60.0 1.1 fusion.2
  61.1 0.0 copy-start.1
  61.2 0.0 copy-done.3
  61.2 0.8 fusion.4.x_ref
  62.0 0.1 squeeze.16
  62.1 0.1 add.142
  62.2 0.1 add.143
  62.3 0.6 fusion.26.slot_ref
  62.9 0.0 copy-done.1
  62.9 98.3 %moe.1 = bf16[64,2048]{1,0:T(8,128)(2,1)} custom-call(bf16[64,2048]{1,0:T(8,128)(2,1)} %fusion.4.x_ref, bf16[64,2048]{1,0:T(8,128)(2,1)} %copy-done.1, s32[8,1,256]{2,1,0:T(1,128)} %fusion.26.slot_ref, f32[8,2,256]{2,1,0:T(2,128)} %pad_maximum_fusion.part_ref, bf16[1,2048,1024]{2,1,0:T(8,128)(2,1)} %wg_ref.1, bf16[1,2048,1024]{2,1,0:T(8,128)(2,1)} %wu_ref.1, ...), custom_call_target="tpu_custom_call" | custom-call | tf_op jit(solution)/shard_map/moe/pallas_call | solution.py:623
  161.2 1.7 %copy.54 = bf16[64,2048]{1,0:T(8,128)(2,1)} copy(bf16[64,2048]{1,0:T(8,128)(2,1)} %moe.1) | data formatting | bytes 524288
  (14 shorter events, 0.1 us)
Async XLA Ops:
  0.0 4.0 %copy-start = (bf16[256,256]{1,0:T(8,128)(2,1)S(1)}, bf16[256,256]{1,0:T(8,128)(2,1)}, u32[]{:S(2)}) copy-start(bf16[256,256]{1,0:T(8,128)(2,1)} %param.15) | copy-start | bytes 393220
  32.2 2.2 %copy-start.4 = (bf16[2048,128]{1,0:T(8,128)(2,1)S(1)}, bf16[2048,128]{1,0:T(8,128)(2,1)}, u32[]{:S(2)}) copy-start(bf16[2048,128]{1,0:T(8,128)(2,1)} %get-tuple-element.32) | copy-start | bytes 1572868
  34.4 25.6 %copy-start.2 = (bf16[64,2048]{1,0:T(8,128)(2,1)S(1)}, bf16[64,2048]{1,0:T(8,128)(2,1)}, u32[]{:S(2)}) copy-start(bf16[64,2048]{1,0:T(8,128)(2,1)} %param.20) | copy-start | bytes 786436
  34.4 26.8 %copy-start.3 = (f32[2048]{0:T(1024)S(1)}, f32[2048]{0:T(1024)}, u32[]{:S(2)}) copy-start(f32[2048]{0:T(1024)} %param.19) | copy-start | bytes 24580
  61.1 1.7 %copy-start.1 = (bf16[64,2048]{1,0:T(8,128)(2,1)}, bf16[64,2048]{1,0:T(8,128)(2,1)S(1)}, u32[]{:S(2)}) copy-start(bf16[64,2048]{1,0:T(8,128)(2,1)S(1)} %get-tuple-element.37.mixed_ref) | copy-start | bytes 786436

commit v2 on v1

--- a/solution.py
+++ b/solution.py
@@ -337,7 +337,7 @@
 
 
 def moe_kernel(
-    n, cuts, x_ref, mixed_ref, slot_ref, part_ref, wg_ref, wu_ref, wd_ref, out_ref,
+    n, cuts, x_ref, slot_ref, part_ref, wg_ref, wu_ref, wd_ref, out_ref,
     tok, wg, wu, wd, picked, hid, wsel, held, own, give, take,
     low, high, from_x, from_y, to_y, to_x, last_y, last_x, acc, zsend, zrecv,
     load, zs, zr, sq_s, sq_r, pd_s, pd_r, tk_s, tk_r, hop_s, hop_r, hz_s, hz_r,
@@ -352,7 +352,7 @@
     share, depth = x_ref.shape
     units = wg.shape[1]
     group = 4 * share
-    slots = wsel.shape[2] // 2
+    slots = wsel.shape[3] // 2
     width = depth // cuts
     half = width // 2
     steps = chips * cuts
@@ -382,110 +382,171 @@
         greet_one({"sp": 2 * lax.rem(chip + d, chips) + core})
     pl.semaphore_wait(barrier, chips + 2)
 
-    def to_plane(p):
-        return remote(x_ref, tok.at[chip, core, mine], zs.at[p], zr.at[chip], {"sp": 2 * p + core})
-
-    def from_plane(p):
-        return remote(x_ref, tok.at[p, core, mine], zs.at[p], zr.at[p], {"sp": 2 * p + core})
+    has_right, has_left = chip < chips - 1, chip > 0
+
+    def cols(h):
+        return pl.ds(pl.multiple_of(h * (depth // 2), depth // 2), depth // 2)
+
+    def own_half(h):
+        return x_ref.at[:, cols(h)]
+
+    def along_z(p, h, way, first=False):
+        block = tok.at[p, core, h, mine]
+        to = 2 * (chip + 1 - 2 * way) + core
+        return remote(
+            own_half(h) if first else block, block, zs.at[p, h, way], zr.at[p, h], {"sp": to}
+        )
 
     upper, lower = pl.ds(0, share // 2), pl.ds(share // 2, share // 2)
 
-    def pass_on(p, way, first=False):
-        block = tok.at[p, core]
+    def pass_on(p, h, way, first=False):
+        block = tok.at[p, core, h]
+        start = own_half(h) if first else block.at[mine]
         src, dst, where = (
-            (x_ref if first else block.at[mine], block.at[mine], across),
-            (x_ref if first else block.at[mine], block.at[mine], along),
+            (start, block.at[mine], across),
+            (start, block.at[mine], along),
             (block.at[across, upper], block.at[across, upper], along),
             (block.at[along, lower], block.at[along, lower], across),
         )[way]
-        return remote(src, dst, sq_s.at[p, way], sq_r.at[p, way], {"tp": where})
-
-    def arrive(p, way):
-        block = tok.at[p, core]
+        return remote(src, dst, sq_s.at[p, h, way], sq_r.at[p, h, way], {"tp": where})
+
+    def arrive(p, h, way):
+        block = tok.at[p, core, h]
         dst = (
             block.at[across],
             block.at[along],
             block.at[corner, upper],
             block.at[corner, lower],
         )[way]
-        remote(dst, dst, sq_s.at[p, way], sq_r.at[p, way], {"tp": across}).wait_recv()
-
-    def hand(p, t, first=False):
-        block = tok.at[p, core, t]
-        return remote(x_ref if first else block, block, pd_s.at[p, t], pd_r.at[p, t], partner)
-
-    def handed(p, t):
-        block = tok.at[p, other, t]
-        remote(block, block, pd_s.at[p, t], pd_r.at[p, t], partner).wait_recv()
-
-    pass_on(chip, 0, True).start()
-    pass_on(chip, 1, True).start()
-    for j in range(1, chips):
-
-        @pl.when(chip + j < chips)
-        def _():
-            to_plane(chip + j).start()
-
-        @pl.when(chip - j >= 0)
-        def _():
-            to_plane(chip - j).start()
-
-    hand(chip, mine, True).start()
-    tok[chip, core, mine] = x_ref[...]
+        remote(dst, dst, sq_s.at[p, h, way], sq_r.at[p, h, way], {"tp": across}).wait_recv()
+
+    def hand(p, h, t, first=False):
+        block = tok.at[p, core, h, t]
+        src = own_half(h) if first else block
+        return remote(src, block, pd_s.at[p, h, t], pd_r.at[p, h, t], partner)
+
+    def handed(p, h, t):
+        block = tok.at[p, other, h, t]
+        remote(block, block, pd_s.at[p, h, t], pd_r.at[p, h, t], partner).wait_recv()
+
+    for h in range(2):
+        pass_on(chip, h, 0, True).start()
+        pass_on(chip, h, 1, True).start()
+
+        @pl.when(has_right)
+        def _():
+            along_z(chip, h, 0, True).start()
+
+        @pl.when(has_left)
+        def _():
+            along_z(chip, h, 1, True).start()
+
+        hand(chip, h, mine, True).start()
+        tok[chip, core, h, mine] = x_ref[:, cols(h)]
+
+    def part(u):
+        return visit(chip, chips, u // 2), lax.rem(u, 2)
+
+    def finish(u):
+        p, h = part(u)
+        arrive(p, h, 2)
+        arrive(p, h, 3)
+        hand(p, h, corner).start()
 
     def expert(p):
-        arrive(p, 2)
-        arrive(p, 3)
-        hand(p, corner).start()
-        for t in range(4):
-            handed(p, t)
+        for h in range(2):
+            for t in range(4):
+                handed(p, h, t)
         for side in range(2):
             spot = slot_ref[2 * p + side]
             hit = lax.broadcasted_iota(jnp.int32, (slots, group), 0) == spot
             pick = jnp.where(hit, 1.0, 0.0).astype(tok.dtype)
             parts = part_ref[2 * p + side]
-            wsel[p, side, :slots] = jnp.where(hit, parts[0:1], 0.0).astype(wsel.dtype)
-            wsel[p, side, slots:] = jnp.where(hit, parts[1:2], 0.0).astype(wsel.dtype)
-
-            @pl.loop(0, cuts)
-            def _(q):
-                block = tok[p, side, :, :, column(q)].reshape(group, width)
+            for i in range(2):
+                turned = jnp.transpose(jnp.where(hit, parts[i : i + 1], 0.0))
+                wsel[p, side, :, i * slots : (i + 1) * slots] = turned.astype(wsel.dtype)
+            for h in range(2):
+                block = tok[p, side, h].reshape(group, depth // 2)
                 rows = jnp.dot(pick, block, preferred_element_type=jnp.float32)
-                picked[side * slots : (side + 1) * slots, column(q)] = rows.astype(picked.dtype)
-
-        @pl.loop(0, units // 256)
+                picked[side * slots : (side + 1) * slots, cols(h)] = rows.astype(picked.dtype)
+
+        @pl.loop(0, units // 512)
         def _(u):
-            cols = pl.ds(pl.multiple_of(u * 256, 256), 256)
-            gate = jnp.dot(picked[...], wg[:, cols], preferred_element_type=jnp.float32)
-            upper_part = jnp.dot(picked[...], wu[:, cols], preferred_element_type=jnp.float32)
-            hid[p, :, cols] = (jax.nn.silu(gate) * upper_part).astype(hid.dtype)
-
-    @pl.loop(0, chips)
-    def _(s):
-        @pl.when(s + 1 < chips)
-        def _():
-            p = visit(chip, chips, s + 1)
-            from_plane(p).wait_recv()
-            pass_on(p, 0).start()
-            pass_on(p, 1).start()
-            hand(p, mine).start()
-
-        p = visit(chip, chips, s)
-        arrive(p, 0)
-        pass_on(p, 2).start()
-        hand(p, across).start()
-        arrive(p, 1)
-        pass_on(p, 3).start()
-        hand(p, along).start()
-
-        @pl.when(s == 0)
+            some = pl.ds(pl.multiple_of(u * 512, 512), 512)
+            gate = jnp.dot(picked[...], wg[:, some], preferred_element_type=jnp.float32)
+            rise = jnp.dot(picked[...], wu[:, some], preferred_element_type=jnp.float32)
+            hid[p, :, some] = (jax.nn.silu(gate) * rise).astype(hid.dtype)
+
+    def forward(u):
+        p, h = part(u)
+        arrive(p, h, 0)
+        pass_on(p, h, 2).start()
+        hand(p, h, across).start()
+        arrive(p, h, 1)
+        pass_on(p, h, 3).start()
+        hand(p, h, along).start()
+
+    last = 2 * chips - 1
+
+    def passes(p):
+        return ((p < chip) & has_right) | ((p > chip) & has_left)
+
+    def relay(u):
+        p, h = part(u)
+
+        @pl.when(passes(p))
+        def _():
+            along_z(p, h, 0).wait_recv()
+
+        @pl.when((p < chip) & has_right)
+        def _():
+            along_z(p, h, 0).start()
+
+        @pl.when((p > chip) & has_left)
+        def _():
+            along_z(p, h, 1).start()
+
+    def open_up(u):
+        p, h = part(u)
+
+        @pl.when(jnp.logical_not(passes(p)))
+        def _():
+            along_z(p, h, 0).wait_recv()
+
+        pass_on(p, h, 0).start()
+        pass_on(p, h, 1).start()
+        hand(p, h, mine).start()
+
+    relay(2)
+    open_up(2)
+
+    @pl.loop(0, last)
+    def _(u):
+        forward(u)
+
+        @pl.when(u + 4 <= last)
+        def _():
+            relay(u + 4)
+
+        @pl.when(u == 0)
+        def _():
+            relay(3)
+
+        @pl.when(u + 3 <= last)
+        def _():
+            open_up(u + 3)
+
+        @pl.when(u == 0)
         def _():
             for c in loads:
                 c.wait()
 
-        @pl.when(s >= 1)
-        def _():
-            expert(visit(chip, chips, s - 1))
+        @pl.when((u == 4) | ((u > 4) & (lax.rem(u, 2) == 1)))
+        def _():
+            j = (u - 3) // 2
+            finish(2 * j)
+            finish(2 * j + 1)
+            expert(visit(chip, chips, j))
 
     def plane_of(k):
         return visit(chip, chips, lax.rem(k // cuts + 1, chips))
@@ -526,9 +587,16 @@
 
         @pl.when(step < steps)
         def _(k=step):
-            @pl.when(k == cuts)
+            @pl.when(k == cuts // 2)
             def _():
-                expert(visit(chip, chips, chips - 1))
+                forward(last)
+
+            @pl.when((k == cuts) | (k == 2 * cuts))
+            def _():
+                late = jnp.where(k == cuts, 0, 1)
+                finish(last - 3 + 2 * late)
+                finish(last - 2 + 2 * late)
+                expert(visit(chip, chips, chips - 2 + late))
 
             p, q = plane_of(k), lax.rem(k, cuts)
             out = jnp.dot(hid[p], wd[q], preferred_element_type=jnp.float32).astype(held.dtype)
@@ -538,10 +606,7 @@
                 held[side, slots:] = block
 
             def spread(side):
-                return lax.dot_general(
-                    wsel[p, side], held[side], (((0,), (0,)), ((), ())),
-                    preferred_element_type=jnp.float32,
-                )
+                return jnp.dot(wsel[p, side], held[side], preferred_element_type=jnp.float32)
 
             give[k] = spread(other).astype(give.dtype)
             swap(k).start()
@@ -576,21 +641,27 @@
 
     @pl.loop(0, cuts)
     def _(q):
-        total = acc[q] + wide(mixed_ref[:, column(q)])
+        total = acc[q]
         for d in range(1, chips):
             p = lax.rem(chip + d, chips)
             homed(p, q).wait_recv()
             total += wide(zrecv[p, q])
-        out_ref[:, column(q)] = total.astype(out_ref.dtype)
-
-    for d in range(1, chips):
-        to_plane(lax.rem(chip + d, chips)).wait_send()
-
-    @pl.loop(0, chips)
-    def _(p):
+        out_ref[:, column(q)] = total
+
+    @pl.loop(0, 2 * chips)
+    def _(u):
+        p, h = u // 2, lax.rem(u, 2)
         for way in range(4):
-            pass_on(p, way).wait_send()
-            hand(p, way).wait_send()
+            pass_on(p, h, way).wait_send()
+            hand(p, h, way).wait_send()
+
+        @pl.when((p <= chip) & has_right)
+        def _():
+            along_z(p, h, 0).wait_send()
+
+        @pl.when((p >= chip) & has_left)
+        def _():
+            along_z(p, h, 1).wait_send()
 
     @pl.loop(0, steps)
     def _(k):
@@ -603,7 +674,7 @@
             home(k).wait_send()
 
 
-def moe(n, normed, mixed, slot_rows, weight_rows, capacity, w_gate, w_up, w_down, cuts=4):
+def moe(n, normed, slot_rows, weight_rows, capacity, w_gate, w_up, w_down, cuts=4):
     share, depth = normed.shape
     units = w_gate.shape[2]
     chips = n // 2
@@ -622,17 +693,17 @@
 
     return pl.pallas_call(
         functools.partial(moe_kernel, n, cuts),
-        out_shape=jax.ShapeDtypeStruct((share, depth), kind),
-        in_specs=in_vmem(4) + [pl.BlockSpec(memory_space=pl.ANY)] * 3,
+        out_shape=jax.ShapeDtypeStruct((share, depth), jnp.float32),
+        in_specs=in_vmem(3) + [pl.BlockSpec(memory_space=pl.ANY)] * 3,
         out_specs=in_vmem(1)[0],
         scratch_shapes=[
-            room(chips, 2, 4, share, depth),
+            room(chips, 2, 2, 4, share, depth // 2),
             room(depth, units),
             room(depth, units),
             room(cuts, units, width),
             room(2 * slots, depth),
             room(chips, 2 * slots, units),
-            room(chips, 2, 2 * slots, group),
+            room(chips, 2, group, 2 * slots),
             room(2, 2 * slots, width),
             exact(2, group, width),
             room(steps, group, width),
@@ -649,12 +720,12 @@
             room(steps - cuts, share, width),
             room(chips, cuts, share, width),
             dma((2 + cuts,)),
-            dma((chips,)),
-            dma((chips,)),
-            dma((chips, 4)),
-            dma((chips, 4)),
-            dma((chips, 4)),
-            dma((chips, 4)),
+            dma((chips, 2, 2)),
+            dma((chips, 2)),
+            dma((chips, 2, 4)),
+            dma((chips, 2, 4)),
+            dma((chips, 2, 4)),
+            dma((chips, 2, 4)),
             dma((steps,)),
             dma((steps,)),
             dma((steps, 4)),
@@ -664,7 +735,7 @@
         ],
         compiler_params=params(2),
         name="moe",
-    )(normed, mixed, slot_rows, weight_rows, w_gate, w_up, w_down)
+    )(normed, slot_rows, weight_rows, w_gate, w_up, w_down)
 
 
 def start_state(batch, rows, width):
@@ -771,10 +842,9 @@
         spots = jnp.where(notes[:, 0] >= 0, notes[:, 0] + base, -1.0).astype(jnp.int32)
         coarse = lax.reduce_precision(notes[:, 1], 8, 7)
         pair = jnp.stack([coarse, notes[:, 1] - coarse], axis=1)
-        return moe(
+        summed = moe(
             sp_count,
             normed,
-            mixed,
             spots.reshape(sp_count, 1, tp_count * tok_dev),
             pair.reshape(sp_count, 2, tp_count * tok_dev),
             capacity,
@@ -782,6 +852,7 @@
             w_up,
             w_down,
         )
+        return (mixed_float_output + summed).astype(jnp.bfloat16)
     flat_routes = routes.reshape(-1)
     one_hot = (flat_routes[:, None] == jnp.arange(sp_count, dtype=jnp.int32)[None, :]).astype(
         jnp.int32

time: 163 us -> 153 us (0.939)
  Pallas kernels: 140 us -> 128 us
  other arithmetic: 12.7 us -> 15.5 us
    pallas_call x1, Pallas kernels: 98.3 us -> 86.6 us  [moe(): pl.pallas_call(functools.partial(moe_kernel, n, cuts), out_shape=jax.Shap...]
    convert_element_type x0 -> x1, other arithmetic: none -> 1.83 us  [local(): return (mixed_float_output + summed).astype(jnp.bfloat16)]
    unnamed x13 -> x12, local copies, waits for them, and re-layouts: 3.52 us -> 1.85 us
where the time goes in v2:
time: 153 us; the launch traced here: 152 us
  Pallas kernels  128 us (84%)
  other arithmetic  15.5 us (10%)
  local copies, waits for them, and re-layouts  4.58 us (3%)
  matrix products  3.64 us (2%)
    pallas_call x1, Pallas kernels, moe(): pl.pallas_call(functools.partial(moe_kernel, n, cuts), out_shape=jax.Shap...  86.6 us
    pallas_call x1, Pallas kernels, project(): pl.pallas_call(project_kernel, out_shape=(jax.ShapeDtypeStruct((share, ou...  21.4 us
    pallas_call x1, Pallas kernels, gather_rows(): pl.pallas_call(functools.partial(gather_kernel, n), out_shape=tuple((jax....  20.4 us

profile of v2, /device:TPU:0, one launch (start us, length us, event | category | flops | bytes accessed | tf_op | source)
XLA Modules:
  0.0 152.3 jit_solution(18411040517379380682)
XLA Ops:
  0.0 0.0 copy-start
  0.0 1.0 fusion.16
  1.0 1.0 fusion.18
  2.0 1.2 fusion.24
  3.2 0.8 maximum_bitcast_fusion.1.k_ref
  4.0 0.0 copy-done
  4.0 0.6 constant_dynamic-slice_fusion.1.v_ref
  4.6 0.7 fusion.28
  5.3 0.1 copy.44
  5.4 0.1 reduce_window_sum.11
  5.5 0.1 copy.45
  5.6 0.7 select_reduce_fusion
  6.3 0.7 maximum_bitcast_fusion.2.n_ref
  6.9 20.4 %gather_rows.1 = (bf16[2048,128]{1,0:T(8,128)(2,1)}, bf16[2048,128]{1,0:T(8,128)(2,1)}, f32[64,128]{1,0:T(8,128)}) custom-call(bf16[256,128]{1,0:T(8,128)(2,1)} %maximum_bitcast_fusion.1.k_ref, bf16[256,128]{1,0:T(8,128)(2,1)} %constant_dynamic-slice_fusion.1.v_ref, f32[8,128]{1,0:T(8,128)} %maximum_bitcast_fusion.2.n_ref), custom_call_target="tpu_custom_call" | custom-call | tf_op jit(solution)/shard_map/gather_rows/pallas_call | solution.py:228
  27.3 0.3 multiply_cosine_fusion.3
  27.6 1.1 copy.40
  28.7 0.1 fusion.2
  28.8 0.8 fusion.3
  29.6 0.1 subtract_convert_fusion.1
  29.7 0.2 copy.41
  29.9 2.4 %multiply_reduce_fusion = (f32[1024]{0:T(1024)S(1)}, f32[1024,2048]{1,0:T(8,128)S(1)}) fusion(bf16[1024,128]{1,0:T(8,128)(2,1)S(1)} %bitcast.34, bf16[2048,128]{1,0:T(8,128)(2,1)} %get-tuple-element.30), kind=kOutput, calls=%fused_computation.2 | convolution fusion | flops 541064192 | bytes 9179136 | tf_op jit(solution)/shard_map/while/body/eval_jaxpr/hxt,ght->hxg/dot_general | solution.py:62
  32.2 0.0 copy-start.4
  32.3 2.1 %convert_reduce_fusion = (f32[1024]{0:T(1024)S(1)}, bf16[1024,2048]{1,0:T(8,128)(2,1)S(1)}) fusion(f32[1024]{0:T(1024)S(1)} %broadcast_maximum_fusion, f32[1024,2048]{1,0:T(8,128)S(1)} %get-tuple-element.62), kind=kLoop, calls=%fused_computation | loop fusion | flops 10484736 | bytes 12591104 | tf_op jit(solution)/shard_map/while/body/eval_jaxpr/reduce_sum | solution.py:70
  34.4 0.0 copy-start.1
  34.4 0.0 copy-start.3
  34.4 0.0 copy-done.4
  34.4 1.3 fusion.1
  35.7 0.2 copy.46
  35.9 0.7 copy.51
  36.7 21.4 %project.1 = (bf16[64,2048]{1,0:T(8,128)(2,1)}, f32[4,64,128]{2,1,0:T(8,128)}) custom-call(bf16[256,512]{1,0:T(8,128)(2,1)} %bitcast.35, bf16[2048,512]{1,0:T(8,128)(2,1)} %w_ref.1, f32[64,128]{1,0:T(8,128)} %get-tuple-element.33.n_ref), custom_call_target="tpu_custom_call" | custom-call | tf_op jit(solution)/shard_map/project/pallas_call | solution.py:304
  58.0 0.0 copy-start.2
  58.0 1.1 reshape.402
  59.3 0.1 stack.10
  59.3 0.1 stack.9
  59.4 0.6 pad_maximum_fusion.part_ref
  60.0 0.1 squeeze.16
  60.1 0.1 add.145
  60.2 0.1 add.146
  60.3 0.6 fusion.27.slot_ref
  60.9 0.0 copy-done.1
  60.9 1.1 fusion.4
  62.1 0.0 copy-done.3
  62.1 1.8 %fusion.6.x_ref = bf16[64,2048]{1,0:T(8,128)(2,1)} fusion(f32[2048]{0:T(1024)S(1)} %copy-done.3, f32[64]{0:T(128)S(1)} %add_rsqrt_fusion.2, bf16[64,2048]{1,0:T(8,128)(2,1)} %get-tuple-element.34, bf16[64,2048]{1,0:T(8,128)(2,1)S(1)} %copy-done.1), kind=kLoop, calls=%fused_computation.15 | loop fusion | flops 1048576 | bytes 794880 | tf_op jit(solution)/shard_map/convert_element_type | solution.py:836
  63.8 86.6 %moe.1 = f32[64,2048]{1,0:T(8,128)} custom-call(bf16[64,2048]{1,0:T(8,128)(2,1)} %fusion.6.x_ref, s32[8,1,256]{2,1,0:T(1,128)} %fusion.27.slot_ref, f32[8,2,256]{2,1,0:T(2,128)} %pad_maximum_fusion.part_ref, bf16[1,2048,1024]{2,1,0:T(8,128)(2,1)} %wg_ref.1, bf16[1,2048,1024]{2,1,0:T(8,128)(2,1)} %wu_ref.1, bf16[1,1024,2048]{2,1,0:T(8,128)(2,1)} %wd_ref.1), custom_call_target="tpu_custom_call" | custom-call | tf_op jit(solution)/shard_map/moe/pallas_call | solution.py:694
  150.4 0.0 copy-done.2
  150.4 1.8 %fusion.7 = bf16[64,2048]{1,0:T(8,128)(2,1)} fusion(f32[64,2048]{1,0:T(8,128)} %moe.1, bf16[64,2048]{1,0:T(8,128)(2,1)S(1)} %copy-done.2, bf16[64,2048]{1,0:T(8,128)(2,1)S(1)} %copy-done.1), kind=kLoop, calls=%fused_computation.16 | loop fusion | flops 917504 | bytes 1310720 | tf_op jit(solution)/shard_map/convert_element_type | solution.py:855
  (14 shorter events, 0.1 us)
Async XLA Ops:
  0.0 4.0 %copy-start = (bf16[256,256]{1,0:T(8,128)(2,1)S(1)}, bf16[256,256]{1,0:T(8,128)(2,1)}, u32[]{:S(2)}) copy-start(bf16[256,256]{1,0:T(8,128)(2,1)} %param.15) | copy-start | bytes 393220
  32.2 2.2 %copy-start.4 = (bf16[2048,128]{1,0:T(8,128)(2,1)S(1)}, bf16[2048,128]{1,0:T(8,128)(2,1)}, u32[]{:S(2)}) copy-start(bf16[2048,128]{1,0:T(8,128)(2,1)} %get-tuple-element.32) | copy-start | bytes 1572868
  34.4 26.5 %copy-start.1 = (bf16[64,2048]{1,0:T(8,128)(2,1)S(1)}, bf16[64,2048]{1,0:T(8,128)(2,1)}, u32[]{:S(2)}) copy-start(bf16[64,2048]{1,0:T(8,128)(2,1)} %param.20) | copy-start | bytes 786436
  34.4 27.7 %copy-start.3 = (f32[2048]{0:T(1024)S(1)}, f32[2048]{0:T(1024)}, u32[]{:S(2)}) copy-start(f32[2048]{0:T(1024)} %param.19) | copy-start | bytes 24580
  58.0 92.4 %copy-start.2 = (bf16[64,2048]{1,0:T(8,128)(2,1)S(1)}, bf16[64,2048]{1,0:T(8,128)(2,1)}, u32[]{:S(2)}) copy-start(bf16[64,2048]{1,0:T(8,128)(2,1)} %get-tuple-element.34) | copy-start | bytes 786436

commit v3 on v2

--- a/solution.py
+++ b/solution.py
@@ -2,6 +2,7 @@
 
 import jax
 import jax.numpy as jnp
+import numpy as np
 from jax import lax
 from jax.experimental import pallas as pl
 from jax.experimental.pallas import tpu as pltpu
@@ -99,229 +100,353 @@
     return mine, mine + 1 - 2 * lax.rem(mine, 2), lax.rem(mine + 2, 4), 3 - mine
 
 
-def gather_kernel(n, k_ref, v_ref, n_ref, ko_ref, vo_ref, no_ref, send, recv):
+def in_vmem(count):
+    return [pl.BlockSpec(memory_space=pltpu.VMEM)] * count
+
+
+def params(number):
+    return pltpu.CompilerParams(
+        collective_id=number, has_side_effects=True, vmem_limit_bytes=VMEM_LIMIT
+    )
+
+
+def turn_tables(width, rows):
+    quarter = width // 4
+    freqs = ROPE_BASE ** (-np.arange(quarter, dtype=np.float32) / np.float32(quarter))
+    zero = np.zeros((max(rows, GRID_W), quarter), np.float32)
+
+    def table(count, blocks):
+        angle = np.arange(count, dtype=np.float32)[:, None] * freqs.astype(np.float32)[None, :]
+        kinds = {"c": np.cos(angle), "s": np.sin(angle), "m": -np.sin(angle), "0": zero[:count]}
+        return np.stack([np.concatenate([kinds[k] for k in b], axis=1) for b in blocks])
+
+    by_col = table(GRID_W, ("00cc", "00m0", "000s"))
+    by_row = table(rows, ("cc00", "m000", "0s00"))
+    return by_col.astype(np.float32), by_row.astype(np.float32)
+
+
+def attend_kernel(
+    n, q_ref, k_ref, v_ref, qg_ref, kg_ref, col_ref, row_ref, res_ref, gain_ref, name_ref, share_ref, w_ref,
+    mixed_ref, normed_ref, notes_ref,
+    w, kv, qs, top, acc, held, total, stage, proj, sheet,
+    load, zs, zr, xs, xr, ds, dr, ns, nr, fs, fr, give, take, tell, told,
+):
     me = lax.axis_index("sp")
     chips = n // 2
     chip, core = me // 2, lax.rem(me, 2)
-    partner = 2 * chip + 1 - core
-    has_right, has_left = chip < chips - 1, chip > 0
-    right, left = me + 2, me - 2
+    other = 1 - core
+    partner = {"sp": 2 * chip + other}
+    mine, across, along, corner = square()
+    x = lax.rem(mine, 2)
+    rows, width = q_ref.shape
+    size = qg_ref.shape[1]
+    heads = width // size
+    pairs = heads // 2
+    share = rows // 4
+    keys_half = rows // 2
+    fetch = pltpu.make_async_copy(w_ref, w, load.at[0])
+    fetch.start()
+
     barrier = pltpu.get_barrier_semaphore()
-    pl.semaphore_signal(barrier, inc=1, device_id={"sp": partner}, device_id_type=MESH)
-
-    @pl.when(has_right)
-    def _():
-        pl.semaphore_signal(barrier, inc=1, device_id={"sp": right}, device_id_type=MESH)
-
-    @pl.when(has_left)
-    def _():
-        pl.semaphore_signal(barrier, inc=1, device_id={"sp": left}, device_id_type=MESH)
-
-    pl.semaphore_wait(barrier, 1 + has_right.astype(jnp.int32) + has_left.astype(jnp.int32))
-
-    pairs = ((k_ref, ko_ref), (v_ref, vo_ref), (n_ref, no_ref))
-
-    def block(out, origin):
-        rows = out.shape[0] // n
-        return out.at[pl.ds(pl.multiple_of(origin * rows, rows), rows)]
-
-    def copies(origin, way, where, own=False):
-        return [
-            remote(
-                ref if own else block(out, origin),
-                block(out, origin),
-                send.at[origin, way, i],
-                recv.at[origin, i],
-                {"sp": where},
-            )
-            for i, (ref, out) in enumerate(pairs)
-        ]
-
-    def start(*args, **kw):
-        for c in copies(*args, **kw):
-            c.start()
-
-    def sent(*args, **kw):
-        for c in copies(*args, **kw):
-            c.wait_send()
-
-    def arrived(origin):
-        for c in copies(origin, 0, partner):
-            c.wait_recv()
-
-    @pl.when(has_right)
-    def _():
-        start(me, 0, right, own=True)
-
-    @pl.when(has_left)
-    def _():
-        start(me, 2, left, own=True)
-
-    start(me, 1, partner, own=True)
-    for ref, out in pairs:
-        block(out, me)[...] = ref[...]
+    peers = [lax.rem(me + d, n) for d in range(1, n)]
+    for p in peers:
+        pl.semaphore_signal(barrier, inc=1, device_id={"sp": p}, device_id_type=MESH)
+    for p in (across, along, corner):
+        pl.semaphore_signal(barrier, inc=1, device_id={"tp": p}, device_id_type=MESH)
+
+    def turned(part, gain_row, g):
+        values = part.astype(jnp.float32)
+        mean = jnp.mean(values * values, axis=-1, keepdims=True)
+        scaled = values * lax.rsqrt(mean + EPS) * gain_row
+        grid_row = pl.ds(me * (rows // GRID_W) + g, 1)
+        turn = [col_ref[i] + row_ref[i, grid_row] for i in range(3)]
+        return (
+            scaled * turn[0]
+            + pltpu.roll(scaled, size - size // 4, 1) * turn[1]
+            + pltpu.roll(scaled, size // 4, 1) * turn[2]
+        ).astype(jnp.bfloat16)
+
+    kv_heads = k_ref.shape[1] // size
+    kv_head = mine * kv_heads // 4
+    at = pl.ds(pl.multiple_of(kv_head * size, size), size)
+    for g in range(rows // GRID_W):
+        span = pl.ds(g * GRID_W, GRID_W)
+        side, low = (g * GRID_W) // keys_half, (g * GRID_W) % keys_half
+        place = pl.ds(low, GRID_W)
+        kv[chip, core, side, 0, place] = turned(k_ref[span, at], kg_ref[...], g)
+        kv[chip, core, side, 1, place] = v_ref[span, at]
+    lanes = lax.broadcasted_iota(jnp.int32, (n, 2 * share), 1)
+    expert = lax.broadcasted_iota(jnp.int32, (n, 2 * share), 0)
+    first_one, second_one = name_ref[0:1] == expert, name_ref[1:2] == expert
+    taken = jnp.where((first_one | second_one) & (lanes < share), 1.0, 0.0)
+    before = lax.broadcasted_iota(jnp.int32, (2 * share, 2 * share), 0)
+    after = lax.broadcasted_iota(jnp.int32, (2 * share, 2 * share), 1)
+    ladder = jnp.where(before < after, 1.0, 0.0).astype(jnp.bfloat16)
+    slot = jnp.dot(taken.astype(jnp.bfloat16), ladder, preferred_element_type=jnp.float32)
+    weight = jnp.where(first_one, share_ref[0:1], 0.0) + jnp.where(second_one, share_ref[1:2], 0.0)
+    sheet[me] = jnp.where(lanes < share, jnp.where(taken > 0, slot, -1.0), weight)
+
+    pl.semaphore_wait(barrier, n + 2)
+
+    def to_plane(p):
+        block = kv.at[chip, core, x]
+        return remote(block, block, zs.at[p], zr.at[chip], {"sp": 2 * p + core})
+
+    def from_plane(p):
+        block = kv.at[p, core, x]
+        remote(block, block, zs.at[p], zr.at[p], partner).wait_recv()
+
+    def sideways(p):
+        block = kv.at[p, core, x]
+        return remote(block, block, xs.at[p], xr.at[p], {"tp": across})
+
+    def from_side(p):
+        block = kv.at[p, core, 1 - x]
+        remote(block, block, xs.at[p], xr.at[p], partner).wait_recv()
+
+    def hand(p, side):
+        block = kv.at[p, core, side]
+        return remote(block, block, ds.at[p, side], dr.at[p, side], partner)
+
+    def handed(p, side):
+        block = kv.at[p, other, side]
+        remote(block, block, ds.at[p, side], dr.at[p, side], partner).wait_recv()
+
     for j in range(1, chips):
 
+        @pl.when(chip + j < chips)
+        def _():
+            to_plane(chip + j).start()
+
         @pl.when(chip - j >= 0)
-        def _(origin=me - 2 * j):
-            arrived(origin)
-
-            @pl.when(has_right)
+        def _():
+            to_plane(chip - j).start()
+
+    for side in range(2):
+        hand(chip, side).start()
+    inform = [
+        remote(sheet.at[me], sheet.at[me], ns.at[d], nr.at[d], {"sp": p})
+        for d, p in enumerate(peers)
+    ]
+    for c in inform:
+        c.start()
+
+    @pl.loop(0, heads)
+    def _(h):
+        @pl.loop(0, rows // GRID_W)
+        def _(g):
+            span = pl.ds(pl.multiple_of(g * GRID_W, GRID_W), GRID_W)
+            block = q_ref[span, pl.ds(pl.multiple_of(h * size, size), size)]
+            qs[h, span] = turned(block, qg_ref[...], g)
+
+        top[h] = jnp.full(top.shape[1:], NEG_START, jnp.float32)
+        acc[h] = jnp.zeros(acc.shape[1:], jnp.float32)
+
+    grade = size ** (-0.5) * 1.4426950408889634
+
+    def first(j, way):
+        block = held.at[mine, j]
+        where = (across, along)[way]
+        return remote(block, block, fs.at[j, way], fr.at[j, way], {"tp": where})
+
+    upper, lower = pl.ds(0, rows // 2), pl.ds(rows // 2, rows // 2)
+
+    def second(j, way):
+        block = (held.at[across, j, upper], held.at[along, j, lower])[way]
+        where = (along, across)[way]
+        return remote(block, block, fs.at[j, 2 + way], fr.at[j, 2 + way], {"tp": where})
+
+    def arrive(j, way):
+        block = (
+            held.at[across, j],
+            held.at[along, j],
+            held.at[corner, j, upper],
+            held.at[corner, j, lower],
+        )[way]
+        remote(block, block, fs.at[j, way], fr.at[j, way], partner).wait_recv()
+
+    @pl.loop(0, chips)
+    def _(s):
+        @pl.when(s + 1 < chips)
+        def _():
+            p = visit(chip, chips, s + 1)
+            from_plane(p)
+            sideways(p).start()
+            hand(p, x).start()
+
+        p = visit(chip, chips, s)
+
+        @pl.when(s > 0)
+        def _():
+            from_side(p)
+            hand(p, 1 - x).start()
+
+        for side in range(2):
+            handed(p, side)
+
+        @pl.loop(0, pairs)
+        def _(j):
+            for i in range(2):
+                h = 2 * j + i
+                keys = kv[p, :, :, 0].reshape(2 * rows, size)
+                values = kv[p, :, :, 1].reshape(2 * rows, size)
+                scores = lax.dot_general(
+                    qs[h], keys, (((1,), (1,)), ((), ())), preferred_element_type=jnp.float32
+                )
+                old = top[h]
+                new = jnp.maximum(old, jnp.max(scores, axis=1, keepdims=True))
+                top[h] = new
+                weights = jnp.exp2((scores - new[:, :1]) * grade).astype(jnp.bfloat16)
+                full = jnp.concatenate([values, jnp.ones_like(values)], axis=1)
+                grown = jnp.dot(weights, full, preferred_element_type=jnp.float32)
+                factor = jnp.exp2((old - new) * grade)
+                acc[h] = acc[h] * jnp.concatenate([factor, factor], axis=1) + grown
+
+            @pl.when(s == chips - 1)
             def _():
-                start(origin, 0, right)
-
-            start(origin, 1, partner)
-
-        @pl.when(chip + j < chips)
-        def _(origin=me + 2 * j):
-            arrived(origin)
-
-            @pl.when(has_left)
-            def _():
-                start(origin, 2, left)
-
-            start(origin, 1, partner)
-
-    for z in range(chips):
-        arrived(2 * z + 1 - core)
-    sent(me, 1, partner, own=True)
-
-    @pl.when(has_right)
-    def _():
-        sent(me, 0, right, own=True)
-
-    @pl.when(has_left)
-    def _():
-        sent(me, 2, left, own=True)
-
-    for j in range(1, chips):
-
-        @pl.when(chip - j >= 0)
-        def _(origin=me - 2 * j):
-            @pl.when(has_right)
-            def _():
-                sent(origin, 0, right)
-
-            sent(origin, 1, partner)
-
-        @pl.when(chip + j < chips)
-        def _(origin=me + 2 * j):
-            @pl.when(has_left)
-            def _():
-                sent(origin, 2, left)
-
-            sent(origin, 1, partner)
-
-
-def in_vmem(count):
-    return [pl.BlockSpec(memory_space=pltpu.VMEM)] * count
-
-
-def params(number):
-    return pltpu.CompilerParams(
-        collective_id=number, has_side_effects=True, vmem_limit_bytes=VMEM_LIMIT
-    )
-
-
-def gather_rows(n, own_keys, own_values, notes):
-    arrays = (own_keys, own_values, notes)
-    return pl.pallas_call(
-        functools.partial(gather_kernel, n),
-        out_shape=tuple(
-            jax.ShapeDtypeStruct((n * a.shape[0], a.shape[1]), a.dtype) for a in arrays
-        ),
-        in_specs=in_vmem(3),
-        out_specs=tuple(in_vmem(3)),
-        scratch_shapes=[pltpu.SemaphoreType.DMA((n, 3, 3)), pltpu.SemaphoreType.DMA((n, 3))],
-        compiler_params=params(0),
-        name="gather_rows",
-    )(*arrays)
-
-
-def project_kernel(
-    attn_ref, w_ref, n_ref, out_ref, no_ref, held, stage, send, recv, give, take, tell, told
-):
-    mine, across, along, corner = square()
-    rows, width = attn_ref.shape
-    half = rows // 2
-    share = out_ref.shape[0]
-    greet([{"tp": across}, {"tp": along}, {"tp": corner}], 3)
-    first = [
-        remote(attn_ref, held.at[mine], send.at[0], recv.at[0], {"tp": across}),
-        remote(attn_ref, held.at[mine], send.at[1], recv.at[1], {"tp": along}),
-    ]
-    for c in first:
-        c.start()
-    notes = [
-        remote(n_ref, no_ref.at[mine], tell.at[i], told.at[i], {"tp": p})
-        for i, p in enumerate((corner, across, along))
-    ]
-    for c in notes:
-        c.start()
-    no_ref[mine] = n_ref[...]
-    top, low = pl.ds(0, half), pl.ds(half, half)
-    second = [
-        remote(held.at[across, top], held.at[across, top], send.at[2], recv.at[2], {"tp": along}),
-        remote(held.at[along, low], held.at[along, low], send.at[3], recv.at[3], {"tp": across}),
-    ]
-
-    def term(rows_here, owner):
-        part = w_ref[pl.ds(pl.multiple_of(owner * width, width), width), :]
-        return jnp.dot(rows_here, part, preferred_element_type=jnp.float32)
-
-    total = term(attn_ref[...], mine)
-    first[0].wait_recv()
-    second[0].start()
-    first[1].wait_recv()
-    second[1].start()
-    total += term(held[across], across)
-    total += term(held[along], along)
-    for c in second:
-        c.wait_recv()
-    total += term(held[corner], corner)
-    stage[...] = total.astype(stage.dtype)
+                for i in range(2):
+                    done = acc[2 * j + i]
+                    ratio = done[:, :size] / done[:, size:]
+                    held[mine, j, :, i * size : (i + 1) * size] = ratio.astype(held.dtype)
+                first(j, 0).start()
+                first(j, 1).start()
+
+        @pl.when(s == chips - 2)
+        def _():
+            for c in inform:
+                c.wait_recv()
+            notes_ref[mine] = sheet[...]
+            for i, p in enumerate((corner, across, along)):
+                remote(sheet, notes_ref.at[mine], tell.at[i], told.at[i], {"tp": p}).start()
+
+    fetch.wait()
+
+    def term(owner, j):
+        start = pl.multiple_of(owner * width + j * 2 * size, 2 * size)
+        part = w[pl.ds(start, 2 * size), :]
+        total[...] += jnp.dot(held[owner, j], part, preferred_element_type=jnp.float32)
+
+    total[...] = jnp.zeros_like(total)
+
+    @pl.loop(0, pairs)
+    def _(j):
+        term(mine, j)
+
+    @pl.loop(0, pairs)
+    def _(j):
+        arrive(j, 0)
+        second(j, 0).start()
+        arrive(j, 1)
+        second(j, 1).start()
+        term(across, j)
+        term(along, j)
+
+    @pl.loop(0, pairs)
+    def _(j):
+        arrive(j, 2)
+        arrive(j, 3)
+        term(corner, j)
+
+    stage[...] = total[...].astype(stage.dtype)
     columns = pl.ds(pl.multiple_of(mine * width, width), width)
 
     def piece(owner):
         return pl.ds(pl.multiple_of(owner * share, share), share)
 
     back = [
-        remote(stage.at[piece(p)], out_ref.at[:, columns], give.at[i], take.at[i], {"tp": p})
+        remote(stage.at[piece(p)], proj.at[:, columns], give.at[i], take.at[i], {"tp": p})
         for i, p in enumerate((corner, across, along))
     ]
     for c in back:
         c.start()
-    out_ref[:, columns] = stage[piece(mine), :]
-    for c in back + notes:
+    proj[:, columns] = stage[piece(mine), :]
+    for c in back:
         c.wait()
-    for c in first + second:
+    mixed = (res_ref[...].astype(jnp.float32) + proj[...].astype(jnp.float32)).astype(mixed_ref.dtype)
+    mixed_ref[...] = mixed
+    mixed = mixed.astype(jnp.float32)
+    mean = jnp.mean(mixed * mixed, axis=-1, keepdims=True)
+    normed_ref[...] = (mixed * lax.rsqrt(mean + EPS) * gain_ref[...]).astype(normed_ref.dtype)
+
+    for i, p in enumerate((corner, across, along)):
+        remote(sheet, notes_ref.at[mine], tell.at[i], told.at[i], {"tp": p}).wait()
+    for c in inform:
         c.wait_send()
-
-
-def project(attn, out_proj, notes, share):
-    rows, width = attn.shape
-    parts = out_proj.shape[0] // width
+    for d in range(1, chips):
+        p = lax.rem(chip + d, chips)
+        to_plane(p).wait_send()
+        sideways(p).wait_send()
+    for p in range(chips):
+        for side in range(2):
+            hand(p, side).wait_send()
+    for j in range(pairs):
+        for way in range(2):
+            first(j, way).wait_send()
+            second(j, way).wait_send()
+
+
+def attend(n, queries, keys, values, query_gain, key_gain, residual, gain, names, shares, out_proj):
+    rows, width = queries.shape
+    size = query_gain.shape[0]
+    heads = width // size
+    share, depth = residual.shape
+    chips = n // 2
+    kind = queries.dtype
+    by_col, by_row = turn_tables(size, n * rows // GRID_W)
+    dma = pltpu.SemaphoreType.DMA
+    exact = jnp.float32
     return pl.pallas_call(
-        project_kernel,
+        functools.partial(attend_kernel, n),
         out_shape=(
-            jax.ShapeDtypeStruct((share, out_proj.shape[1] * parts), jnp.bfloat16),
-            jax.ShapeDtypeStruct((parts,) + notes.shape, notes.dtype),
+            jax.ShapeDtypeStruct((share, depth), kind),
+            jax.ShapeDtypeStruct((share, depth), kind),
+            jax.ShapeDtypeStruct((4, n, n, 2 * share), exact),
         ),
-        in_specs=in_vmem(3),
-        out_specs=tuple(in_vmem(2)),
+        in_specs=in_vmem(11) + [pl.BlockSpec(memory_space=pl.ANY)],
+        out_specs=tuple(in_vmem(3)),
         scratch_shapes=[
-            pltpu.VMEM((parts, rows, width), jnp.bfloat16),
-            pltpu.VMEM((rows, out_proj.shape[1]), jnp.bfloat16),
-            pltpu.SemaphoreType.DMA((4,)),
-            pltpu.SemaphoreType.DMA((4,)),
-            pltpu.SemaphoreType.DMA((3,)),
-            pltpu.SemaphoreType.DMA((3,)),
-            pltpu.SemaphoreType.DMA((3,)),
-            pltpu.SemaphoreType.DMA((3,)),
+            pltpu.VMEM(out_proj.shape, kind),
+            pltpu.VMEM((chips, 2, 2, 2, rows // 2, size), kind),
+            pltpu.VMEM((heads, rows, size), kind),
+            pltpu.VMEM((heads, rows, size), exact),
+            pltpu.VMEM((heads, rows, 2 * size), exact),
+            pltpu.VMEM((4, heads // 2, rows, 2 * size), kind),
+            pltpu.VMEM((rows, width), exact),
+            pltpu.VMEM((rows, width), kind),
+            pltpu.VMEM((share, depth), kind),
+            pltpu.VMEM((n, n, 2 * share), exact),
+            dma((1,)),
+            dma((chips,)),
+            dma((chips,)),
+            dma((chips,)),
+            dma((chips,)),
+            dma((chips, 2)),
+            dma((chips, 2)),
+            dma((n - 1,)),
+            dma((n - 1,)),
+            dma((heads // 2, 4)),
+            dma((heads // 2, 4)),
+            dma((3,)),
+            dma((3,)),
+            dma((3,)),
+            dma((3,)),
         ],
         compiler_params=params(1),
-        name="project",
-    )(attn, out_proj, notes)
+        name="attend",
+    )(
+        queries,
+        keys,
+        values,
+        query_gain[None, :],
+        key_gain[None, :],
+        jnp.asarray(by_col),
+        jnp.asarray(by_row),
+        residual,
+        gain[None, :],
+        names,
+        shares,
+        out_proj,
+    )
 
 
 def visit(chip, chips, step):
@@ -337,7 +462,7 @@
 
 
 def moe_kernel(
-    n, cuts, x_ref, slot_ref, part_ref, wg_ref, wu_ref, wd_ref, out_ref,
+    n, cuts, x_ref, note_ref, wg_ref, wu_ref, wd_ref, out_ref,
     tok, wg, wu, wd, picked, hid, wsel, held, own, give, take,
     low, high, from_x, from_y, to_y, to_x, last_y, last_x, acc, zsend, zrecv,
     load, zs, zr, sq_s, sq_r, pd_s, pd_r, tk_s, tk_r, hop_s, hop_r, hz_s, hz_r,
@@ -458,12 +583,33 @@
             for t in range(4):
                 handed(p, h, t)
         for side in range(2):
-            spot = slot_ref[2 * p + side]
+            tiles = [note_ref[t, 2 * p + side] for t in range(4)]
+            lane = lax.broadcasted_iota(jnp.int32, (n, 2 * share), 1)
+            chosen = lax.broadcasted_iota(jnp.int32, (n, 2 * share), 0) == me
+
+            def across_two(even, odd, swap_even):
+                moved = pltpu.roll(even if swap_even else odd, share, 1)
+                return jnp.where(lane < share, moved, odd) if swap_even else jnp.where(
+                    lane < share, even, moved
+                )
+
+            def row_of(swap_even):
+                parts_two = [across_two(tiles[t], tiles[t + 1], swap_even) for t in (0, 2)]
+                picks = [
+                    jnp.sum(jnp.where(chosen, v, 0.0), axis=0, keepdims=True) for v in parts_two
+                ]
+                return jnp.concatenate(picks, axis=1)
+
+            spot = row_of(False)
+            base = lax.broadcasted_iota(jnp.int32, (1, group), 1) // share * (slots // 4)
+            spot = jnp.where(spot >= 0, spot.astype(jnp.int32) + base, -1)
+            weight = row_of(True)
+            coarse = weight.astype(jnp.bfloat16).astype(jnp.float32)
+            parts = (coarse, weight - coarse)
             hit = lax.broadcasted_iota(jnp.int32, (slots, group), 0) == spot
             pick = jnp.where(hit, 1.0, 0.0).astype(tok.dtype)
-            parts = part_ref[2 * p + side]
             for i in range(2):
-                turned = jnp.transpose(jnp.where(hit, parts[i : i + 1], 0.0))
+                turned = jnp.transpose(jnp.where(hit, parts[i], 0.0))
                 wsel[p, side, :, i * slots : (i + 1) * slots] = turned.astype(wsel.dtype)
             for h in range(2):
                 block = tok[p, side, h].reshape(group, depth // 2)
@@ -674,7 +820,7 @@
             home(k).wait_send()
 
 
-def moe(n, normed, slot_rows, weight_rows, capacity, w_gate, w_up, w_down, cuts=4):
+def moe(n, normed, notes, capacity, w_gate, w_up, w_down, cuts=4):
     share, depth = normed.shape
     units = w_gate.shape[2]
     chips = n // 2
@@ -694,7 +840,7 @@
     return pl.pallas_call(
         functools.partial(moe_kernel, n, cuts),
         out_shape=jax.ShapeDtypeStruct((share, depth), jnp.float32),
-        in_specs=in_vmem(3) + [pl.BlockSpec(memory_space=pl.ANY)] * 3,
+        in_specs=in_vmem(2) + [pl.BlockSpec(memory_space=pl.ANY)] * 3,
         out_specs=in_vmem(1)[0],
         scratch_shapes=[
             room(chips, 2, 2, 4, share, depth // 2),
@@ -735,7 +881,7 @@
         ],
         compiler_params=params(2),
         name="moe",
-    )(normed, slot_rows, weight_rows, w_gate, w_up, w_down)
+    )(normed, notes, w_gate, w_up, w_down)
 
 
 def start_state(batch, rows, width):
@@ -772,6 +918,35 @@
     scale = head_size ** (-0.5)
     tp_index = lax.axis_index("tp")
     sp_index = lax.axis_index("sp")
+    tok_dev = residual.shape[0]
+    top = routes.shape[1]
+    capacity = max(2, 2 * tok_dev * top // sp_count)
+    direct = (
+        tp_count == 4
+        and sp_count % 2 == 0
+        and capacity % 16 == 0
+        and 2 * tok_dev % 128 == 0
+        and tok_sp % (2 * GRID_W) == 0
+        and heads_dev % 2 == 0
+        and 2 * heads_dev <= group
+        and tok_sp == tp_count * tok_dev
+    )
+    if direct:
+        mixed, normed, notes = attend(
+            sp_count,
+            queries,
+            keys,
+            values,
+            query_gain,
+            key_gain,
+            residual,
+            expert_norm_scale,
+            jnp.tile(routes.T, (1, 2)),
+            jnp.tile(route_weights.T, (1, 2)),
+            out_proj,
+        )
+        summed = moe(sp_count, normed, notes, capacity, w_gate, w_up, w_down)
+        return (mixed.astype(jnp.float32) + summed).astype(jnp.bfloat16)
     position = sp_index * tok_sp + jnp.arange(tok_sp, dtype=jnp.int32)
     q_rot = prepare(queries, query_gain, position)
     shared_value_head = tp_index * heads_dev // group
@@ -786,22 +961,8 @@
         .transpose(1, 0, 2)
         .reshape(1, heads_dev * tok_sp, head_size)
     )
-    tok_dev = residual.shape[0]
-    top = routes.shape[1]
-    capacity = max(2, 2 * tok_dev * top // sp_count)
-    direct = (
-        tp_count == 4 and sp_count % 2 == 0 and capacity % 16 == 0 and 2 * tok_dev % 128 == 0
-    )
-    named = routes[:, :, None] == jnp.arange(sp_count, dtype=jnp.int32)[None, None, :]
-    if direct:
-        taken = jnp.any(named, axis=1).astype(jnp.int32)
-        place = jnp.where(taken > 0, jnp.cumsum(taken, axis=0) - 1, -1).astype(jnp.float32)
-        load = jnp.sum(jnp.where(named, route_weights[:, :, None], 0.0), axis=1)
-        notes = jnp.concatenate([place, load], axis=0).T
-        key_piece, value_piece, notes = gather_rows(sp_count, own_keys, own_values, notes)
-    else:
-        key_piece = lax.all_gather(own_keys, "sp", axis=0, tiled=True)
-        value_piece = lax.all_gather(own_values, "sp", axis=0, tiled=True)
+    key_piece = lax.all_gather(own_keys, "sp", axis=0, tiled=True)
+    value_piece = lax.all_gather(own_values, "sp", axis=0, tiled=True)
     run_max, run_sum, run_acc = absorb(
         start_state(1, heads_dev * tok_sp, head_size),
         query_matrix,
@@ -815,17 +976,14 @@
         .transpose(1, 0, 2)
         .reshape(tok_sp, heads_dev * head_size)
     )
-    if direct:
-        projected, notes = project(attn, out_proj, notes, tok_dev)
-    else:
-        columns = jnp.dot(
-            lax.all_gather(attn, "tp", axis=1, tiled=True),
-            out_proj,
-            preferred_element_type=jnp.float32,
-        )
-        projected = lax.all_to_all(
-            columns.astype(jnp.bfloat16), "tp", split_axis=0, concat_axis=1, tiled=True
-        )
+    columns = jnp.dot(
+        lax.all_gather(attn, "tp", axis=1, tiled=True),
+        out_proj,
+        preferred_element_type=jnp.float32,
+    )
+    projected = lax.all_to_all(
+        columns.astype(jnp.bfloat16), "tp", split_axis=0, concat_axis=1, tiled=True
+    )
     mixed_float_output = residual.astype(jnp.float32) + projected.astype(jnp.float32)
     mixed = mixed_float_output.astype(jnp.bfloat16)
     mixed_float_output = mixed.astype(jnp.float32)
@@ -834,25 +992,6 @@
         * lax.rsqrt(jnp.mean(mixed_float_output * mixed_float_output, axis=-1, keepdims=True) + EPS)
         * expert_norm_scale
     ).astype(jnp.bfloat16)
-    if direct:
-        notes = notes.reshape(tp_count, sp_count, sp_count, 2, tok_dev)
-        notes = lax.dynamic_index_in_dim(notes, sp_index, 2, keepdims=False)
-        notes = notes.transpose(1, 2, 0, 3)
-        base = capacity * jnp.arange(tp_count, dtype=jnp.float32)[:, None]
-        spots = jnp.where(notes[:, 0] >= 0, notes[:, 0] + base, -1.0).astype(jnp.int32)
-        coarse = lax.reduce_precision(notes[:, 1], 8, 7)
-        pair = jnp.stack([coarse, notes[:, 1] - coarse], axis=1)
-        summed = moe(
-            sp_count,
-            normed,
-            spots.reshape(sp_count, 1, tp_count * tok_dev),
-            pair.reshape(sp_count, 2, tp_count * tok_dev),
-            capacity,
-            w_gate,
-            w_up,
-            w_down,
-        )
-        return (mixed_float_output + summed).astype(jnp.bfloat16)
     flat_routes = routes.reshape(-1)
     one_hot = (flat_routes[:, None] == jnp.arange(sp_count, dtype=jnp.int32)[None, :]).astype(
         jnp.int32

time: 153 us -> 131 us (0.86)
  other arithmetic: 15.5 us -> 1.79 us
  matrix products: 3.64 us -> 0 us
  local copies, waits for them, and re-layouts: 4.58 us -> 2.65 us
    reduce_sum x5 -> x0, other arithmetic: 5.01 us -> none  [the longest x1 2.11 us: step(): jnp.sum(weight_tensors.astype(jnp.float32), axis=-1)]
    dot_general x2 -> x0, matrix products: 3.64 us -> none  [the longest x1 2.37 us: step(): jnp.einsum('hxt,ght->hxg', query_matrix, key_tile_rows, preferred_element...]
    convert_element_type x7 -> x1, other arithmetic: 4.99 us -> 1.79 us  [local(): return (mixed.astype(jnp.float32) + summed).astype(jnp.bfloat16)]
    another operation x3 -> x4, local copies, waits for them, and re-layouts: 0.24 us -> 2.65 us  [the longest x2 1.32 us: local(): jnp.tile(routes.T, (1, 2))]
    another operation x4 -> x0, other arithmetic: 2 us -> none
    unnamed x12 -> x2, local copies, waits for them, and re-layouts: 1.85 us -> 0.01 us
    mul x4 -> x0, other arithmetic: 1.74 us -> none  [the longest x2 1.72 us: prepare(): values_f * lax.rsqrt(jnp.mean(values_f * values_f, axis=-1, keepdims=True...]
    pallas_call x2 -> x1, Pallas kernels: 41.8 us -> 40 us  [attend(): pl.pallas_call(functools.partial(attend_kernel, n), out_shape=(jax.ShapeD...]
where the time goes in v3:
time: 131 us
  Pallas kernels  127 us (97%)
  local copies, waits for them, and re-layouts  2.65 us (2%)
  other arithmetic  1.79 us (1%)
    pallas_call x1, Pallas kernels, moe(): pl.pallas_call(functools.partial(moe_kernel, n, cuts), out_shape=jax.Shap...  86.5 us
    pallas_call x1, Pallas kernels, attend(): pl.pallas_call(functools.partial(attend_kernel, n), out_shape=(jax.ShapeD...  40 us

profile of v3, /device:TPU:0, one launch (start us, length us, event | category | flops | bytes accessed | tf_op | source)
XLA Modules:
  0.0 131.0 jit_solution(2990791660791097068)
XLA Ops:
  0.0 0.7 tile.8
  0.7 0.6 tile.9.name_ref
  1.3 0.7 tile.20
  2.0 0.6 tile.21.share_ref
  2.6 40.0 %attend.1 = (bf16[64,2048]{1,0:T(8,128)(2,1)}, bf16[64,2048]{1,0:T(8,128)(2,1)}, f32[4,8,8,128]{3,2,1,0:T(8,128)}) custom-call(bf16[256,512]{1,0:T(8,128)(2,1)} %q_ref.1, bf16[256,256]{1,0:T(8,128)(2,1)} %k_ref.1, bf16[256,256]{1,0:T(8,128)(2,1)} %v_ref.1, f32[1,128]{1,0:T(1,128)} %bitcast.8, f32[1,128]{1,0:T(1,128)} %bitcast.9, ...), custom_call_target="tpu_custom_call" | custom-call | tf_op jit(solution)/shard_map/attend/pallas_call | solution.py:398
  42.7 0.0 copy-start
  42.7 86.5 %moe.1 = f32[64,2048]{1,0:T(8,128)} custom-call(bf16[64,2048]{1,0:T(8,128)(2,1)} %get-tuple-element.9.x_ref, f32[4,8,8,128]{3,2,1,0:T(8,128)} %get-tuple-element.10.note_ref, bf16[1,2048,1024]{2,1,0:T(8,128)(2,1)} %wg_ref.1, bf16[1,2048,1024]{2,1,0:T(8,128)(2,1)} %wu_ref.1, bf16[1,1024,2048]{2,1,0:T(8,128)(2,1)} %wd_ref.1), custom_call_target="tpu_custom_call" | custom-call | tf_op jit(solution)/shard_map/moe/pallas_call | solution.py:840
  129.2 0.0 copy-done
  129.2 1.8 %add_convert_fusion = bf16[64,2048]{1,0:T(8,128)(2,1)} fusion(f32[64,2048]{1,0:T(8,128)} %moe.1, bf16[64,2048]{1,0:T(8,128)(2,1)S(1)} %copy-done), kind=kLoop, calls=%fused_computation | loop fusion | flops 393216 | bytes 1048576 | tf_op jit(solution)/shard_map/convert_element_type | solution.py:949
Async XLA Ops:
  42.7 86.5 %copy-start = (bf16[64,2048]{1,0:T(8,128)(2,1)S(1)}, bf16[64,2048]{1,0:T(8,128)(2,1)}, u32[]{:S(2)}) copy-start(bf16[64,2048]{1,0:T(8,128)(2,1)} %get-tuple-element.8) | copy-start | bytes 786436

commit v4 on v3

--- a/solution.py
+++ b/solution.py
@@ -177,13 +177,18 @@
         kv[chip, core, side, 1, place] = v_ref[span, at]
     lanes = lax.broadcasted_iota(jnp.int32, (n, 2 * share), 1)
     expert = lax.broadcasted_iota(jnp.int32, (n, 2 * share), 0)
-    first_one, second_one = name_ref[0:1] == expert, name_ref[1:2] == expert
+    def as_row(ref, i):
+        column = jnp.broadcast_to(ref[:, i : i + 1].astype(jnp.float32), (share, 2 * share))
+        return jnp.transpose(jnp.concatenate([column, column], axis=0))[:n]
+
+    first_one, second_one = [as_row(name_ref, i).astype(jnp.int32) == expert for i in range(2)]
     taken = jnp.where((first_one | second_one) & (lanes < share), 1.0, 0.0)
     before = lax.broadcasted_iota(jnp.int32, (2 * share, 2 * share), 0)
     after = lax.broadcasted_iota(jnp.int32, (2 * share, 2 * share), 1)
     ladder = jnp.where(before < after, 1.0, 0.0).astype(jnp.bfloat16)
     slot = jnp.dot(taken.astype(jnp.bfloat16), ladder, preferred_element_type=jnp.float32)
-    weight = jnp.where(first_one, share_ref[0:1], 0.0) + jnp.where(second_one, share_ref[1:2], 0.0)
+    weight = jnp.where(first_one, as_row(share_ref, 0), 0.0)
+    weight += jnp.where(second_one, as_row(share_ref, 1), 0.0)
     sheet[me] = jnp.where(lanes < share, jnp.where(taken > 0, slot, -1.0), weight)
 
     pl.semaphore_wait(barrier, n + 2)
@@ -451,8 +456,9 @@
 
 def visit(chip, chips, step):
     near = jnp.minimum(chip, chips - 1 - chip)
-    swing = chip + ((step + 1) // 2) * (1 - 2 * lax.rem(step, 2))
     up = chip < chips - 1 - chip
+    swing = (step + 1) // 2 * (2 * lax.rem(step, 2) - 1)
+    swing = jnp.where(up, chip + swing, chip - swing)
     tail = jnp.where(up, chip + (step - near), chip - (step - near))
     return jnp.where(step <= 2 * near, swing, tail)
 
@@ -464,8 +470,8 @@
 def moe_kernel(
     n, cuts, x_ref, note_ref, wg_ref, wu_ref, wd_ref, out_ref,
     tok, wg, wu, wd, picked, hid, wsel, held, own, give, take,
-    low, high, from_x, from_y, to_y, to_x, last_y, last_x, acc, zsend, zrecv,
-    load, zs, zr, sq_s, sq_r, pd_s, pd_r, tk_s, tk_r, hop_s, hop_r, hz_s, hz_r,
+    low, high, from_x, from_y, to_y, to_x, last_y, last_x, acc, zsend, zrecv, zmid,
+    load, zs, zr, sq_s, sq_r, pd_s, pd_r, tk_s, tk_r, hop_s, hop_r, hz_s, hz_r, mid_r,
 ):
     me = lax.axis_index("sp")
     chips = n // 2
@@ -533,7 +539,7 @@
             (block.at[across, upper], block.at[across, upper], along),
             (block.at[along, lower], block.at[along, lower], across),
         )[way]
-        return remote(src, dst, sq_s.at[p, h, way], sq_r.at[p, h, way], {"tp": where})
+        return remote(src, dst, sq_s.at[way], sq_r.at[p, h, way], {"tp": where})
 
     def arrive(p, h, way):
         block = tok.at[p, core, h]
@@ -543,16 +549,16 @@
             block.at[corner, upper],
             block.at[corner, lower],
         )[way]
-        remote(dst, dst, sq_s.at[p, h, way], sq_r.at[p, h, way], {"tp": across}).wait_recv()
+        remote(dst, dst, sq_s.at[way], sq_r.at[p, h, way], {"tp": across}).wait_recv()
 
     def hand(p, h, t, first=False):
         block = tok.at[p, core, h, t]
         src = own_half(h) if first else block
-        return remote(src, block, pd_s.at[p, h, t], pd_r.at[p, h, t], partner)
+        return remote(src, block, pd_s.at[0], pd_r.at[p, h, t], partner)
 
     def handed(p, h, t):
         block = tok.at[p, other, h, t]
-        remote(block, block, pd_s.at[p, h, t], pd_r.at[p, h, t], partner).wait_recv()
+        remote(block, block, pd_s.at[0], pd_r.at[p, h, t], partner).wait_recv()
 
     for h in range(2):
         pass_on(chip, h, 0, True).start()
@@ -578,50 +584,59 @@
         arrive(p, h, 3)
         hand(p, h, corner).start()
 
-    def expert(p):
+    def wait_rows(p):
         for h in range(2):
             for t in range(4):
                 handed(p, h, t)
-        for side in range(2):
-            tiles = [note_ref[t, 2 * p + side] for t in range(4)]
-            lane = lax.broadcasted_iota(jnp.int32, (n, 2 * share), 1)
-            chosen = lax.broadcasted_iota(jnp.int32, (n, 2 * share), 0) == me
-
-            def across_two(even, odd, swap_even):
-                moved = pltpu.roll(even if swap_even else odd, share, 1)
-                return jnp.where(lane < share, moved, odd) if swap_even else jnp.where(
-                    lane < share, even, moved
-                )
-
-            def row_of(swap_even):
-                parts_two = [across_two(tiles[t], tiles[t + 1], swap_even) for t in (0, 2)]
-                picks = [
-                    jnp.sum(jnp.where(chosen, v, 0.0), axis=0, keepdims=True) for v in parts_two
-                ]
-                return jnp.concatenate(picks, axis=1)
-
-            spot = row_of(False)
-            base = lax.broadcasted_iota(jnp.int32, (1, group), 1) // share * (slots // 4)
-            spot = jnp.where(spot >= 0, spot.astype(jnp.int32) + base, -1)
-            weight = row_of(True)
-            coarse = weight.astype(jnp.bfloat16).astype(jnp.float32)
-            parts = (coarse, weight - coarse)
-            hit = lax.broadcasted_iota(jnp.int32, (slots, group), 0) == spot
-            pick = jnp.where(hit, 1.0, 0.0).astype(tok.dtype)
-            for i in range(2):
-                turned = jnp.transpose(jnp.where(hit, parts[i], 0.0))
-                wsel[p, side, :, i * slots : (i + 1) * slots] = turned.astype(wsel.dtype)
-            for h in range(2):
-                block = tok[p, side, h].reshape(group, depth // 2)
-                rows = jnp.dot(pick, block, preferred_element_type=jnp.float32)
-                picked[side * slots : (side + 1) * slots, cols(h)] = rows.astype(picked.dtype)
+
+    def pick_rows(p, side):
+        tiles = [note_ref[t, 2 * p + side] for t in range(4)]
+        lane = lax.broadcasted_iota(jnp.int32, (n, 2 * share), 1)
+        chosen = lax.broadcasted_iota(jnp.int32, (n, 2 * share), 0) == me
+
+        def across_two(even, odd, swap_even):
+            moved = pltpu.roll(even if swap_even else odd, share, 1)
+            return jnp.where(lane < share, moved, odd) if swap_even else jnp.where(
+                lane < share, even, moved
+            )
+
+        def row_of(swap_even):
+            parts_two = [across_two(tiles[t], tiles[t + 1], swap_even) for t in (0, 2)]
+            picks = [
+                jnp.sum(jnp.where(chosen, v, 0.0), axis=0, keepdims=True) for v in parts_two
+            ]
+            return jnp.concatenate(picks, axis=1)
+
+        spot = row_of(False)
+        base = lax.broadcasted_iota(jnp.int32, (1, group), 1) // share * (slots // 4)
+        spot = jnp.where(spot >= 0, spot.astype(jnp.int32) + base, -1)
+        weight = row_of(True)
+        coarse = weight.astype(jnp.bfloat16).astype(jnp.float32)
+        parts = (coarse, weight - coarse)
+        hit = lax.broadcasted_iota(jnp.int32, (slots, group), 0) == spot
+        pick = jnp.where(hit, 1.0, 0.0).astype(tok.dtype)
+        for i in range(2):
+            turned = jnp.transpose(jnp.where(hit, parts[i], 0.0))
+            wsel[p, side, :, i * slots : (i + 1) * slots] = turned.astype(wsel.dtype)
+        for h in range(2):
+            block = tok[p, side, h].reshape(group, depth // 2)
+            rows = jnp.dot(pick, block, preferred_element_type=jnp.float32)
+            picked[side * slots : (side + 1) * slots, cols(h)] = rows.astype(picked.dtype)
+
+    def activate(p, u):
+        some = pl.ds(pl.multiple_of(u * 512, 512), 512)
+        gate = jnp.dot(picked[...], wg[:, some], preferred_element_type=jnp.float32)
+        rise = jnp.dot(picked[...], wu[:, some], preferred_element_type=jnp.float32)
+        hid[p, :, some] = (jax.nn.silu(gate) * rise).astype(hid.dtype)
+
+    def expert(p):
+        wait_rows(p)
+        pick_rows(p, 0)
+        pick_rows(p, 1)
 
         @pl.loop(0, units // 512)
         def _(u):
-            some = pl.ds(pl.multiple_of(u * 512, 512), 512)
-            gate = jnp.dot(picked[...], wg[:, some], preferred_element_type=jnp.float32)
-            rise = jnp.dot(picked[...], wu[:, some], preferred_element_type=jnp.float32)
-            hid[p, :, some] = (jax.nn.silu(gate) * rise).astype(hid.dtype)
+            activate(p, u)
 
     def forward(u):
         p, h = part(u)
@@ -689,16 +704,21 @@
 
         @pl.when((u == 4) | ((u > 4) & (lax.rem(u, 2) == 1)))
         def _():
-            j = (u - 3) // 2
-            finish(2 * j)
-            finish(2 * j + 1)
-            expert(visit(chip, chips, j))
+            expert(visit(chip, chips, (u - 3) // 2))
+
+        @pl.when((u >= 2) & (lax.rem(u, 2) == 0))
+        def _():
+            finish(u - 2)
+
+            @pl.when(u < last - 1)
+            def _():
+                finish(u - 1)
 
     def plane_of(k):
         return visit(chip, chips, lax.rem(k // cuts + 1, chips))
 
     def swap(k):
-        return remote(give.at[k], take.at[k], tk_s.at[k], tk_r.at[k], partner)
+        return remote(give.at[k], take.at[k], tk_s.at[0], tk_r.at[k], partner)
 
     def hop(k, way):
         src, dst, where = (
@@ -707,42 +727,95 @@
             (to_y.at[k], last_y.at[k], along),
             (to_x.at[k], last_x.at[k], across),
         )[way]
-        return remote(src, dst, hop_s.at[k, way], hop_r.at[k, way], {"tp": where})
+        return remote(src, dst, hop_s.at[way], hop_r.at[k, way], {"tp": where})
 
     def home(k):
         p, q = plane_of(k), lax.rem(k, cuts)
         return remote(
-            zsend.at[k], zrecv.at[chip, q], hz_s.at[k], hz_r.at[chip, q], {"sp": 2 * p + core}
+            zsend.at[k], zrecv.at[chip, q], hz_s.at[0], hz_r.at[chip, q], {"sp": 2 * p + core}
+        )
+
+    is_end = (chip == 0) | (chip == chips - 1)
+
+    def lend(k):
+        to = chip + jnp.where(chip == 0, 1, -1)
+        return remote(
+            zsend.at[k], zmid.at[lax.rem(k, cuts)], hz_s.at[0], mid_r.at[lax.rem(k, cuts)],
+            {"sp": 2 * to + core},
         )
 
     def homed(p, q):
         return remote(zsend.at[0], zrecv.at[p, q], hz_s.at[0], hz_r.at[p, q], partner)
 
-    @pl.loop(0, steps + 5)
+    def settle(k):
+        swap(k).wait_recv()
+        total = own[lax.rem(k, 3)] + wide(take[k])
+        cast = total.astype(low.dtype).reshape(4, share, width)
+        for t in range(4):
+            low[k, t % 2, t // 2] = cast[t, :, :half]
+            high[k, t // 2, t % 2] = cast[t, :, half:]
+        hop(k, 0).start()
+        hop(k, 1).start()
+
+    @pl.loop(0, steps + 6)
     def _(step):
-        @pl.when((step >= 1) & (step <= steps))
-        def _(k=step - 1):
-            swap(k).wait_recv()
-            total = own[lax.rem(k, 2)] + wide(take[k])
-            cast = total.astype(low.dtype).reshape(4, share, width)
-            for t in range(4):
-                low[k, t % 2, t // 2] = cast[t, :, :half]
-                high[k, t // 2, t % 2] = cast[t, :, half:]
-            hop(k, 0).start()
-            hop(k, 1).start()
+        @pl.when((step >= 2) & (step < steps + 2))
+        def _():
+            settle(step - 2)
+
+        @pl.when((step >= 4) & (step < steps + 4))
+        def _(k=step - 4):
+            hop(k, 0).wait_recv()
+            to_y[k] = (wide(low[k, x, 1 - y]) + wide(from_x[k, 1 - y])).astype(to_y.dtype)
+            hop(k, 2).start()
+            hop(k, 1).wait_recv()
+            to_x[k] = (wide(high[k, y, 1 - x]) + wide(from_y[k, 1 - x])).astype(to_x.dtype)
+            hop(k, 3).start()
+
+        @pl.when(step >= 6)
+        def _(k=step - 6):
+            hop(k, 2).wait_recv()
+            left = wide(low[k, x, y]) + wide(from_x[k, y]) + wide(last_y[k])
+            hop(k, 3).wait_recv()
+            right = wide(high[k, y, x]) + wide(from_y[k, x]) + wide(last_x[k])
+
+            far = (k >= steps - 2 * cuts) & (k < steps - cuts)
+
+            @pl.when((k < steps - cuts) & jnp.logical_not(far & jnp.logical_not(is_end)))
+            def _():
+                zsend[k, :, :half] = left.astype(zsend.dtype)
+                zsend[k, :, half:] = right.astype(zsend.dtype)
+
+                @pl.when(far)
+                def _():
+                    lend(k).start()
+
+                @pl.when(jnp.logical_not(far))
+                def _():
+                    home(k).start()
+
+            @pl.when(far & jnp.logical_not(is_end))
+            def _():
+                lend(k).wait_recv()
+                more = wide(zmid[lax.rem(k, cuts)])
+                zsend[k, :, :half] = (left + more[:, :half]).astype(zsend.dtype)
+                zsend[k, :, half:] = (right + more[:, half:]).astype(zsend.dtype)
+                home(k).start()
+
+            @pl.when(k >= steps - cuts)
+            def _():
+                acc[lax.rem(k, cuts), :, :half] = left
+                acc[lax.rem(k, cuts), :, half:] = right
 
         @pl.when(step < steps)
         def _(k=step):
-            @pl.when(k == cuts // 2)
+            third, fourth = visit(chip, chips, chips - 2), visit(chip, chips, chips - 1)
+
+            @pl.when(k == cuts)
             def _():
-                forward(last)
-
-            @pl.when((k == cuts) | (k == 2 * cuts))
-            def _():
-                late = jnp.where(k == cuts, 0, 1)
-                finish(last - 3 + 2 * late)
-                finish(last - 2 + 2 * late)
-                expert(visit(chip, chips, chips - 2 + late))
+                @pl.loop(0, units // 512)
+                def _(u):
+                    activate(third, u)
 
             p, q = plane_of(k), lax.rem(k, cuts)
             out = jnp.dot(hid[p], wd[q], preferred_element_type=jnp.float32).astype(held.dtype)
@@ -756,51 +829,48 @@
 
             give[k] = spread(other).astype(give.dtype)
             swap(k).start()
-            own[lax.rem(k, 2)] = spread(core)
-
-        @pl.when((step >= 3) & (step < steps + 3))
-        def _(k=step - 3):
-            hop(k, 0).wait_recv()
-            to_y[k] = (wide(low[k, x, 1 - y]) + wide(from_x[k, 1 - y])).astype(to_y.dtype)
-            hop(k, 2).start()
-            hop(k, 1).wait_recv()
-            to_x[k] = (wide(high[k, y, 1 - x]) + wide(from_y[k, 1 - x])).astype(to_x.dtype)
-            hop(k, 3).start()
-
-        @pl.when(step >= 5)
-        def _(k=step - 5):
-            hop(k, 2).wait_recv()
-            left = wide(low[k, x, y]) + wide(from_x[k, y]) + wide(last_y[k])
-            hop(k, 3).wait_recv()
-            right = wide(high[k, y, x]) + wide(from_y[k, x]) + wide(last_x[k])
-
-            @pl.when(k < steps - cuts)
+            own[lax.rem(k, 3)] = spread(core)
+
+            @pl.when(k == cuts // 2)
             def _():
-                zsend[k, :, :half] = left.astype(zsend.dtype)
-                zsend[k, :, half:] = right.astype(zsend.dtype)
-                home(k).start()
-
-            @pl.when(k >= steps - cuts)
+                forward(last)
+                finish(last - 2)
+
+            @pl.when(k == cuts)
             def _():
-                acc[lax.rem(k, cuts), :, :half] = left
-                acc[lax.rem(k, cuts), :, half:] = right
+                finish(last - 1)
+                finish(last)
+
+            @pl.when((k == cuts - 1) | (k == cuts + 1))
+            def _():
+                p = jnp.where(k < cuts, third, fourth)
+                wait_rows(p)
+                pick_rows(p, 0)
+                pick_rows(p, 1)
+
+            each = units // 1024
+
+            @pl.when((k >= cuts + 2) & (k < cuts + 4))
+            def _():
+                @pl.loop(0, each)
+                def _(u):
+                    activate(fourth, (k - cuts - 2) * each + u)
 
     @pl.loop(0, cuts)
     def _(q):
-        total = acc[q]
         for d in range(1, chips):
             p = lax.rem(chip + d, chips)
-            homed(p, q).wait_recv()
-            total += wide(zrecv[p, q])
-        out_ref[:, column(q)] = total
+
+            @pl.when(jnp.logical_not(is_end & (p == chips - 1 - chip)))
+            def _():
+                homed(p, q).wait_recv()
+                acc[q] += wide(zrecv[p, q])
+
+        out_ref[:, column(q)] = acc[q]
 
     @pl.loop(0, 2 * chips)
     def _(u):
         p, h = u // 2, lax.rem(u, 2)
-        for way in range(4):
-            pass_on(p, h, way).wait_send()
-            hand(p, h, way).wait_send()
-
         @pl.when((p <= chip) & has_right)
         def _():
             along_z(p, h, 0).wait_send()
@@ -809,15 +879,17 @@
         def _():
             along_z(p, h, 1).wait_send()
 
-    @pl.loop(0, steps)
-    def _(k):
-        swap(k).wait_send()
-        for way in range(4):
-            hop(k, way).wait_send()
-
-        @pl.when(k < steps - cuts)
-        def _():
-            home(k).wait_send()
+    def all_left(ref, sem):
+        remote(ref, ref, sem, sem, partner).wait_send()
+
+    whole = tok.at[:, 0, :, 0]
+    for way, ref in enumerate((whole, whole, whole.at[:, :, upper], whole.at[:, :, lower])):
+        all_left(ref, sq_s.at[way])
+    all_left(tok.at[:, 0], pd_s.at[0])
+    all_left(give, tk_s.at[0])
+    for way, ref in enumerate((from_x, from_y, to_y, to_x)):
+        all_left(ref, hop_s.at[way])
+    all_left(zsend, hz_s.at[0])
 
 
 def moe(n, normed, notes, capacity, w_gate, w_up, w_down, cuts=4):
@@ -851,7 +923,7 @@
             room(chips, 2 * slots, units),
             room(chips, 2, group, 2 * slots),
             room(2, 2 * slots, width),
-            exact(2, group, width),
+            exact(3, group, width),
             room(steps, group, width),
             room(steps, group, width),
             room(steps, 2, 2, share, half),
@@ -865,19 +937,21 @@
             exact(cuts, share, width),
             room(steps - cuts, share, width),
             room(chips, cuts, share, width),
+            room(cuts, share, width),
             dma((2 + cuts,)),
             dma((chips, 2, 2)),
             dma((chips, 2)),
+            dma((4,)),
             dma((chips, 2, 4)),
+            dma((1,)),
             dma((chips, 2, 4)),
-            dma((chips, 2, 4)),
-            dma((chips, 2, 4)),
+            dma((1,)),
             dma((steps,)),
-            dma((steps,)),
+            dma((4,)),
             dma((steps, 4)),
-            dma((steps, 4)),
-            dma((steps,)),
+            dma((1,)),
             dma((chips, cuts)),
+            dma((cuts,)),
         ],
         compiler_params=params(2),
         name="moe",
@@ -923,6 +997,7 @@
     capacity = max(2, 2 * tok_dev * top // sp_count)
     direct = (
         tp_count == 4
+        and sp_count // 2 == 4
         and sp_count % 2 == 0
         and capacity % 16 == 0
         and 2 * tok_dev % 128 == 0
@@ -941,8 +1016,8 @@
             key_gain,
             residual,
             expert_norm_scale,
-            jnp.tile(routes.T, (1, 2)),
-            jnp.tile(route_weights.T, (1, 2)),
+            routes,
+            route_weights,
             out_proj,
         )
         summed = moe(sp_count, normed, notes, capacity, w_gate, w_up, w_down)

time: 131 us -> 124 us (0.947)
  Pallas kernels: 127 us -> 119 us
    pallas_call x1, Pallas kernels: 86.5 us -> 79.1 us  [moe(): pl.pallas_call(functools.partial(moe_kernel, n, cuts), out_shape=jax.Shap...]
    unnamed x2 -> x4, local copies, waits for them, and re-layouts: 0.01 us -> 2.75 us
    another operation x4 -> x0, local copies, waits for them, and re-layouts: 2.65 us -> none  [the longest x2 1.32 us: local(): jnp.tile(routes.T, (1, 2))]
where the time goes in v4:
time: 124 us
  Pallas kernels  119 us (96%)
  local copies, waits for them, and re-layouts  2.75 us (2%)
  other arithmetic  1.79 us (1%)
    pallas_call x1, Pallas kernels, moe(): pl.pallas_call(functools.partial(moe_kernel, n, cuts), out_shape=jax.Shap...  79.1 us
    pallas_call x1, Pallas kernels, attend(): pl.pallas_call(functools.partial(attend_kernel, n), out_shape=(jax.ShapeD...  40 us
    unnamed x4, local copies, waits for them, and re-layouts  2.75 us

profile of v4, /device:TPU:0, one launch (start us, length us, event | category | flops | bytes accessed | tf_op | source)
XLA Modules:
  0.0 123.7 jit_solution(624012388701373308)
XLA Ops:
  0.0 1.4 %copy.16.name_ref = s32[64,2]{1,0:T(8,128)} copy(s32[64,2]{0,1:T(2,128)} %param.23) | data formatting | bytes 1024 | tf_op args[8]
  1.4 1.4 %copy.17.share_ref = f32[64,2]{1,0:T(8,128)} copy(f32[64,2]{0,1:T(2,128)} %param.24) | data formatting | bytes 1024 | tf_op args[9]
  2.8 40.0 %attend.1 = (bf16[64,2048]{1,0:T(8,128)(2,1)}, bf16[64,2048]{1,0:T(8,128)(2,1)}, f32[4,8,8,128]{3,2,1,0:T(8,128)}) custom-call(bf16[256,512]{1,0:T(8,128)(2,1)} %q_ref.1, bf16[256,256]{1,0:T(8,128)(2,1)} %k_ref.1, bf16[256,256]{1,0:T(8,128)(2,1)} %v_ref.1, f32[1,128]{1,0:T(1,128)} %bitcast.4, f32[1,128]{1,0:T(1,128)} %bitcast.5, ...), custom_call_target="tpu_custom_call" | custom-call | tf_op jit(solution)/shard_map/attend/pallas_call | solution.py:403
  42.8 0.0 copy-start
  42.8 79.1 %moe.1 = f32[64,2048]{1,0:T(8,128)} custom-call(bf16[64,2048]{1,0:T(8,128)(2,1)} %get-tuple-element.9.x_ref, f32[4,8,8,128]{3,2,1,0:T(8,128)} %get-tuple-element.10.note_ref, bf16[1,2048,1024]{2,1,0:T(8,128)(2,1)} %wg_ref.1, bf16[1,2048,1024]{2,1,0:T(8,128)(2,1)} %wu_ref.1, bf16[1,1024,2048]{2,1,0:T(8,128)(2,1)} %wd_ref.1), custom_call_target="tpu_custom_call" | custom-call | tf_op jit(solution)/shard_map/moe/pallas_call | solution.py:912
  121.9 0.0 copy-done
  121.9 1.8 %add_convert_fusion = bf16[64,2048]{1,0:T(8,128)(2,1)} fusion(f32[64,2048]{1,0:T(8,128)} %moe.1, bf16[64,2048]{1,0:T(8,128)(2,1)S(1)} %copy-done), kind=kLoop, calls=%fused_computation | loop fusion | flops 393216 | bytes 1048576 | tf_op jit(solution)/shard_map/convert_element_type | solution.py:1024
Async XLA Ops:
  42.8 79.1 %copy-start = (bf16[64,2048]{1,0:T(8,128)(2,1)S(1)}, bf16[64,2048]{1,0:T(8,128)(2,1)}, u32[]{:S(2)}) copy-start(bf16[64,2048]{1,0:T(8,128)(2,1)} %get-tuple-element.8) | copy-start | bytes 786436

commit v5 on v4

v5 whole, which is shorter than its diff:
```python
import functools

import jax
import jax.numpy as jnp
import numpy as np
from jax import lax
from jax.experimental import pallas as pl
from jax.experimental.pallas import tpu as pltpu
from jax.sharding import PartitionSpec as P

GRID_W = 64


EPS = 1e-06
ROPE_BASE = 10000.0
NEG_START = -1e30


def rotate(field, position):
    half = field.shape[-1] // 2
    quarter = half // 2
    freqs = ROPE_BASE ** (-jnp.arange(quarter, dtype=jnp.float32) / quarter)
    grid_row = (position // GRID_W).astype(jnp.float32)
    grid_col = (position % GRID_W).astype(jnp.float32)

    def turn_half(part, coord):
        angle = coord[:, None] * freqs[None, :]
        cosine = jnp.cos(angle)[:, None, :]
        sine = jnp.sin(angle)[:, None, :]
        first, second = (part[..., :quarter], part[..., quarter:])
        return jnp.concatenate(
            [first * cosine - second * sine, second * cosine + first * sine], axis=-1
        )

    return jnp.concatenate(
        [turn_half(field[..., :half], grid_row), turn_half(field[..., half:], grid_col)], axis=-1
    )


def prepare(field, gain, position):
    count = field.shape[0]
    width = gain.shape[0]
    heads_here = field.shape[1] // width
    values_f = field.reshape(count, heads_here, width).astype(jnp.float32)
    scaled = (
        values_f * lax.rsqrt(jnp.mean(values_f * values_f, axis=-1, keepdims=True) + EPS) * gain
    )
    return rotate(scaled, position).reshape(count, heads_here * width).astype(jnp.bfloat16)


def absorb(carry, query_matrix, key_rows, value_rows, scale):
    count = key_rows.shape[0]
    width = 2048 if count > 2048 and count % 2048 == 0 else count
    key_blocks = key_rows.reshape(count // width, width, key_rows.shape[1], key_rows.shape[2])
    value_blocks = value_rows.reshape(
        count // width, width, value_rows.shape[1], value_rows.shape[2]
    )

    def step(state, block):
        run_max, run_sum, run_acc = state
        key_tile_rows, value_tile_rows = block
        scores = (
            jnp.einsum(
                "hxt,ght->hxg", query_matrix, key_tile_rows, preferred_element_type=jnp.float32
            )
            * scale
        )
        new_max = jnp.maximum(run_max, jnp.max(scores, axis=-1))
        weight_tensors = jnp.exp(scores - new_max[..., None]).astype(jnp.bfloat16)
        factor = jnp.exp(run_max - new_max)
        run_sum = run_sum * factor + jnp.sum(weight_tensors.astype(jnp.float32), axis=-1)
        run_acc = run_acc * factor[..., None] + jnp.einsum(
            "zij,jzu->ziu", weight_tensors, value_tile_rows, preferred_element_type=jnp.float32
        )
        return ((new_max, run_sum, run_acc), None)

    result, unused = lax.scan(step, carry, (key_blocks, value_blocks))
    return result


MESH = pl.DeviceIdType.MESH
VMEM_LIMIT = 60 * 1024 * 1024


def greet(partners, count):
    barrier = pltpu.get_barrier_semaphore()
    for where in partners:
        pl.semaphore_signal(barrier, inc=1, device_id=where, device_id_type=MESH)
    pl.semaphore_wait(barrier, count)


def remote(src, dst, send, recv, where):
    return pltpu.make_async_remote_copy(
        src_ref=src, dst_ref=dst, send_sem=send, recv_sem=recv, device_id=where, device_id_type=MESH
    )


def square():
    mine = lax.axis_index("tp")
    return mine, mine + 1 - 2 * lax.rem(mine, 2), lax.rem(mine + 2, 4), 3 - mine


def in_vmem(count):
    return [pl.BlockSpec(memory_space=pltpu.VMEM)] * count


def params(number):
    return pltpu.CompilerParams(
        collective_id=number, has_side_effects=True, vmem_limit_bytes=VMEM_LIMIT
    )


def turn_tables(width, rows):
    quarter = width // 4
    freqs = ROPE_BASE ** (-np.arange(quarter, dtype=np.float32) / np.float32(quarter))
    zero = np.zeros((max(rows, GRID_W), quarter), np.float32)

    def table(count, blocks):
        angle = np.arange(count, dtype=np.float32)[:, None] * freqs.astype(np.float32)[None, :]
        kinds = {"c": np.cos(angle), "s": np.sin(angle), "m": -np.sin(angle), "0": zero[:count]}
        return np.stack([np.concatenate([kinds[k] for k in b], axis=1) for b in blocks])

    by_col = table(GRID_W, ("00cc", "00m0", "000s"))
    by_row = table(rows, ("cc00", "m000", "0s00"))
    return by_col.astype(np.float32), by_row.astype(np.float32)


def attend_part(
    n, q_ref, k_ref, v_ref, qg_ref, kg_ref, col_ref, row_ref, res_ref, gain_ref, name_ref, share_ref, w_ref,
    mixed_ref, normed_ref, notes_ref, loads,
    w, kv, qs, top, acc, held, total, stage, proj, sheet,
    load, zs, zr, xs, xr, ds, dr, ns, nr, fs, fr, give, take, tell, told, names, shares,
):
    me = lax.axis_index("sp")
    chips = n // 2
    chip, core = me // 2, lax.rem(me, 2)
    other = 1 - core
    partner = {"sp": 2 * chip + other}
    mine, across, along, corner = square()
    x = lax.rem(mine, 2)
    rows, width = q_ref.shape
    size = qg_ref.shape[1]
    heads = width // size
    pairs = heads // 2
    share = rows // 4
    keys_half = rows // 2
    fetch = pltpu.make_async_copy(w_ref, w, load.at[0])
    fetch.start()
    for c in loads:
        c.start()

    barrier = pltpu.get_barrier_semaphore()
    peers = [lax.rem(me + d, n) for d in range(1, n)]
    for p in peers:
        pl.semaphore_signal(barrier, inc=1, device_id={"sp": p}, device_id_type=MESH)
    for p in (across, along, corner):
        pl.semaphore_signal(barrier, inc=1, device_id={"tp": p}, device_id_type=MESH)

    def turned(part, gain_row, g):
        values = part.astype(jnp.float32)
        mean = jnp.mean(values * values, axis=-1, keepdims=True)
        scaled = values * lax.rsqrt(mean + EPS) * gain_row
        grid_row = pl.ds(me * (rows // GRID_W) + g, 1)
        turn = [col_ref[i] + row_ref[i, grid_row] for i in range(3)]
        return (
            scaled * turn[0]
            + pltpu.roll(scaled, size - size // 4, 1) * turn[1]
            + pltpu.roll(scaled, size // 4, 1) * turn[2]
        ).astype(jnp.bfloat16)

    kv_heads = k_ref.shape[1] // size
    kv_head = mine * kv_heads // 4
    at = pl.ds(pl.multiple_of(kv_head * size, size), size)
    for g in range(rows // GRID_W):
        span = pl.ds(g * GRID_W, GRID_W)
        side, low = (g * GRID_W) // keys_half, (g * GRID_W) % keys_half
        place = pl.ds(low, GRID_W)
        kv[chip, core, side, 0, place] = turned(k_ref[span, at], kg_ref[...], g)
        kv[chip, core, side, 1, place] = v_ref[span, at]
    lanes = lax.broadcasted_iota(jnp.int32, (n, 2 * share), 1)
    expert = lax.broadcasted_iota(jnp.int32, (n, 2 * share), 0)
    def as_rows(ref, into):
        into[:, :share] = jnp.broadcast_to(ref[0:1].astype(jnp.float32), (n, share))
        into[:, share:] = jnp.broadcast_to(ref[1:2].astype(jnp.float32), (n, share))
        both = into[...]
        swapped = pltpu.roll(both, share, 1)
        return jnp.where(lanes < share, both, swapped), jnp.where(lanes < share, swapped, both)

    first_one, second_one = [r.astype(jnp.int32) == expert for r in as_rows(name_ref, names)]
    first_part, second_part = as_rows(share_ref, shares)
    taken = jnp.where((first_one | second_one) & (lanes < share), 1.0, 0.0)
    before = lax.broadcasted_iota(jnp.int32, (2 * share, 2 * share), 0)
    after = lax.broadcasted_iota(jnp.int32, (2 * share, 2 * share), 1)
    ladder = jnp.where(before < after, 1.0, 0.0).astype(jnp.bfloat16)
    slot = jnp.dot(taken.astype(jnp.bfloat16), ladder, preferred_element_type=jnp.float32)
    weight = jnp.where(first_one, first_part, 0.0) + jnp.where(second_one, second_part, 0.0)
    sheet[me] = jnp.where(lanes < share, jnp.where(taken > 0, slot, -1.0), weight)

    pl.semaphore_wait(barrier, n + 2)

    def to_plane(p):
        block = kv.at[chip, core, x]
        return remote(block, block, zs.at[p], zr.at[chip], {"sp": 2 * p + core})

    def from_plane(p):
        block = kv.at[p, core, x]
        remote(block, block, zs.at[p], zr.at[p], partner).wait_recv()

    def sideways(p):
        block = kv.at[p, core, x]
        return remote(block, block, xs.at[p], xr.at[p], {"tp": across})

    def from_side(p):
        block = kv.at[p, core, 1 - x]
        remote(block, block, xs.at[p], xr.at[p], partner).wait_recv()

    def hand(p, side):
        block = kv.at[p, core, side]
        return remote(block, block, ds.at[p, side], dr.at[p, side], partner)

    def handed(p, side):
        block = kv.at[p, other, side]
        remote(block, block, ds.at[p, side], dr.at[p, side], partner).wait_recv()

    for j in range(1, chips):

        @pl.when(chip + j < chips)
        def _():
            to_plane(chip + j).start()

        @pl.when(chip - j >= 0)
        def _():
            to_plane(chip - j).start()

    for side in range(2):
        hand(chip, side).start()
    inform = [
        remote(sheet.at[me], sheet.at[me], ns.at[d], nr.at[d], {"sp": p})
        for d, p in enumerate(peers)
    ]
    for c in inform:
        c.start()

    @pl.loop(0, heads)
    def _(h):
        @pl.loop(0, rows // GRID_W)
        def _(g):
            span = pl.ds(pl.multiple_of(g * GRID_W, GRID_W), GRID_W)
            block = q_ref[span, pl.ds(pl.multiple_of(h * size, size), size)]
            qs[h, span] = turned(block, qg_ref[...], g)

        top[h] = jnp.full(top.shape[1:], NEG_START, jnp.float32)
        acc[h] = jnp.zeros(acc.shape[1:], jnp.float32)

    grade = size ** (-0.5) * 1.4426950408889634

    def first(j, way):
        block = held.at[mine, j]
        where = (across, along)[way]
        return remote(block, block, fs.at[j, way], fr.at[j, way], {"tp": where})

    upper, lower = pl.ds(0, rows // 2), pl.ds(rows // 2, rows // 2)

    def second(j, way):
        block = (held.at[across, j, upper], held.at[along, j, lower])[way]
        where = (along, across)[way]
        return remote(block, block, fs.at[j, 2 + way], fr.at[j, 2 + way], {"tp": where})

    def arrive(j, way):
        block = (
            held.at[across, j],
            held.at[along, j],
            held.at[corner, j, upper],
            held.at[corner, j, lower],
        )[way]
        remote(block, block, fs.at[j, way], fr.at[j, way], partner).wait_recv()

    def bring(p):
        from_plane(p)
        sideways(p).start()
        hand(p, x).start()

    def bring_side(p):
        from_side(p)
        hand(p, 1 - x).start()

    @pl.loop(0, chips)
    def _(s):
        p = visit(chip, chips, s)
        for side in range(2):
            handed(p, side)

        @pl.loop(0, pairs)
        def _(j):
            for i in range(2):
                h = 2 * j + i
                keys = kv[p, :, :, 0].reshape(2 * rows, size)
                values = kv[p, :, :, 1].reshape(2 * rows, size)
                scores = lax.dot_general(
                    qs[h], keys, (((1,), (1,)), ((), ())), preferred_element_type=jnp.float32
                )
                old = top[h]
                new = jnp.maximum(old, jnp.max(scores, axis=1, keepdims=True))
                top[h] = new
                weights = jnp.exp2((scores - new[:, :1]) * grade).astype(jnp.bfloat16)
                full = jnp.concatenate([values, jnp.ones_like(values)], axis=1)
                grown = jnp.dot(weights, full, preferred_element_type=jnp.float32)
                factor = jnp.exp2((old - new) * grade)
                acc[h] = acc[h] * jnp.concatenate([factor, factor], axis=1) + grown

            @pl.when(s == chips - 1)
            def _():
                for i in range(2):
                    done = acc[2 * j + i]
                    ratio = done[:, :size] / done[:, size:]
                    held[mine, j, :, i * size : (i + 1) * size] = ratio.astype(held.dtype)
                first(j, 0).start()
                first(j, 1).start()

        @pl.when(s == 0)
        def _():
            bring(visit(chip, chips, 1))

        @pl.when(s + 2 < chips)
        def _():
            bring(visit(chip, chips, s + 2))

        @pl.when(s + 1 < chips)
        def _():
            bring_side(visit(chip, chips, s + 1))

        @pl.when(s == chips - 2)
        def _():
            for c in inform:
                c.wait_recv()
            notes_ref[mine] = sheet[...]
            for i, p in enumerate((corner, across, along)):
                remote(sheet, notes_ref.at[mine], tell.at[i], told.at[i], {"tp": p}).start()

    fetch.wait()

    def term(owner, j):
        start = pl.multiple_of(owner * width + j * 2 * size, 2 * size)
        part = w[pl.ds(start, 2 * size), :]
        total[...] += jnp.dot(held[owner, j], part, preferred_element_type=jnp.float32)

    total[...] = jnp.zeros_like(total)

    @pl.loop(0, pairs)
    def _(j):
        term(mine, j)

    @pl.loop(0, pairs)
    def _(j):
        arrive(j, 0)
        second(j, 0).start()
        arrive(j, 1)
        second(j, 1).start()
        term(across, j)
        term(along, j)

    @pl.loop(0, pairs)
    def _(j):
        arrive(j, 2)
        arrive(j, 3)
        term(corner, j)

    stage[...] = total[...].astype(stage.dtype)
    columns = pl.ds(pl.multiple_of(mine * width, width), width)

    def piece(owner):
        return pl.ds(pl.multiple_of(owner * share, share), share)

    back = [
        remote(stage.at[piece(p)], proj.at[:, columns], give.at[i], take.at[i], {"tp": p})
        for i, p in enumerate((corner, across, along))
    ]
    for c in back:
        c.start()
    proj[:, columns] = stage[piece(mine), :]
    for c in back:
        c.wait()
    mixed = (res_ref[...].astype(jnp.float32) + proj[...].astype(jnp.float32)).astype(mixed_ref.dtype)
    mixed_ref[...] = mixed
    mixed = mixed.astype(jnp.float32)
    mean = jnp.mean(mixed * mixed, axis=-1, keepdims=True)
    normed_ref[...] = (mixed * lax.rsqrt(mean + EPS) * gain_ref[...]).astype(normed_ref.dtype)

    for i, p in enumerate((corner, across, along)):
        remote(sheet, notes_ref.at[mine], tell.at[i], told.at[i], {"tp": p}).wait()

    def settle_sends():
        for c in inform:
            c.wait_send()
        for d in range(1, chips):
            p = lax.rem(chip + d, chips)
            to_plane(p).wait_send()
            sideways(p).wait_send()
        for p in range(chips):
            for side in range(2):
                hand(p, side).wait_send()
        for j in range(pairs):
            for way in range(2):
                first(j, way).wait_send()
                second(j, way).wait_send()

    return settle_sends


def visit(chip, chips, step):
    near = jnp.minimum(chip, chips - 1 - chip)
    up = chip < chips - 1 - chip
    swing = (step + 1) // 2 * (2 * lax.rem(step, 2) - 1)
    swing = jnp.where(up, chip + swing, chip - swing)
    tail = jnp.where(up, chip + (step - near), chip - (step - near))
    return jnp.where(step <= 2 * near, swing, tail)


def wide(value):
    return value.astype(jnp.float32)


def moe_part(
    n, cuts, x_ref, note_ref, mixed_ref, loads, out_ref,
    tok, wg, wu, wd, picked, hid, wsel, held, own, give, take,
    low, high, from_x, from_y, to_y, to_x, last_y, last_x, acc, zsend, zrecv, zmid,
    zs, zr, sq_s, sq_r, pd_s, pd_r, tk_s, tk_r, hop_s, hop_r, hz_s, hz_r, mid_r,
):
    me = lax.axis_index("sp")
    chips = n // 2
    chip, core = me // 2, lax.rem(me, 2)
    other = 1 - core
    partner = {"sp": 2 * chip + other}
    mine, across, along, corner = square()
    x, y = lax.rem(mine, 2), mine // 2
    share, depth = x_ref.shape
    units = wg.shape[1]
    group = 4 * share
    slots = wsel.shape[3] // 2
    width = depth // cuts
    half = width // 2
    steps = chips * cuts

    def column(k):
        return pl.ds(pl.multiple_of(k * width, width), width)

    has_right, has_left = chip < chips - 1, chip > 0

    def cols(h):
        return pl.ds(pl.multiple_of(h * (depth // 2), depth // 2), depth // 2)

    def own_half(h):
        return x_ref.at[:, cols(h)]

    def along_z(p, h, way, first=False):
        block = tok.at[p, core, h, mine]
        to = 2 * (chip + 1 - 2 * way) + core
        return remote(
            own_half(h) if first else block, block, zs.at[p, h, way], zr.at[p, h], {"sp": to}
        )

    upper, lower = pl.ds(0, share // 2), pl.ds(share // 2, share // 2)

    def pass_on(p, h, way, first=False):
        block = tok.at[p, core, h]
        start = own_half(h) if first else block.at[mine]
        src, dst, where = (
            (start, block.at[mine], across),
            (start, block.at[mine], along),
            (block.at[across, upper], block.at[across, upper], along),
            (block.at[along, lower], block.at[along, lower], across),
        )[way]
        return remote(src, dst, sq_s.at[way], sq_r.at[p, h, way], {"tp": where})

    def arrive(p, h, way):
        block = tok.at[p, core, h]
        dst = (
            block.at[across],
            block.at[along],
            block.at[corner, upper],
            block.at[corner, lower],
        )[way]
        remote(dst, dst, sq_s.at[way], sq_r.at[p, h, way], {"tp": across}).wait_recv()

    def hand(p, h, t, first=False):
        block = tok.at[p, core, h, t]
        src = own_half(h) if first else block
        return remote(src, block, pd_s.at[0], pd_r.at[p, h, t], partner)

    def handed(p, h, t):
        block = tok.at[p, other, h, t]
        remote(block, block, pd_s.at[0], pd_r.at[p, h, t], partner).wait_recv()

    for h in range(2):
        pass_on(chip, h, 0, True).start()
        pass_on(chip, h, 1, True).start()

        @pl.when(has_right)
        def _():
            along_z(chip, h, 0, True).start()

        @pl.when(has_left)
        def _():
            along_z(chip, h, 1, True).start()

        hand(chip, h, mine, True).start()
        tok[chip, core, h, mine] = x_ref[:, cols(h)]

    def part(u):
        return visit(chip, chips, u // 2), lax.rem(u, 2)

    def finish(u):
        p, h = part(u)
        arrive(p, h, 2)
        arrive(p, h, 3)
        hand(p, h, corner).start()

    def wait_rows(p):
        for h in range(2):
            for t in range(4):
                handed(p, h, t)

    def pick_rows(p, side):
        tiles = [note_ref[t, 2 * p + side] for t in range(4)]
        lane = lax.broadcasted_iota(jnp.int32, (n, 2 * share), 1)
        chosen = lax.broadcasted_iota(jnp.int32, (n, 2 * share), 0) == me

        def across_two(even, odd, swap_even):
            moved = pltpu.roll(even if swap_even else odd, share, 1)
            return jnp.where(lane < share, moved, odd) if swap_even else jnp.where(
                lane < share, even, moved
            )

        def row_of(swap_even):
            parts_two = [across_two(tiles[t], tiles[t + 1], swap_even) for t in (0, 2)]
            picks = [
                jnp.sum(jnp.where(chosen, v, 0.0), axis=0, keepdims=True) for v in parts_two
            ]
            return jnp.concatenate(picks, axis=1)

        spot = row_of(False)
        base = lax.broadcasted_iota(jnp.int32, (1, group), 1) // share * (slots // 4)
        spot = jnp.where(spot >= 0, spot.astype(jnp.int32) + base, -1)
        weight = row_of(True)
        coarse = weight.astype(jnp.bfloat16).astype(jnp.float32)
        parts = (coarse, weight - coarse)
        hit = lax.broadcasted_iota(jnp.int32, (slots, group), 0) == spot
        pick = jnp.where(hit, 1.0, 0.0).astype(tok.dtype)
        for i in range(2):
            turned = jnp.transpose(jnp.where(hit, parts[i], 0.0))
            wsel[p, side, :, i * slots : (i + 1) * slots] = turned.astype(wsel.dtype)
        for h in range(2):
            block = tok[p, side, h].reshape(group, depth // 2)
            rows = jnp.dot(pick, block, preferred_element_type=jnp.float32)
            picked[side * slots : (side + 1) * slots, cols(h)] = rows.astype(picked.dtype)

    def activate(p, u):
        some = pl.ds(pl.multiple_of(u * 512, 512), 512)
        gate = jnp.dot(picked[...], wg[:, some], preferred_element_type=jnp.float32)
        rise = jnp.dot(picked[...], wu[:, some], preferred_element_type=jnp.float32)
        hid[p, :, some] = (jax.nn.silu(gate) * rise).astype(hid.dtype)

    def expert(p):
        wait_rows(p)
        pick_rows(p, 0)
        pick_rows(p, 1)

        @pl.loop(0, units // 512)
        def _(u):
            activate(p, u)

    def forward(u):
        p, h = part(u)
        arrive(p, h, 0)
        pass_on(p, h, 2).start()
        hand(p, h, across).start()
        arrive(p, h, 1)
        pass_on(p, h, 3).start()
        hand(p, h, along).start()

    last = 2 * chips - 1

    def passes(p):
        return ((p < chip) & has_right) | ((p > chip) & has_left)

    def relay(u):
        p, h = part(u)

        @pl.when(passes(p))
        def _():
            along_z(p, h, 0).wait_recv()

        @pl.when((p < chip) & has_right)
        def _():
            along_z(p, h, 0).start()

        @pl.when((p > chip) & has_left)
        def _():
            along_z(p, h, 1).start()

    def open_up(u):
        p, h = part(u)

        @pl.when(jnp.logical_not(passes(p)))
        def _():
            along_z(p, h, 0).wait_recv()

        pass_on(p, h, 0).start()
        pass_on(p, h, 1).start()
        hand(p, h, mine).start()

    relay(2)
    open_up(2)

    @pl.loop(0, last)
    def _(u):
        forward(u)

        @pl.when(u + 4 <= last)
        def _():
            relay(u + 4)

        @pl.when(u == 0)
        def _():
            relay(3)

        @pl.when(u + 3 <= last)
        def _():
            open_up(u + 3)

        @pl.when(u == 0)
        def _():
            for c in loads:
                c.wait()

        @pl.when((u == 4) | ((u > 4) & (lax.rem(u, 2) == 1)))
        def _():
            expert(visit(chip, chips, (u - 3) // 2))

        @pl.when((u >= 2) & (lax.rem(u, 2) == 0))
        def _():
            finish(u - 2)

            @pl.when(u < last - 1)
            def _():
                finish(u - 1)

    def plane_of(k):
        return visit(chip, chips, lax.rem(k // cuts + 1, chips))

    def swap(k):
        return remote(give.at[k], take.at[k], tk_s.at[0], tk_r.at[k], partner)

    def hop(k, way):
        src, dst, where = (
            (low.at[k, 1 - x], from_x.at[k], across),
            (high.at[k, 1 - y], from_y.at[k], along),
            (to_y.at[k], last_y.at[k], along),
            (to_x.at[k], last_x.at[k], across),
        )[way]
        return remote(src, dst, hop_s.at[way], hop_r.at[k, way], {"tp": where})

    def home(k):
        p, q = plane_of(k), lax.rem(k, cuts)
        return remote(
            zsend.at[k], zrecv.at[chip, q], hz_s.at[0], hz_r.at[chip, q], {"sp": 2 * p + core}
        )

    is_end = (chip == 0) | (chip == chips - 1)

    def lend(k):
        to = chip + jnp.where(chip == 0, 1, -1)
        return remote(
            zsend.at[k], zmid.at[lax.rem(k, cuts)], hz_s.at[0], mid_r.at[lax.rem(k, cuts)],
            {"sp": 2 * to + core},
        )

    def homed(p, q):
        return remote(zsend.at[0], zrecv.at[p, q], hz_s.at[0], hz_r.at[p, q], partner)

    def settle(k):
        swap(k).wait_recv()
        total = own[lax.rem(k, 3)] + wide(take[k])
        cast = total.astype(low.dtype).reshape(4, share, width)
        for t in range(4):
            low[k, t % 2, t // 2] = cast[t, :, :half]
            high[k, t // 2, t % 2] = cast[t, :, half:]
        hop(k, 0).start()
        hop(k, 1).start()

    @pl.loop(0, steps + 6)
    def _(step):
        @pl.when((step >= 2) & (step < steps + 2))
        def _():
            settle(step - 2)

        @pl.when((step >= 4) & (step < steps + 4))
        def _(k=step - 4):
            hop(k, 0).wait_recv()
            to_y[k] = (wide(low[k, x, 1 - y]) + wide(from_x[k, 1 - y])).astype(to_y.dtype)
            hop(k, 2).start()
            hop(k, 1).wait_recv()
            to_x[k] = (wide(high[k, y, 1 - x]) + wide(from_y[k, 1 - x])).astype(to_x.dtype)
            hop(k, 3).start()

        @pl.when(step >= 6)
        def _(k=step - 6):
            hop(k, 2).wait_recv()
            left = wide(low[k, x, y]) + wide(from_x[k, y]) + wide(last_y[k])
            hop(k, 3).wait_recv()
            right = wide(high[k, y, x]) + wide(from_y[k, x]) + wide(last_x[k])

            far = (k >= steps - 2 * cuts) & (k < steps - cuts)

            @pl.when((k < steps - cuts) & jnp.logical_not(far & jnp.logical_not(is_end)))
            def _():
                zsend[k, :, :half] = left.astype(zsend.dtype)
                zsend[k, :, half:] = right.astype(zsend.dtype)

                @pl.when(far)
                def _():
                    lend(k).start()

                @pl.when(jnp.logical_not(far))
                def _():
                    home(k).start()

            @pl.when(far & jnp.logical_not(is_end))
            def _():
                lend(k).wait_recv()
                more = wide(zmid[lax.rem(k, cuts)])
                zsend[k, :, :half] = (left + more[:, :half]).astype(zsend.dtype)
                zsend[k, :, half:] = (right + more[:, half:]).astype(zsend.dtype)
                home(k).start()

            @pl.when(k >= steps - cuts)
            def _():
                acc[lax.rem(k, cuts), :, :half] = left
                acc[lax.rem(k, cuts), :, half:] = right

        @pl.when(step < steps)
        def _(k=step):
            third, fourth = visit(chip, chips, chips - 2), visit(chip, chips, chips - 1)

            @pl.when(k == cuts)
            def _():
                @pl.loop(0, units // 512)
                def _(u):
                    activate(third, u)

            p, q = plane_of(k), lax.rem(k, cuts)
            out = jnp.dot(hid[p], wd[q], preferred_element_type=jnp.float32).astype(held.dtype)
            for side in range(2):
                block = out[side * slots : (side + 1) * slots]
                held[side, :slots] = block
                held[side, slots:] = block

            def spread(side):
                return jnp.dot(wsel[p, side], held[side], preferred_element_type=jnp.float32)

            give[k] = spread(other).astype(give.dtype)
            swap(k).start()
            own[lax.rem(k, 3)] = spread(core)

            @pl.when(k == cuts // 2)
            def _():
                forward(last)
                finish(last - 2)

            @pl.when(k == cuts)
            def _():
                finish(last - 1)
                finish(last)

            @pl.when((k == cuts - 1) | (k == cuts + 1))
            def _():
                p = jnp.where(k < cuts, third, fourth)
                wait_rows(p)
                pick_rows(p, 0)
                pick_rows(p, 1)

            each = units // 1024

            @pl.when((k >= cuts + 2) & (k < cuts + 4))
            def _():
                @pl.loop(0, each)
                def _(u):
                    activate(fourth, (k - cuts - 2) * each + u)

    @pl.loop(0, cuts)
    def _(q):
        for d in range(1, chips):
            p = lax.rem(chip + d, chips)

            @pl.when(jnp.logical_not(is_end & (p == chips - 1 - chip)))
            def _():
                homed(p, q).wait_recv()
                acc[q] += wide(zrecv[p, q])

        out_ref[:, column(q)] = (acc[q] + wide(mixed_ref[:, column(q)])).astype(out_ref.dtype)

    @pl.loop(0, 2 * chips)
    def _(u):
        p, h = u // 2, lax.rem(u, 2)
        @pl.when((p <= chip) & has_right)
        def _():
            along_z(p, h, 0).wait_send()

        @pl.when((p >= chip) & has_left)
        def _():
            along_z(p, h, 1).wait_send()

    def all_left(ref, sem):
        remote(ref, ref, sem, sem, partner).wait_send()

    whole = tok.at[:, 0, :, 0]
    for way, ref in enumerate((whole, whole, whole.at[:, :, upper], whole.at[:, :, lower])):
        all_left(ref, sq_s.at[way])
    all_left(tok.at[:, 0], pd_s.at[0])
    all_left(give, tk_s.at[0])
    for way, ref in enumerate((from_x, from_y, to_y, to_x)):
        all_left(ref, hop_s.at[way])
    all_left(zsend, hz_s.at[0])


def layer_kernel(n, cuts, *refs):
    attend_in, (wg_ref, wu_ref, wd_ref, out_ref), refs = refs[:12], refs[12:16], refs[16:]
    (mixed, normed, notes, load), refs = refs[:4], refs[4:]
    attend_room, moe_room = refs[:27], refs[27:]
    tok, wg, wu, wd = moe_room[:4]
    width = wd.shape[2]
    loads = [
        pltpu.make_async_copy(wg_ref.at[0], wg, load.at[0]),
        pltpu.make_async_copy(wu_ref.at[0], wu, load.at[1]),
    ] + [
        pltpu.make_async_copy(wd_ref.at[0, :, pl.ds(q * width, width)], wd.at[q], load.at[2 + q])
        for q in range(cuts)
    ]
    settle_sends = attend_part(n, *attend_in, mixed, normed, notes, loads, *attend_room)
    moe_part(n, cuts, normed, notes, mixed, loads, out_ref, *moe_room)
    settle_sends()


def layer(
    n, queries, keys, values, query_gain, key_gain, residual, gain, names, shares, out_proj,
    w_gate, w_up, w_down, capacity, cuts=4,
):
    rows, width = queries.shape
    size = query_gain.shape[0]
    heads = width // size
    share, depth = residual.shape
    units = w_gate.shape[2]
    chips = n // 2
    kind = queries.dtype
    cut = depth // cuts
    half = cut // 2
    steps = chips * cuts
    group, slots = 4 * share, 4 * capacity
    by_col, by_row = turn_tables(size, n * rows // GRID_W)
    dma = pltpu.SemaphoreType.DMA

    def room(*extent):
        return pltpu.VMEM(extent, kind)

    def exact(*extent):
        return pltpu.VMEM(extent, jnp.float32)

    return pl.pallas_call(
        functools.partial(layer_kernel, n, cuts),
        out_shape=jax.ShapeDtypeStruct((share, depth), kind),
        in_specs=in_vmem(11) + [pl.BlockSpec(memory_space=pl.ANY)] * 4,
        out_specs=in_vmem(1)[0],
        scratch_shapes=[
            room(share, depth),
            room(share, depth),
            exact(4, n, n, 2 * share),
            dma((2 + cuts,)),
            room(*out_proj.shape),
            room(chips, 2, 2, 2, rows // 2, size),
            room(heads, rows, size),
            exact(heads, rows, size),
            exact(heads, rows, 2 * size),
            room(4, heads // 2, rows, 2 * size),
            exact(rows, width),
            room(rows, width),
            room(share, depth),
            exact(n, n, 2 * share),
            dma((1,)),
            dma((chips,)),
            dma((chips,)),
            dma((chips,)),
            dma((chips,)),
            dma((chips, 2)),
            dma((chips, 2)),
            dma((n - 1,)),
            dma((n - 1,)),
            dma((heads // 2, 4)),
            dma((heads // 2, 4)),
            dma((3,)),
            dma((3,)),
            dma((3,)),
            dma((3,)),
            exact(n, 2 * share),
            exact(n, 2 * share),
            room(chips, 2, 2, 4, share, depth // 2),
            room(depth, units),
            room(depth, units),
            room(cuts, units, cut),
            room(2 * slots, depth),
            room(chips, 2 * slots, units),
            room(chips, 2, group, 2 * slots),
            room(2, 2 * slots, cut),
            exact(3, group, cut),
            room(steps, group, cut),
            room(steps, group, cut),
            room(steps, 2, 2, share, half),
            room(steps, 2, 2, share, half),
            room(steps, 2, share, half),
            room(steps, 2, share, half),
            room(steps, share, half),
            room(steps, share, half),
            room(steps, share, half),
            room(steps, share, half),
            exact(cuts, share, cut),
            room(steps - cuts, share, cut),
            room(chips, cuts, share, cut),
            room(cuts, share, cut),
            dma((chips, 2, 2)),
            dma((chips, 2)),
            dma((4,)),
            dma((chips, 2, 4)),
            dma((1,)),
            dma((chips, 2, 4)),
            dma((1,)),
            dma((steps,)),
            dma((4,)),
            dma((steps, 4)),
            dma((1,)),
            dma((chips, cuts)),
            dma((cuts,)),
        ],
        compiler_params=params(0),
        name="layer",
    )(
        queries,
        keys,
        values,
        query_gain[None, :],
        key_gain[None, :],
        jnp.asarray(by_col),
        jnp.asarray(by_row),
        residual,
        gain[None, :],
        names,
        shares,
        out_proj,
        w_gate,
        w_up,
        w_down,
    )


def start_state(batch, rows, width):
    return (
        jnp.full((batch, rows), NEG_START, jnp.float32),
        jnp.zeros((batch, rows), jnp.float32),
        jnp.zeros((batch, rows, width), jnp.float32),
    )


def local(
    queries,
    keys,
    values,
    query_gain,
    key_gain,
    out_proj,
    expert_norm_scale,
    residual,
    routes,
    route_weights,
    w_gate,
    w_up,
    w_down,
):
    head_size = query_gain.shape[0]
    tok_sp = queries.shape[0]
    tp_count = lax.axis_size("tp")
    sp_count = lax.axis_size("sp")
    heads_dev = queries.shape[1] // head_size
    all_heads = heads_dev * tp_count
    kv_heads = keys.shape[1] // head_size
    group = all_heads // kv_heads
    scale = head_size ** (-0.5)
    tp_index = lax.axis_index("tp")
    sp_index = lax.axis_index("sp")
    tok_dev = residual.shape[0]
    top = routes.shape[1]
    capacity = max(2, 2 * tok_dev * top // sp_count)
    direct = (
        tp_count == 4
        and sp_count // 2 == 4
        and sp_count % 2 == 0
        and capacity % 16 == 0
        and 2 * tok_dev % 128 == 0
        and tok_sp % (2 * GRID_W) == 0
        and heads_dev % 2 == 0
        and 2 * heads_dev <= group
        and tok_sp == tp_count * tok_dev
    )
    if direct:
        return layer(
            sp_count,
            queries,
            keys,
            values,
            query_gain,
            key_gain,
            residual,
            expert_norm_scale,
            routes.T,
            route_weights.T,
            out_proj,
            w_gate,
            w_up,
            w_down,
            capacity,
        )
    position = sp_index * tok_sp + jnp.arange(tok_sp, dtype=jnp.int32)
    q_rot = prepare(queries, query_gain, position)
    shared_value_head = tp_index * heads_dev // group
    own_keys = prepare(
        lax.dynamic_slice_in_dim(keys, shared_value_head * head_size, head_size, 1),
        key_gain,
        position,
    )
    own_values = lax.dynamic_slice_in_dim(values, shared_value_head * head_size, head_size, 1)
    query_matrix = (
        q_rot.reshape(tok_sp, heads_dev, head_size)
        .transpose(1, 0, 2)
        .reshape(1, heads_dev * tok_sp, head_size)
    )
    key_piece = lax.all_gather(own_keys, "sp", axis=0, tiled=True)
    value_piece = lax.all_gather(own_values, "sp", axis=0, tiled=True)
    run_max, run_sum, run_acc = absorb(
        start_state(1, heads_dev * tok_sp, head_size),
        query_matrix,
        key_piece[:, None, :],
        value_piece[:, None, :],
        scale,
    )
    attn = (run_acc / run_sum[..., None]).astype(jnp.bfloat16)
    attn = (
        attn.reshape(heads_dev, tok_sp, head_size)
        .transpose(1, 0, 2)
        .reshape(tok_sp, heads_dev * head_size)
    )
    columns = jnp.dot(
        lax.all_gather(attn, "tp", axis=1, tiled=True),
        out_proj,
        preferred_element_type=jnp.float32,
    )
    projected = lax.all_to_all(
        columns.astype(jnp.bfloat16), "tp", split_axis=0, concat_axis=1, tiled=True
    )
    mixed_float_output = residual.astype(jnp.float32) + projected.astype(jnp.float32)
    mixed = mixed_float_output.astype(jnp.bfloat16)
    mixed_float_output = mixed.astype(jnp.float32)
    normed = (
        mixed_float_output
        * lax.rsqrt(jnp.mean(mixed_float_output * mixed_float_output, axis=-1, keepdims=True) + EPS)
        * expert_norm_scale
    ).astype(jnp.bfloat16)
    flat_routes = routes.reshape(-1)
    one_hot = (flat_routes[:, None] == jnp.arange(sp_count, dtype=jnp.int32)[None, :]).astype(
        jnp.int32
    )
    earlier = jnp.cumsum(one_hot, axis=0) - one_hot
    slot_index = jnp.sum(earlier * one_hot, axis=1)
    target = flat_routes * capacity + slot_index
    selector = (
        jnp.arange(sp_count * capacity, dtype=jnp.int32)[:, None] == target[None, :]
    ).astype(jnp.bfloat16)
    selector = jnp.sum(selector.reshape(sp_count * capacity, tok_dev, top), axis=2)
    send_rows = jnp.dot(selector, normed, preferred_element_type=jnp.float32).astype(jnp.bfloat16)
    arrived = lax.all_to_all(send_rows, "sp", split_axis=0, concat_axis=0, tiled=True)
    piece = lax.all_gather(arrived, "tp", axis=0, tiled=True)
    gate = jnp.dot(piece, w_gate[0], preferred_element_type=jnp.float32)
    upper = jnp.dot(piece, w_up[0], preferred_element_type=jnp.float32)
    hidden = (jax.nn.silu(gate) * upper).astype(jnp.bfloat16)
    partial = jnp.dot(hidden, w_down[0], preferred_element_type=jnp.float32).astype(jnp.bfloat16)
    expert_out = lax.psum_scatter(partial, "tp", scatter_dimension=0, tiled=True)
    returned = lax.all_to_all(expert_out, "sp", split_axis=0, concat_axis=0, tiled=True)
    picked = (
        jnp.take(returned, target, axis=0)
        .astype(jnp.float32)
        .reshape(tok_dev, top, returned.shape[1])
    )
    moe_sum = jnp.sum(picked * route_weights[:, :, None], axis=1)
    return (mixed_float_output + moe_sum).astype(jnp.bfloat16)


def solution(mesh):
    placed = (
        P("sp", "tp"),
        P("sp", None),
        P("sp", None),
        P(),
        P(),
        P(None, "tp"),
        P(),
        P(("sp", "tp"), None),
        P(("sp", "tp"), None),
        P(("sp", "tp"), None),
        P("sp", None, "tp"),
        P("sp", None, "tp"),
        P("sp", "tp", None),
    )
    return jax.shard_map(
        local, mesh=mesh, in_specs=placed, out_specs=P(("sp", "tp"), None), check_vma=False
    )
```

time: 124 us -> 117 us (0.944)
  Pallas kernels: 119 us -> 115 us
  other arithmetic: 1.79 us -> 0 us
    pallas_call x2 -> x1, Pallas kernels: 119 us -> 115 us  [layer(): pl.pallas_call(functools.partial(layer_kernel, n, cuts), out_shape=jax.Sh...]
    convert_element_type x1 -> x0, other arithmetic: 1.79 us -> none  [local(): return (mixed.astype(jnp.float32) + summed).astype(jnp.bfloat16)]
    unnamed x4 -> x1, local copies, waits for them, and re-layouts: 2.75 us -> 1.67 us
where the time goes in v5:
time: 117 us
  Pallas kernels  115 us (98%)
  local copies, waits for them, and re-layouts  1.67 us (1%)
    pallas_call x1, Pallas kernels, layer(): pl.pallas_call(functools.partial(layer_kernel, n, cuts), out_shape=jax.Sh...  115 us

profile of v5, /device:TPU:0, one launch (start us, length us, event | category | flops | bytes accessed | tf_op | source)
XLA Modules:
  0.0 116.7 jit_solution(9916285608289035220)
XLA Ops:
  0.0 115.0 %layer.1 = bf16[64,2048]{1,0:T(8,128)(2,1)} custom-call(bf16[256,512]{1,0:T(8,128)(2,1)} %refs_0_.1, bf16[256,256]{1,0:T(8,128)(2,1)} %refs_1_.1, bf16[256,256]{1,0:T(8,128)(2,1)} %refs_2_.1, f32[1,128]{1,0:T(1,128)} %bitcast.8, f32[1,128]{1,0:T(1,128)} %bitcast.9, f32[3,64,128]{2,1,0:T(8,128)} %constant.4.clone.refs_5_, ...), custom_call_target="tpu_custom_call" | custom-call | tf_op jit(solution)/shard_map/layer/pallas_call | solution.py:868
  115.0 1.7 %copy.17 = bf16[64,2048]{1,0:T(8,128)(2,1)} copy(bf16[64,2048]{1,0:T(8,128)(2,1)} %layer.1) | data formatting | bytes 524288

commit v6 on v5

--- a/solution.py
+++ b/solution.py
@@ -196,6 +196,17 @@
     weight = jnp.where(first_one, first_part, 0.0) + jnp.where(second_one, second_part, 0.0)
     sheet[me] = jnp.where(lanes < share, jnp.where(taken > 0, slot, -1.0), weight)
 
+    @pl.loop(0, heads // 2)
+    def _(h):
+        @pl.loop(0, rows // GRID_W)
+        def _(g):
+            span = pl.ds(pl.multiple_of(g * GRID_W, GRID_W), GRID_W)
+            block = q_ref[span, pl.ds(pl.multiple_of(h * size, size), size)]
+            qs[h, span] = turned(block, qg_ref[...], g)
+
+        top[h] = jnp.full(top.shape[1:], NEG_START, jnp.float32)
+        acc[h] = jnp.zeros(acc.shape[1:], jnp.float32)
+
     pl.semaphore_wait(barrier, n + 2)
 
     def to_plane(p):
@@ -241,7 +252,7 @@
     for c in inform:
         c.start()
 
-    @pl.loop(0, heads)
+    @pl.loop(heads // 2, heads)
     def _(h):
         @pl.loop(0, rows // GRID_W)
         def _(g):
@@ -425,6 +436,7 @@
     tok, wg, wu, wd, picked, hid, wsel, held, own, give, take,
     low, high, from_x, from_y, to_y, to_x, last_y, last_x, acc, zsend, zrecv, zmid,
     zs, zr, sq_s, sq_r, pd_s, pd_r, tk_s, tk_r, hop_s, hop_r, hz_s, hz_r, mid_r,
+    outbox, inbox, out_s, in_r, kept,
 ):
     me = lax.axis_index("sp")
     chips = n // 2
@@ -609,13 +621,15 @@
         pass_on(p, h, 1).start()
         hand(p, h, mine).start()
 
-    relay(2)
-    open_up(2)
-
     @pl.loop(0, last)
     def _(u):
         forward(u)
 
+        @pl.when(u == 0)
+        def _():
+            relay(2)
+            open_up(2)
+
         @pl.when(u + 4 <= last)
         def _():
             relay(u + 4)
@@ -645,8 +659,19 @@
             def _():
                 finish(u - 1)
 
+    fold = cuts - 1
+
+    def is_whole(k):
+        return k == 0
+
+    def rank_of(k):
+        return lax.rem(k // cuts + 1, chips)
+
+    def cut_of(k):
+        return lax.rem(jnp.where(k < cuts, k + fold, k), cuts)
+
     def plane_of(k):
-        return visit(chip, chips, lax.rem(k // cuts + 1, chips))
+        return visit(chip, chips, rank_of(k))
 
     def swap(k):
         return remote(give.at[k], take.at[k], tk_s.at[0], tk_r.at[k], partner)
@@ -661,7 +686,7 @@
         return remote(src, dst, hop_s.at[way], hop_r.at[k, way], {"tp": where})
 
     def home(k):
-        p, q = plane_of(k), lax.rem(k, cuts)
+        p, q = plane_of(k), cut_of(k)
         return remote(
             zsend.at[k], zrecv.at[chip, q], hz_s.at[0], hz_r.at[chip, q], {"sp": 2 * p + core}
         )
@@ -671,22 +696,48 @@
     def lend(k):
         to = chip + jnp.where(chip == 0, 1, -1)
         return remote(
-            zsend.at[k], zmid.at[lax.rem(k, cuts)], hz_s.at[0], mid_r.at[lax.rem(k, cuts)],
+            zsend.at[k], zmid.at[cut_of(k)], hz_s.at[0], mid_r.at[cut_of(k)],
             {"sp": 2 * to + core},
         )
 
     def homed(p, q):
         return remote(zsend.at[0], zrecv.at[p, q], hz_s.at[0], hz_r.at[p, q], partner)
+
+    def whole_to(k):
+        p, i = plane_of(k), cut_of(k) - fold
+        spot = jnp.where(chip < p, 0, 1)
+        return remote(
+            outbox.at[i], inbox.at[spot, i], out_s.at[i], in_r.at[spot, i], {"sp": 2 * p + core}
+        )
 
     def settle(k):
         swap(k).wait_recv()
         total = own[lax.rem(k, 3)] + wide(take[k])
-        cast = total.astype(low.dtype).reshape(4, share, width)
-        for t in range(4):
-            low[k, t % 2, t // 2] = cast[t, :, :half]
-            high[k, t // 2, t % 2] = cast[t, :, half:]
-        hop(k, 0).start()
-        hop(k, 1).start()
+
+        @pl.when(is_whole(k))
+        def _():
+            outbox[cut_of(k) - fold] = total.astype(outbox.dtype)
+            whole_to(k).start()
+
+        @pl.when(jnp.logical_not(is_whole(k)))
+        def _():
+            own[lax.rem(k, 3)] = total
+
+            @pl.when((k == steps - 1) & jnp.logical_not(is_end))
+            def _():
+                i = 0
+                for spot in range(2):
+                    remote(
+                        outbox.at[i], inbox.at[spot, i], out_s.at[i], in_r.at[spot, i], partner
+                    ).wait_recv()
+                    own[lax.rem(k, 3)] += wide(inbox[spot, i])
+
+            cast = own[lax.rem(k, 3)].astype(low.dtype).reshape(4, share, width)
+            for t in range(4):
+                low[k, t % 2, t // 2] = cast[t, :, :half]
+                high[k, t // 2, t % 2] = cast[t, :, half:]
+            hop(k, 0).start()
+            hop(k, 1).start()
 
     @pl.loop(0, steps + 6)
     def _(step):
@@ -694,7 +745,7 @@
         def _():
             settle(step - 2)
 
-        @pl.when((step >= 4) & (step < steps + 4))
+        @pl.when((step >= 4) & (step < steps + 4) & jnp.logical_not(is_whole(step - 4)))
         def _(k=step - 4):
             hop(k, 0).wait_recv()
             to_y[k] = (wide(low[k, x, 1 - y]) + wide(from_x[k, 1 - y])).astype(to_y.dtype)
@@ -703,16 +754,16 @@
             to_x[k] = (wide(high[k, y, 1 - x]) + wide(from_y[k, 1 - x])).astype(to_x.dtype)
             hop(k, 3).start()
 
-        @pl.when(step >= 6)
+        @pl.when((step >= 6) & jnp.logical_not(is_whole(step - 6)))
         def _(k=step - 6):
             hop(k, 2).wait_recv()
             left = wide(low[k, x, y]) + wide(from_x[k, y]) + wide(last_y[k])
             hop(k, 3).wait_recv()
             right = wide(high[k, y, x]) + wide(from_y[k, x]) + wide(last_x[k])
 
-            far = (k >= steps - 2 * cuts) & (k < steps - cuts)
-
-            @pl.when((k < steps - cuts) & jnp.logical_not(far & jnp.logical_not(is_end)))
+            far, own_plane = rank_of(k) == chips - 1, rank_of(k) == 0
+
+            @pl.when(jnp.logical_not(own_plane | (far & jnp.logical_not(is_end))))
             def _():
                 zsend[k, :, :half] = left.astype(zsend.dtype)
                 zsend[k, :, half:] = right.astype(zsend.dtype)
@@ -727,16 +778,22 @@
 
             @pl.when(far & jnp.logical_not(is_end))
             def _():
-                lend(k).wait_recv()
-                more = wide(zmid[lax.rem(k, cuts)])
-                zsend[k, :, :half] = (left + more[:, :half]).astype(zsend.dtype)
-                zsend[k, :, half:] = (right + more[:, half:]).astype(zsend.dtype)
-                home(k).start()
-
-            @pl.when(k >= steps - cuts)
+                kept[cut_of(k), :, :half] = left
+                kept[cut_of(k), :, half:] = right
+
+            @pl.when(own_plane)
             def _():
-                acc[lax.rem(k, cuts), :, :half] = left
-                acc[lax.rem(k, cuts), :, half:] = right
+                acc[cut_of(k), :, :half] = left
+                acc[cut_of(k), :, half:] = right
+
+        due = step - 8
+
+        @pl.when((due >= 2 * cuts) & (due < 3 * cuts) & jnp.logical_not(is_end))
+        def _():
+            lend(due).wait_recv()
+            q = cut_of(due)
+            zsend[due] = (kept[q] + wide(zmid[q])).astype(zsend.dtype)
+            home(due).start()
 
         @pl.when(step < steps)
         def _(k=step):
@@ -748,7 +805,7 @@
                 def _(u):
                     activate(third, u)
 
-            p, q = plane_of(k), lax.rem(k, cuts)
+            p, q = plane_of(k), cut_of(k)
             out = jnp.dot(hid[p], wd[q], preferred_element_type=jnp.float32).astype(held.dtype)
             for side in range(2):
                 block = out[side * slots : (side + 1) * slots]
@@ -792,7 +849,9 @@
         for d in range(1, chips):
             p = lax.rem(chip + d, chips)
 
-            @pl.when(jnp.logical_not(is_end & (p == chips - 1 - chip)))
+            folded = jnp.logical_not(is_end) & (jnp.abs(p - chip) == 1) & (q >= fold)
+
+            @pl.when(jnp.logical_not((is_end & (p == chips - 1 - chip)) | folded))
             def _():
                 homed(p, q).wait_recv()
                 acc[q] += wide(zrecv[p, q])
@@ -813,14 +872,16 @@
     def all_left(ref, sem):
         remote(ref, ref, sem, sem, partner).wait_send()
 
-    whole = tok.at[:, 0, :, 0]
-    for way, ref in enumerate((whole, whole, whole.at[:, :, upper], whole.at[:, :, lower])):
+    blocks = tok.at[:, 0, :, 0]
+    halves = (blocks.at[:, :, upper], blocks.at[:, :, lower])
+    for way, ref in enumerate((blocks, blocks) + halves):
         all_left(ref, sq_s.at[way])
     all_left(tok.at[:, 0], pd_s.at[0])
     all_left(give, tk_s.at[0])
     for way, ref in enumerate((from_x, from_y, to_y, to_x)):
-        all_left(ref, hop_s.at[way])
-    all_left(zsend, hz_s.at[0])
+        all_left(ref.at[pl.ds(0, steps - 1)], hop_s.at[way])
+    all_left(zsend.at[pl.ds(0, steps - cuts - 1)], hz_s.at[0])
+    whole_to(0).wait_send()
 
 
 def layer_kernel(n, cuts, *refs):
@@ -922,7 +983,7 @@
             room(steps, share, half),
             room(steps, share, half),
             exact(cuts, share, cut),
-            room(steps - cuts, share, cut),
+            room(steps, share, cut),
             room(chips, cuts, share, cut),
             room(cuts, share, cut),
             dma((chips, 2, 2)),
@@ -938,6 +999,11 @@
             dma((1,)),
             dma((chips, cuts)),
             dma((cuts,)),
+            room(1, group, cut),
+            room(2, 1, group, cut),
+            dma((1,)),
+            dma((2, 1)),
+            exact(cuts, share, cut),
         ],
         compiler_params=params(0),
         name="layer",

time: 117 us -> 116 us (level)
  no operation moved by 1% of the time
where the time goes in v6:
time: 116 us
  Pallas kernels  114 us (98%)
  local copies, waits for them, and re-layouts  1.67 us (1%)
    pallas_call x1, Pallas kernels, layer(): pl.pallas_call(functools.partial(layer_kernel, n, cuts), out_shape=jax.Sh...  114 us

profile of v6, /device:TPU:0, one launch (start us, length us, event | category | flops | bytes accessed | tf_op | source)
XLA Modules:
  0.0 115.7 jit_solution(8753220180569209690)
XLA Ops:
  0.0 114.0 %layer.1 = bf16[64,2048]{1,0:T(8,128)(2,1)} custom-call(bf16[256,512]{1,0:T(8,128)(2,1)} %refs_0_.1, bf16[256,256]{1,0:T(8,128)(2,1)} %refs_1_.1, bf16[256,256]{1,0:T(8,128)(2,1)} %refs_2_.1, f32[1,128]{1,0:T(1,128)} %bitcast.8, f32[1,128]{1,0:T(1,128)} %bitcast.9, f32[3,64,128]{2,1,0:T(8,128)} %constant.4.clone.refs_5_, ...), custom_call_target="tpu_custom_call" | custom-call | tf_op jit(solution)/shard_map/layer/pallas_call | solution.py:929
  114.0 1.7 %copy.17 = bf16[64,2048]{1,0:T(8,128)(2,1)} copy(bf16[64,2048]{1,0:T(8,128)(2,1)} %layer.1) | data formatting | bytes 524288
